TPU v7x, 512 devices: a whole 4x4x16 slice. The times are simulated.
512 devices in a mesh: kv: 16 (over y, x), tp: 32 (over z, core).
Axes of the slice: x: 4, y: 4, z: 16, core: 2. Of those that a mesh axis runs over, the one named last changes fastest.
Arguments:
- tokens: bfloat16 [128, 4, 4096], P(None, None, ('kv', 'tp')), may hold values from -36 to 36
- lengths: int32 [128], replicated, may hold values from 1 to 4, 224 in all
- state: float32 [128, 128, 4096], P('kv', None, 'tp'), may hold values from -0.6 to 0.6
- attn_gain: float32 [4096], P('kv'), may hold values from 0.1 to 1.9
- w_query: bfloat16 [4096, 4096], P('kv', 'tp'), may hold values from -0.09375 to 0.09375
- w_key: bfloat16 [4096, 4096], P('kv', 'tp'), may hold values from -0.09375 to 0.09375
- w_value: bfloat16 [4096, 4096], P('kv', 'tp'), may hold values from -0.09375 to 0.09375
- w_beta: bfloat16 [4096, 32], replicated, may hold values from -0.09375 to 0.09375
- w_alpha: bfloat16 [4096, 32], replicated, may hold values from -0.09375 to 0.09375
- decay_rate: float32 [32], replicated, may hold values from 0.05 to 3
- decay_bias: float32 [32], replicated, may hold values from -3 to 3
- out_gain: float32 [128], replicated, may hold values from 0.1 to 1.9
- w_out: bfloat16 [4096, 4096], P('tp', 'kv'), may hold values from -0.09375 to 0.09375
- mix_gain: float32 [4096], P('kv'), may hold values from 0.1 to 1.9
- w_gate: bfloat16 [4096, 11008], P('kv', 'tp'), may hold values from -0.09375 to 0.09375
- w_up: bfloat16 [4096, 11008], P('kv', 'tp'), may hold values from -0.09375 to 0.09375
- w_down: bfloat16 [11008, 4096], P('tp', 'kv'), may hold values from -0.0546875 to 0.0546875
Outputs:
- mixed: bfloat16 [128, 4, 4096], P(None, None, ('kv', 'tp'))
- new_state: float32 [128, 128, 4096], P('kv', None, 'tp')
Inputs may be any that keep to these rules, and one draw needn't show every extreme that they name: Each sequence has 1 to 4 live tokens, the first ones of its block, and the lengths sum to 224.
All inputs are finite; a program needn't handle non-finite values.
Results may differ from a plain program's by a relative error of at most 0.015.
Values may be sent and summed in bfloat16 or wider, within the bound.
No kernel may reach another device: no remote copies, remote signals or barrier semaphores. Data moves between devices by JAX's collectives and lax.ppermute only.
A program may use at most 64 MiB of HBM per device.

v0:
```python
import math

import jax
import jax.numpy as jnp
from jax import lax
from jax.sharding import PartitionSpec as P

D = 4096
HEAD_DIM = 128


EPSILON = 1e-06


def joined_along(tiles, dim):
    dims = list(tiles.shape[1:])
    dims[dim] *= tiles.shape[0]
    return jnp.moveaxis(tiles, 0, dim).reshape(dims)


def copy_for_each(shard, axis):
    length = lax.axis_size(axis)
    return lax.all_to_all(
        jnp.broadcast_to(shard[None], (length, *shard.shape)), axis, 0, 0, tiled=True
    )


def gather_directly(shard, axis, dim):
    return joined_along(copy_for_each(shard, axis), dim)


def in_blocks(shard, dim, length):
    before, after = (shard.shape[:dim], shard.shape[dim + 1 :])
    return jnp.moveaxis(shard.reshape(*before, length, -1, *after), dim, 0)


def summed_on_arrival(shard, axis, dim):
    tiles = in_blocks(shard, dim, lax.axis_size(axis))
    arrived = lax.all_to_all(tiles, axis, split_axis=0, concat_axis=0, tiled=True)
    return arrived.astype(jnp.float32).sum(axis=0)


def sent_together(arrays, axis, dim, along):
    widths = [math.prod(a.shape[along:]) for a in arrays]
    both = jnp.concatenate(
        [a.reshape(*a.shape[:along], w) for a, w in zip(arrays, widths)], axis=along
    )
    out = summed_on_arrival(both, axis, dim)
    tiles = jnp.split(out, [sum(widths[:k]) for k in range(1, len(widths))], axis=along)
    return tuple((b.reshape(*out.shape[:along], *a.shape[along:]) for a, b in zip(arrays, tiles)))


def unit_rows(vectors):
    return vectors * lax.rsqrt(jnp.sum(vectors * vectors, axis=-1, keepdims=True) + EPSILON)


def delta_block(queries, unit_keys, values_split, beta, log_decay, carried):
    highest = lax.Precision.HIGHEST
    seq_count, span_len, heads_here = beta.shape
    cumulative = jnp.cumsum(log_decay, axis=1)
    position = jnp.arange(span_len)
    inclusive = (position[:, None] >= position[None, :])[None, :, :, None]
    strict = (position[:, None] > position[None, :])[None, :, :, None]
    gap_matrix = cumulative[:, :, None, :] - cumulative[:, None, :, :]
    decay_matrix = jnp.where(inclusive, jnp.exp(jnp.where(inclusive, gap_matrix, 0.0)), 0.0)
    key_dots = jnp.einsum("nihd,njhd->nijh", unit_keys, unit_keys, precision=highest)
    query_dots = jnp.einsum("nihd,njhd->nijh", queries, unit_keys, precision=highest) * decay_matrix
    lower_part = jnp.where(strict, key_dots * decay_matrix * beta[:, :, None, :], 0.0)
    identity = jnp.eye(span_len, dtype=jnp.float32)
    inverse_rows = []
    for step in range(span_len):
        row_now = jnp.broadcast_to(identity[step][None, :, None], (seq_count, span_len, heads_here))
        for prior in range(step):
            row_now = row_now - lower_part[:, step, prior, :][:, None, :] * inverse_rows[prior]
        inverse_rows.append(row_now)
    inverse = jnp.stack(inverse_rows, axis=1)
    beta_value = beta[..., None] * values_split
    beta_key = (beta * jnp.exp(cumulative))[..., None] * unit_keys
    base_update = jnp.einsum("nich,nche->nihe", inverse, beta_value, precision=highest)
    key_weights = jnp.einsum("nich,nchd->nihd", inverse, beta_key, precision=highest)
    corrected = base_update - jnp.einsum("nihd,ndhe->nihe", key_weights, carried, precision=highest)
    decayed_queries = queries * jnp.exp(cumulative)[..., None]
    attended = jnp.einsum("nihd,ndhe->nihe", decayed_queries, carried, precision=highest)
    attended = attended + jnp.einsum("nijh,njhe->nihe", query_dots, corrected, precision=highest)
    block_total = cumulative[:, -1, :]
    key_tail = unit_keys * jnp.exp(block_total[:, None, :] - cumulative)[..., None]
    updated = carried * jnp.exp(block_total)[:, None, :, None]
    updated = updated + jnp.einsum("nihd,nihe->ndhe", key_tail, corrected, precision=highest)
    return (attended, updated)


def body(
    tokens,
    lengths,
    state,
    attn_gain,
    w_query,
    w_key,
    w_value,
    w_beta,
    w_alpha,
    decay_rate,
    decay_bias,
    out_gain,
    w_out,
    mix_gain,
    w_gate,
    w_up,
    w_down,
):
    kv_index = lax.axis_index("kv")
    tp_index = lax.axis_index("tp")
    kv_count = lax.axis_size("kv")
    batch_all, span_len, own_cols = tokens.shape
    row_count = batch_all * span_len
    seq_count = state.shape[0]
    local_rows = seq_count * span_len
    head_size = state.shape[1]
    heads_here = state.shape[2] // head_size
    block_width = attn_gain.shape[0]
    flat_rows = tokens.reshape(row_count, own_cols)
    live_all = (jnp.arange(span_len, dtype=jnp.int32)[None, :] < lengths[:, None]).reshape(
        row_count, 1
    )
    gathered = gather_directly(flat_rows, "tp", 1).astype(jnp.float32)
    squares_in = jnp.sum(gathered * gathered, axis=1)
    normed_in = (gathered * attn_gain).astype(jnp.bfloat16)
    beta_rows = lax.dynamic_slice_in_dim(w_beta, kv_index * block_width, block_width, 0)
    alpha_rows = lax.dynamic_slice_in_dim(w_alpha, kv_index * block_width, block_width, 0)
    query_part = jnp.dot(normed_in, w_query, preferred_element_type=jnp.float32)
    key_part = jnp.dot(normed_in, w_key, preferred_element_type=jnp.float32)
    value_part = jnp.dot(normed_in, w_value, preferred_element_type=jnp.float32)
    beta_part = jnp.dot(normed_in, beta_rows, preferred_element_type=jnp.float32)
    alpha_part = jnp.dot(normed_in, alpha_rows, preferred_element_type=jnp.float32)
    query_sum, key_sum, value_sum, beta_sum, alpha_sum, squares_own = sent_together(
        (
            query_part.astype(jnp.bfloat16),
            key_part.astype(jnp.bfloat16),
            value_part.astype(jnp.bfloat16),
            beta_part.astype(jnp.bfloat16),
            alpha_part.astype(jnp.bfloat16),
            squares_in.astype(jnp.bfloat16),
        ),
        "kv",
        0,
        1,
    )
    row_scale = lax.rsqrt(squares_own / D + EPSILON)[:, None]
    head_start = tp_index * heads_here
    lengths_own = lax.dynamic_slice_in_dim(lengths, kv_index * seq_count, seq_count, 0)
    live_own = (jnp.arange(span_len, dtype=jnp.int32)[None, :] < lengths_own[:, None])[..., None]
    beta_heads = lax.dynamic_slice_in_dim(beta_sum, head_start, heads_here, 1) * row_scale
    alpha_heads = lax.dynamic_slice_in_dim(alpha_sum, head_start, heads_here, 1) * row_scale
    rate_here = lax.dynamic_slice_in_dim(decay_rate, head_start, heads_here, 0)
    bias_here = lax.dynamic_slice_in_dim(decay_bias, head_start, heads_here, 0)
    beta = jnp.where(
        live_own, jax.nn.sigmoid(beta_heads).reshape(seq_count, span_len, heads_here), 0.0
    )
    log_decay = -rate_here * jax.nn.softplus(alpha_heads + bias_here)
    log_decay = jnp.where(live_own, log_decay.reshape(seq_count, span_len, heads_here), 0.0)
    split_shape = (seq_count, span_len, heads_here, head_size)
    queries = unit_rows((query_sum * row_scale).reshape(split_shape)) * HEAD_DIM ** (-0.5)
    unit_keys = unit_rows((key_sum * row_scale).reshape(split_shape))
    values_split = (value_sum * row_scale).reshape(split_shape)
    carried = state.reshape(seq_count, head_size, heads_here, head_size)
    attended, updated = delta_block(queries, unit_keys, values_split, beta, log_decay, carried)
    head_out = (
        attended
        * lax.rsqrt(jnp.mean(attended * attended, axis=-1, keepdims=True) + EPSILON)
        * out_gain
    )
    head_out = head_out.astype(jnp.bfloat16).reshape(local_rows, heads_here * head_size)
    pack_rows = min((batch_all * 7 // 4 + kv_count - 1) // kv_count * kv_count, row_count)
    live_flat = live_all.reshape(row_count).astype(jnp.int32)
    slot_index = jnp.cumsum(live_flat) - 1
    picker = (
        (slot_index[None, :] == jnp.arange(pack_rows, dtype=jnp.int32)[:, None])
        & (live_flat[None, :] > 0)
    ).astype(jnp.bfloat16)
    heads_every = gather_directly(head_out, "kv", 0)
    packed_heads = jnp.dot(picker, heads_every, preferred_element_type=jnp.float32).astype(
        jnp.bfloat16
    )
    attn_part = jnp.dot(packed_heads, w_out, preferred_element_type=jnp.float32)
    base_rows = jnp.dot(picker, flat_rows, preferred_element_type=jnp.float32)
    attn_own = summed_on_arrival(attn_part.astype(jnp.bfloat16), "tp", 1)
    middle = (base_rows + attn_own).astype(jnp.bfloat16)
    middle_rows = gather_directly(middle, "tp", 1).astype(jnp.float32)
    squares_mid = jnp.sum(middle_rows * middle_rows, axis=1)
    normed_mid = (middle_rows * mix_gain).astype(jnp.bfloat16)
    gate_part = jnp.dot(normed_mid, w_gate, preferred_element_type=jnp.float32)
    up_part = jnp.dot(normed_mid, w_up, preferred_element_type=jnp.float32)
    gate_share, up_share, squares_share = sent_together(
        (
            gate_part.astype(jnp.bfloat16),
            up_part.astype(jnp.bfloat16),
            squares_mid.astype(jnp.bfloat16),
        ),
        "kv",
        0,
        1,
    )
    share_scale = lax.rsqrt(squares_share / D + EPSILON)[:, None]
    hidden_share = (jax.nn.silu(gate_share * share_scale) * (up_share * share_scale)).astype(
        jnp.bfloat16
    )
    down_part = jnp.dot(
        gather_directly(hidden_share, "kv", 0), w_down, preferred_element_type=jnp.float32
    )
    down_own = summed_on_arrival(down_part.astype(jnp.bfloat16), "tp", 1)
    result_rows = middle.astype(jnp.float32) + down_own
    result_rows = jnp.dot(
        picker.astype(jnp.float32).T,
        result_rows,
        precision=lax.Precision.HIGHEST,
        preferred_element_type=jnp.float32,
    )
    mixed = (
        jnp.where(live_all, result_rows, 0.0)
        .astype(jnp.bfloat16)
        .reshape(batch_all, span_len, own_cols)
    )
    return (mixed, updated.reshape(seq_count, head_size, heads_here * head_size))


def solution(mesh):
    return jax.shard_map(
        body,
        mesh=mesh,
        in_specs=(
            P(None, None, ("kv", "tp")),
            P(),
            P("kv", None, "tp"),
            P("kv"),
            P("kv", "tp"),
            P("kv", "tp"),
            P("kv", "tp"),
            P(),
            P(),
            P(),
            P(),
            P(),
            P("tp", "kv"),
            P("kv"),
            P("kv", "tp"),
            P("kv", "tp"),
            P("tp", "kv"),
        ),
        out_specs=(P(None, None, ("kv", "tp")), P("kv", None, "tp")),
        check_vma=False,
    )
```

profile of v0, /device:TPU:1, one launch (start us, length us, event | category | flops | bytes accessed | tf_op | source)
XLA Modules:
  0.0 175.0 jit_solution(14326076393199106244)
XLA Ops:
  0.6 0.9 copy.115
  1.6 0.7 broadcast_in_dim.56
  2.4 16.7 %all-to-all-start = ((bf16[32,512,8]{1,2,0:T(8,128)(2,1)}), bf16[32,512,8]{1,2,0:T(8,128)(2,1)S(1)}, u32[]{:S(2)}, u32[]{:S(2)}) async-start(bf16[32,512,8]{1,2,0:T(8,128)(2,1)} %broadcast_in_dim.56), calls=%async_computation | async-start | bytes 524288 | tf_op jit(solution)/shard_map/all_to_all | solution.py:23
  19.1 0.6 copy-done.13
  19.8 0.6 dynamic_slice.24
  21.0 0.6 dynamic_slice.26
  21.6 0.7 copy-done.10
  22.8 0.3 reduce-window.9
  23.5 17.8 %all-to-all-done = bf16[32,512,8]{1,2,0:T(8,128)(2,1)S(1)} async-done(((bf16[32,512,8]{1,2,0:T(8,128)(2,1)}), bf16[32,512,8]{1,2,0:T(8,128)(2,1)S(1)}, u32[]{:S(2)}, u32[]{:S(2)}) %all-to-all-start) | async-done | bytes 262176 | tf_op jit(solution)/shard_map/all_to_all | solution.py:23
  41.7 0.9 convolution_convert_fusion.8
  42.9 0.3 convert_element_type.188
  43.2 0.6 copy-done.5
  43.7 0.3 convolution_convert_fusion.4
  44.1 0.5 copy-done.6
  44.6 0.3 convolution_convert_fusion.3
  44.9 0.5 copy-done.7
  45.4 0.3 convolution_convert_fusion.2
  45.8 1.1 concatenate.27
  46.8 6.8 %all-to-all-start.1 = ((bf16[16,32,449]{2,1,0:T(8,128)(2,1)}), bf16[16,32,449]{2,1,0:T(8,128)(2,1)S(1)}, u32[]{:S(2)}, u32[]{:S(2)}) async-start(bf16[16,32,449]{2,1,0:T(8,128)(2,1)} %concatenate.27), calls=%async_computation.1 | async-start | bytes 1048576 | tf_op jit(solution)/shard_map/all_to_all | solution.py:39
  53.7 10.4 %all-to-all-done.1 = bf16[16,32,449]{2,1,0:T(8,128)(2,1)S(1)} async-done(((bf16[16,32,449]{2,1,0:T(8,128)(2,1)}), bf16[16,32,449]{2,1,0:T(8,128)(2,1)S(1)}, u32[]{:S(2)}, u32[]{:S(2)}) %all-to-all-start.1) | async-done | bytes 459808 | tf_op jit(solution)/shard_map/all_to_all | solution.py:39
  64.2 0.9 fusion.41
  66.0 0.3 fusion.47
  66.5 0.3 fusion.34
  67.7 0.3 convolution_bitcast_fusion.1
  68.0 0.5 convolution_bitcast_fusion.2
  68.5 0.6 convolution_bitcast_fusion.3
  69.1 0.3 fusion.3
  69.4 0.3 multiply_reduce_fusion
  69.7 0.7 copy-done.11
  70.4 0.7 broadcast_in_dim.66
  71.1 3.6 %all-to-all-start.2 = ((bf16[16,32,128]{2,1,0:T(8,128)(2,1)}), bf16[16,32,128]{2,1,0:T(8,128)(2,1)S(1)}, u32[]{:S(2)}, u32[]{:S(2)}) async-start(bf16[16,32,128]{2,1,0:T(8,128)(2,1)} %broadcast_in_dim.66), calls=%async_computation.2 | async-start | bytes 262144 | tf_op jit(solution)/shard_map/all_to_all | solution.py:23
  74.7 6.8 %all-to-all-done.2 = bf16[16,32,128]{2,1,0:T(8,128)(2,1)S(1)} async-done(((bf16[16,32,128]{2,1,0:T(8,128)(2,1)}), bf16[16,32,128]{2,1,0:T(8,128)(2,1)S(1)}, u32[]{:S(2)}, u32[]{:S(2)}) %all-to-all-start.2) | async-done | bytes 131104 | tf_op jit(solution)/shard_map/all_to_all | solution.py:23
  81.5 0.4 convolution_convert_fusion.5
  82.0 22.0 %all_to_all.40 = bf16[32,224,8]{1,2,0:T(8,128)(2,1)S(1)} all-to-all(bf16[32,224,8]{1,2,0:T(8,128)(2,1)S(1)} %bitcast.144), channel_id=1, replica_groups=mesh['kv'=16,'tp'=32] {'tp'}, dimensions={0} | all-to-all | bytes 229376 | tf_op jit(solution)/shard_map/all_to_all | solution.py:39
  104.4 20.3 %all_to_all.41 = bf16[32,224,8]{1,2,0:T(8,128)(2,1)S(1)} all-to-all(bf16[32,224,8]{1,2,0:T(8,128)(2,1)S(1)} %broadcast_in_dim.67), channel_id=1, replica_groups=mesh['kv'=16,'tp'=32] {'tp'}, dimensions={0} | all-to-all | bytes 229376 | tf_op jit(solution)/shard_map/all_to_all | solution.py:23
  124.6 0.3 convolution_convert_fusion.1
  125.1 0.8 copy-done.4
  125.9 0.3 convolution_convert_fusion
  126.8 11.2 %all_to_all.42 = bf16[16,14,689]{2,1,0:T(8,128)(2,1)S(1)} all-to-all(bf16[16,14,689]{2,1,0:T(8,128)(2,1)S(1)} %pad_maximum_fusion), channel_id=1, replica_groups=mesh['kv'=16,'tp'=32] {'kv'}, dimensions={0} | all-to-all | bytes 617344 | tf_op jit(solution)/shard_map/all_to_all | solution.py:39
  138.4 9.8 %all_to_all.43 = bf16[16,14,344]{2,1,0:T(8,128)(2,1)S(1)} all-to-all(bf16[16,14,344]{2,1,0:T(8,128)(2,1)S(1)} %broadcast_in_dim.68), channel_id=1, replica_groups=mesh['kv'=16,'tp'=32] {'kv'}, dimensions={0} | all-to-all | bytes 308224 | tf_op jit(solution)/shard_map/all_to_all | solution.py:23
  148.3 0.8 copy-done.2
  149.3 0.7 copy.133
  150.1 7.6 %all-to-all-start.7 = ((bf16[32,224,8]{1,2,0:T(8,128)(2,1)}), bf16[32,224,8]{1,2,0:T(8,128)(2,1)S(1)}, u32[]{:S(2)}, u32[]{:S(2)}) async-start(bf16[32,224,8]{1,2,0:T(8,128)(2,1)} %bitcast.48), calls=%async_computation.7 | async-start | bytes 262144 | tf_op jit(solution)/shard_map/all_to_all | solution.py:39
  158.0 1.1 fusion.1
  159.0 1.0 copy.138
  160.0 13.8 %all-to-all-done.7 = bf16[32,224,8]{1,2,0:T(8,128)(2,1)S(1)} async-done(((bf16[32,224,8]{1,2,0:T(8,128)(2,1)}), bf16[32,224,8]{1,2,0:T(8,128)(2,1)S(1)}, u32[]{:S(2)}, u32[]{:S(2)}) %all-to-all-start.7) | async-done | bytes 114720 | tf_op jit(solution)/shard_map/all_to_all | solution.py:39
  173.9 0.3 fusion.4
  174.3 0.7 copy.137
  (92 shorter events, 6.0 us)
Async XLA Ops:
  0.6 40.7 %copy-start = (bf16[4096,32]{0,1:T(8,128)(2,1)S(1)}, bf16[4096,32]{0,1:T(8,128)(2,1)}, u32[]{:S(2)}) copy-start(bf16[4096,32]{0,1:T(8,128)(2,1)} %param.24) | copy-start | bytes 786436
  2.4 39.0 %all-to-all-start = ((bf16[32,512,8]{1,2,0:T(8,128)(2,1)}), bf16[32,512,8]{1,2,0:T(8,128)(2,1)S(1)}, u32[]{:S(2)}, u32[]{:S(2)}) async-start(bf16[32,512,8]{1,2,0:T(8,128)(2,1)} %broadcast_in_dim.56), calls=%async_computation | async-start | bytes 524288 | tf_op jit(solution)/shard_map/all_to_all | solution.py:23
  19.1 0.7 copy-start.13
  20.4 0.7 copy-start.14
  21.6 0.7 copy-start.10
  23.4 18.0 %copy-start.8 = (f32[256]{0:T(256)S(1)}, f32[256]{0:T(256)}, u32[]{:S(2)}) copy-start(f32[256]{0:T(256)} %param.20) | copy-start | bytes 3076
  42.9 0.8 copy-start.5
  43.7 0.8 copy-start.6
  44.6 0.8 copy-start.7
  46.8 17.2 %all-to-all-start.1 = ((bf16[16,32,449]{2,1,0:T(8,128)(2,1)}), bf16[16,32,449]{2,1,0:T(8,128)(2,1)S(1)}, u32[]{:S(2)}, u32[]{:S(2)}) async-start(bf16[16,32,449]{2,1,0:T(8,128)(2,1)} %concatenate.27), calls=%async_computation.1 | async-start | bytes 1048576 | tf_op jit(solution)/shard_map/all_to_all | solution.py:39
  64.1 3.9 %copy-start.1 = (f32[8,128,128]{2,1,0:T(8,128)S(1)}, f32[8,128,128]{2,1,0:T(8,128)}, u32[]{:S(2)}) copy-start(f32[8,128,128]{2,1,0:T(8,128)} %param.19) | copy-start | bytes 1572868
  69.7 0.7 copy-start.11
  71.1 10.5 %copy-start.12 = (bf16[128,256]{1,0:T(8,128)(2,1)S(1)}, bf16[128,256]{1,0:T(8,128)(2,1)}, u32[]{:S(2)}) copy-start(bf16[128,256]{1,0:T(8,128)(2,1)} %param.29) | copy-start | bytes 196612
  71.1 10.5 %all-to-all-start.2 = ((bf16[16,32,128]{2,1,0:T(8,128)(2,1)}), bf16[16,32,128]{2,1,0:T(8,128)(2,1)S(1)}, u32[]{:S(2)}, u32[]{:S(2)}) async-start(bf16[16,32,128]{2,1,0:T(8,128)(2,1)} %broadcast_in_dim.66), calls=%async_computation.2 | async-start | bytes 262144 | tf_op jit(solution)/shard_map/all_to_all | solution.py:23
  104.3 20.3 %copy-start.3 = (bf16[256,344]{0,1:T(8,128)(2,1)S(1)}, bf16[256,344]{0,1:T(8,128)(2,1)}, u32[]{:S(2)}) copy-start(bf16[256,344]{0,1:T(8,128)(2,1)} %param.31) | copy-start | bytes 528388
  104.3 20.3 %copy-start.9 = (f32[256]{0:T(256)S(1)}, f32[256]{0:T(256)}, u32[]{:S(2)}) copy-start(f32[256]{0:T(256)} %param.30) | copy-start | bytes 3076
  125.0 0.9 copy-start.4
  148.2 0.9 copy-start.2
  150.1 23.8 %all-to-all-start.7 = ((bf16[32,224,8]{1,2,0:T(8,128)(2,1)}), bf16[32,224,8]{1,2,0:T(8,128)(2,1)S(1)}, u32[]{:S(2)}, u32[]{:S(2)}) async-start(bf16[32,224,8]{1,2,0:T(8,128)(2,1)} %bitcast.48), calls=%async_computation.7 | async-start | bytes 262144 | tf_op jit(solution)/shard_map/all_to_all | solution.py:39
where the time goes:
time: 176 us; the launch traced here: 175 us
  blocking collectives  63.3 us (36%)
  waiting for transfers between devices  48.8 us (28%)
  starting transfers between devices  34.7 us (20%)
  local copies, waits for them, and re-layouts  16.1 us (9%)
  matrix products  7.45 us (4%)
  other arithmetic  2.96 us (2%)
    all_to_all x2, blocking collectives, summed_on_arrival(): lax.all_to_all(tiles, axis, split_axis=0, concat_axis=0, tiled=True)  33.2 us
    all_to_all x2, blocking collectives, copy_for_each(): lax.all_to_all(jnp.broadcast_to(shard[None], (length, *shard.shape)), axi...  30.1 us
    all_to_all x2, waiting for transfers between devices, copy_for_each(): lax.all_to_all(jnp.broadcast_to(shard[None], (length, *shard.shape)), axi...  24.6 us
    all_to_all x2, waiting for transfers between devices, summed_on_arrival(): lax.all_to_all(tiles, axis, split_axis=0, concat_axis=0, tiled=True)  24.2 us
    all_to_all x2, starting transfers between devices, copy_for_each(): lax.all_to_all(jnp.broadcast_to(shard[None], (length, *shard.shape)), axi...  20.4 us
    all_to_all x2, starting transfers between devices, summed_on_arrival(): lax.all_to_all(tiles, axis, split_axis=0, concat_axis=0, tiled=True)  14.3 us
    unnamed x34, local copies, waits for them, and re-layouts  8.02 us
  transfers between devices with their start and end apart: 4, of which 4 were waited for; matrix products, arithmetic and copies ran while one was open for 3% of the time, Pallas kernels for 0%

commit v1 on v0

v1 whole, which is shorter than its diff:
```python
import jax
import jax.numpy as jnp
from jax import lax
from jax.sharding import Mesh, PartitionSpec as P

D = 4096
HEAD_DIM = 128
EPSILON = 1e-06
F32 = jnp.float32
BF16 = jnp.bfloat16


def swap(tiles, axis):
    return lax.all_to_all(tiles, axis, split_axis=0, concat_axis=0, tiled=True)


def spread(shard, axis):
    return swap(jnp.broadcast_to(shard[None], (lax.axis_size(axis), *shard.shape)), axis)


def gather_features(shard):
    every = lax.all_gather(spread(shard, "z"), "c", axis=0, tiled=False)
    own, rows = shard.shape
    return jnp.swapaxes(every, 0, 1).reshape(-1, rows)


def sum_to_owner(part):
    feats, rows = part.shape
    z_count, c_count = lax.axis_size("z"), lax.axis_size("c")
    pair = lax.all_gather(part.astype(BF16), "c", axis=0, tiled=False)
    pair = pair.reshape(c_count, z_count, c_count, -1, rows)
    mine = lax.dynamic_index_in_dim(pair, lax.axis_index("c"), 2, keepdims=False)
    both = mine.astype(F32).sum(axis=0).astype(BF16)
    return swap(both, "z").astype(F32).sum(axis=0)


def unit_rows(vectors):
    return vectors * lax.rsqrt(jnp.sum(vectors * vectors, axis=-1, keepdims=True) + EPSILON)


def delta_block(queries, unit_keys, values_split, beta, log_decay, carried):
    highest = lax.Precision.HIGHEST
    seq_count, span_len, heads_here = beta.shape
    cumulative = jnp.cumsum(log_decay, axis=1)
    position = jnp.arange(span_len)
    inclusive = (position[:, None] >= position[None, :])[None, :, :, None]
    strict = (position[:, None] > position[None, :])[None, :, :, None]
    gap_matrix = cumulative[:, :, None, :] - cumulative[:, None, :, :]
    decay_matrix = jnp.where(inclusive, jnp.exp(jnp.where(inclusive, gap_matrix, 0.0)), 0.0)
    key_dots = jnp.einsum("nihd,njhd->nijh", unit_keys, unit_keys, precision=highest)
    query_dots = jnp.einsum("nihd,njhd->nijh", queries, unit_keys, precision=highest) * decay_matrix
    lower_part = jnp.where(strict, key_dots * decay_matrix * beta[:, :, None, :], 0.0)
    identity = jnp.eye(span_len, dtype=jnp.float32)
    inverse_rows = []
    for step in range(span_len):
        row_now = jnp.broadcast_to(identity[step][None, :, None], (seq_count, span_len, heads_here))
        for prior in range(step):
            row_now = row_now - lower_part[:, step, prior, :][:, None, :] * inverse_rows[prior]
        inverse_rows.append(row_now)
    inverse = jnp.stack(inverse_rows, axis=1)
    beta_value = beta[..., None] * values_split
    beta_key = (beta * jnp.exp(cumulative))[..., None] * unit_keys
    base_update = jnp.einsum("nich,nche->nihe", inverse, beta_value, precision=highest)
    key_weights = jnp.einsum("nich,nchd->nihd", inverse, beta_key, precision=highest)
    corrected = base_update - jnp.einsum("nihd,ndhe->nihe", key_weights, carried, precision=highest)
    decayed_queries = queries * jnp.exp(cumulative)[..., None]
    attended = jnp.einsum("nihd,ndhe->nihe", decayed_queries, carried, precision=highest)
    attended = attended + jnp.einsum("nijh,njhe->nihe", query_dots, corrected, precision=highest)
    block_total = cumulative[:, -1, :]
    key_tail = unit_keys * jnp.exp(block_total[:, None, :] - cumulative)[..., None]
    updated = carried * jnp.exp(block_total)[:, None, :, None]
    updated = updated + jnp.einsum("nihd,nihe->ndhe", key_tail, corrected, precision=highest)
    return (attended, updated)


def rows_dot(features_rows, weights):
    return lax.dot_general(
        features_rows, weights, (((0,), (0,)), ((), ())), preferred_element_type=F32
    )


def body(
    tokens,
    lengths,
    state,
    attn_gain,
    w_query,
    w_key,
    w_value,
    w_beta,
    w_alpha,
    decay_rate,
    decay_bias,
    out_gain,
    w_out,
    mix_gain,
    w_gate,
    w_up,
    w_down,
):
    kv_index = lax.axis_index("kv")
    kv_count = lax.axis_size("kv")
    head = lax.axis_index("z") * lax.axis_size("c") + lax.axis_index("c")
    batch_all, span_len, own_cols = tokens.shape
    row_count = batch_all * span_len
    seq_count, head_size, _ = state.shape
    local_rows = seq_count * span_len
    block_width = attn_gain.shape[0]
    slots = 256

    flat_t = tokens.reshape(row_count, own_cols).T
    gathered = gather_features(flat_t).astype(F32)
    squares_in = jnp.sum(gathered * gathered, axis=0)
    normed_in = (gathered * attn_gain[:, None]).astype(BF16)
    beta_rows = lax.dynamic_slice_in_dim(w_beta, kv_index * block_width, block_width, 0)
    alpha_rows = lax.dynamic_slice_in_dim(w_alpha, kv_index * block_width, block_width, 0)
    beta_col = lax.dynamic_slice_in_dim(beta_rows, head, 1, 1)
    alpha_col = lax.dynamic_slice_in_dim(alpha_rows, head, 1, 1)
    small = rows_dot(normed_in, jnp.concatenate([beta_col, alpha_col], axis=1)).astype(BF16)
    sent = jnp.concatenate(
        [
            rows_dot(normed_in, w_query).astype(BF16),
            rows_dot(normed_in, w_key).astype(BF16),
            rows_dot(normed_in, w_value).astype(BF16),
            small,
            squares_in.astype(BF16)[:, None],
        ],
        axis=1,
    ).reshape(kv_count, local_rows, -1)
    sums = swap(sent, "kv").astype(F32).sum(axis=0)

    row_scale = lax.rsqrt(sums[:, 386:387] / D + EPSILON)
    lengths_own = lax.dynamic_slice_in_dim(lengths, kv_index * seq_count, seq_count, 0)
    live_own = (jnp.arange(span_len, dtype=jnp.int32)[None, :] < lengths_own[:, None])[..., None]
    rate_here = lax.dynamic_slice_in_dim(decay_rate, head, 1, 0)
    bias_here = lax.dynamic_slice_in_dim(decay_bias, head, 1, 0)
    beta = jnp.where(
        live_own,
        jax.nn.sigmoid(sums[:, 384:385] * row_scale).reshape(seq_count, span_len, 1),
        0.0,
    )
    log_decay = -rate_here * jax.nn.softplus(sums[:, 385:386] * row_scale + bias_here)
    log_decay = jnp.where(live_own, log_decay.reshape(seq_count, span_len, 1), 0.0)
    split_shape = (seq_count, span_len, 1, head_size)
    queries = unit_rows((sums[:, 0:128] * row_scale).reshape(split_shape)) * HEAD_DIM ** (-0.5)
    unit_keys = unit_rows((sums[:, 128:256] * row_scale).reshape(split_shape))
    values_split = (sums[:, 256:384] * row_scale).reshape(split_shape)
    carried = state.reshape(seq_count, head_size, 1, head_size)
    attended, updated = delta_block(queries, unit_keys, values_split, beta, log_decay, carried)
    head_out = (
        attended
        * lax.rsqrt(jnp.mean(attended * attended, axis=-1, keepdims=True) + EPSILON)
        * out_gain
    )
    head_out = head_out.astype(BF16).reshape(local_rows, head_size)

    live_all = (jnp.arange(span_len, dtype=jnp.int32)[None, :] < lengths[:, None]).reshape(
        row_count
    )
    slot_index = jnp.cumsum(live_all.astype(jnp.int32)) - 1
    picker = (
        (slot_index[None, :] == jnp.arange(slots, dtype=jnp.int32)[:, None])
        & live_all[None, :]
    ).astype(BF16)
    base_rows = lax.dot_general(
        flat_t, picker, (((1,), (1,)), ((), ())), preferred_element_type=F32
    )
    heads_every = spread(head_out, "kv").reshape(row_count, head_size)
    packed_heads = jnp.dot(picker, heads_every, preferred_element_type=F32).astype(BF16)
    attn_part = lax.dot_general(
        w_out, packed_heads, (((0,), (1,)), ((), ())), preferred_element_type=F32
    )
    middle = (base_rows + sum_to_owner(attn_part)).astype(BF16)
    middle_rows = gather_features(middle).astype(F32)
    squares_mid = jnp.sum(middle_rows * middle_rows, axis=0)
    normed_mid = (middle_rows * mix_gain[:, None]).astype(BF16)
    share = jnp.concatenate(
        [
            rows_dot(normed_mid, w_gate).astype(BF16),
            rows_dot(normed_mid, w_up).astype(BF16),
            squares_mid.astype(BF16)[:, None],
        ],
        axis=1,
    ).reshape(kv_count, slots // kv_count, -1)
    share = swap(share, "kv").astype(F32).sum(axis=0)
    units = w_gate.shape[1]
    share_scale = lax.rsqrt(share[:, 2 * units :] / D + EPSILON)
    hidden = (
        jax.nn.silu(share[:, :units] * share_scale)
        * (share[:, units : 2 * units] * share_scale)
    ).astype(BF16)
    hidden_every = spread(hidden, "kv").reshape(slots, units)
    down_part = lax.dot_general(
        w_down, hidden_every, (((0,), (1,)), ((), ())), preferred_element_type=F32
    )
    result = (middle.astype(F32) + sum_to_owner(down_part)).astype(BF16)
    mixed = jnp.dot(result, picker, preferred_element_type=F32).astype(BF16)
    mixed = mixed.T.reshape(batch_all, span_len, own_cols)
    return (mixed, updated.reshape(seq_count, head_size, head_size))


def solution(mesh):
    split = Mesh(mesh.devices.reshape(mesh.shape["kv"], -1, 2), ("kv", "z", "c"))
    tp = ("z", "c")
    return jax.shard_map(
        body,
        mesh=split,
        in_specs=(
            P(None, None, ("kv", "z", "c")),
            P(),
            P("kv", None, tp),
            P("kv"),
            P("kv", tp),
            P("kv", tp),
            P("kv", tp),
            P(),
            P(),
            P(),
            P(),
            P(),
            P(tp, "kv"),
            P("kv"),
            P("kv", tp),
            P("kv", tp),
            P(tp, "kv"),
        ),
        out_specs=(P(None, None, ("kv", "z", "c")), P("kv", None, tp)),
        check_vma=False,
    )
```

time: 176 us -> 163 us (0.926)
  waiting for transfers between devices: 48.8 us -> 33.3 us
  blocking collectives: 63.3 us -> 70.8 us
  starting transfers between devices: 34.7 us -> 29.6 us
    all_gather x0 -> x4, blocking collectives: none -> 17.9 us  [the longest x2 9.18 us: gather_features(): every = lax.all_gather(spread(shard, 'z'), 'c', axis=0, tiled=False)]
    all_to_all x4, waiting for transfers between devices: 48.8 us -> 33.3 us  [swap(): return lax.all_to_all(tiles, axis, split_axis=0, concat_axis=0, tiled=True)]
    all_to_all x4, blocking collectives: 63.3 us -> 52.8 us  [swap(): return lax.all_to_all(tiles, axis, split_axis=0, concat_axis=0, tiled=True)]
    all_to_all x4, starting transfers between devices: 34.7 us -> 29.6 us  [swap(): return lax.all_to_all(tiles, axis, split_axis=0, concat_axis=0, tiled=True)]
    dot_general x11 -> x10, matrix products: 3.96 us -> 2.36 us  [the longest x6 1.33 us: rows_dot(): lax.dot_general(features_rows, weights, (((0,), (0,)), ((), ())), preferr...]
    unnamed x34 -> x32, local copies, waits for them, and re-layouts: 8.02 us -> 7.94 us
  transfers between devices with their start and end apart: 4 -> 4, of which waited for: 4 -> 4; matrix products, arithmetic and copies ran while one was open for 3% -> 4% of each run, Pallas kernels for 0% -> 0%
where the time goes in v1:
time: 163 us; the launch traced here: 162 us
  blocking collectives  70.8 us (43%)
  waiting for transfers between devices  33.3 us (20%)
  starting transfers between devices  29.6 us (18%)
  local copies, waits for them, and re-layouts  17 us (10%)
  matrix products  5.84 us (4%)
  other arithmetic  3.8 us (2%)
  between operations  1.8 us (1%)
    all_to_all x4, blocking collectives, swap(): return lax.all_to_all(tiles, axis, split_axis=0, concat_axis=0, tiled=True)  52.8 us
    all_to_all x4, waiting for transfers between devices, swap(): return lax.all_to_all(tiles, axis, split_axis=0, concat_axis=0, tiled=True)  33.3 us
    all_to_all x4, starting transfers between devices, swap(): return lax.all_to_all(tiles, axis, split_axis=0, concat_axis=0, tiled=True)  29.6 us
    all_gather x2, blocking collectives, gather_features(): every = lax.all_gather(spread(shard, 'z'), 'c', axis=0, tiled=False)  9.18 us
    all_gather x2, blocking collectives, sum_to_owner(): pair = lax.all_gather(part.astype(BF16), 'c', axis=0, tiled=False)  8.75 us
    unnamed x32, local copies, waits for them, and re-layouts  7.94 us
  transfers between devices with their start and end apart: 4, of which 4 were waited for; matrix products, arithmetic and copies ran while one was open for 4% of the time, Pallas kernels for 0%

profile of v1, /device:TPU:1, one launch (start us, length us, event | category | flops | bytes accessed | tf_op | source)
XLA Modules:
  0.0 162.1 jit_solution(17874365881180876897)
XLA Ops:
  0.6 0.9 copy.147
  1.6 0.7 broadcast_in_dim.47
  2.3 15.7 %all-to-all-start = ((bf16[16,8,512]{2,1,0:T(8,128)(2,1)}), bf16[16,8,512]{2,1,0:T(8,128)(2,1)S(1)}, u32[]{:S(2)}, u32[]{:S(2)}) async-start(bf16[16,8,512]{2,1,0:T(8,128)(2,1)} %broadcast_in_dim.47), calls=%async_computation | async-start | bytes 262144 | tf_op jit(solution)/shard_map/all_to_all | solution.py:14
  18.1 0.8 dynamic_slice.24
  18.8 0.8 dynamic_slice.25
  20.1 9.9 %all-to-all-done = bf16[16,8,512]{2,1,0:T(8,128)(2,1)S(1)} async-done(((bf16[16,8,512]{2,1,0:T(8,128)(2,1)}), bf16[16,8,512]{2,1,0:T(8,128)(2,1)S(1)}, u32[]{:S(2)}, u32[]{:S(2)}) %all-to-all-start) | async-done | bytes 131104 | tf_op jit(solution)/shard_map/all_to_all | solution.py:14
  30.0 5.4 %all-gather = bf16[32,8,512]{2,1,0:T(8,128)(2,1)S(1)} all-gather(bf16[16,8,512]{2,1,0:T(8,128)(2,1)S(1)} %all-to-all-done), channel_id=2, replica_groups=mesh['kv'=16,'z'=16,'c'=2] {'c'}, dimensions={0}, use_global_device_ids=true | all-gather | bytes 393216 | tf_op jit(solution)/shard_map/all_gather | solution.py:22
  35.5 0.3 convert_element_type.197
  35.9 0.6 copy-done.8
  36.9 0.7 copy-done.4
  37.6 0.3 convolution_convert_fusion.4
  37.9 0.6 copy-done.5
  38.4 0.3 convolution_convert_fusion.5
  38.7 0.6 copy-done.6
  39.5 1.0 concatenate.28
  40.5 6.8 %all-to-all-start.1 = ((bf16[16,32,387]{2,1,0:T(8,128)(2,1)}), bf16[16,32,387]{2,1,0:T(8,128)(2,1)S(1)}, u32[]{:S(2)}, u32[]{:S(2)}) async-start(bf16[16,32,387]{2,1,0:T(8,128)(2,1)} %concatenate.28), calls=%async_computation.1 | async-start | bytes 1048576 | tf_op jit(solution)/shard_map/all_to_all | solution.py:14
  47.4 0.6 copy-done.12
  48.0 0.6 dynamic_slice.28
  48.6 0.7 dynamic_slice.27
  50.1 0.3 reduce-window.9
  50.7 7.4 %all-to-all-done.1 = bf16[16,32,387]{2,1,0:T(8,128)(2,1)S(1)} async-done(((bf16[16,32,387]{2,1,0:T(8,128)(2,1)}), bf16[16,32,387]{2,1,0:T(8,128)(2,1)S(1)}, u32[]{:S(2)}, u32[]{:S(2)}) %all-to-all-start.1) | async-done | bytes 396320 | tf_op jit(solution)/shard_map/all_to_all | solution.py:14
  58.1 0.9 fusion.42
  60.4 0.3 fusion.48
  61.6 0.6 convolution_bitcast_fusion.3
  62.2 0.3 convolution_bitcast_fusion.1
  62.4 0.5 convolution_bitcast_fusion.2
  63.0 0.3 fusion.5
  63.2 0.3 multiply_reduce_fusion
  63.5 0.7 copy-done.10
  64.3 0.7 broadcast_in_dim.57
  64.9 3.6 %all-to-all-start.2 = ((bf16[16,32,128]{2,1,0:T(8,128)(2,1)}), bf16[16,32,128]{2,1,0:T(8,128)(2,1)S(1)}, u32[]{:S(2)}, u32[]{:S(2)}) async-start(bf16[16,32,128]{2,1,0:T(8,128)(2,1)} %broadcast_in_dim.57), calls=%async_computation.2 | async-start | bytes 262144 | tf_op jit(solution)/shard_map/all_to_all | solution.py:14
  68.7 6.7 %all-to-all-done.2 = bf16[16,32,128]{2,1,0:T(8,128)(2,1)S(1)} async-done(((bf16[16,32,128]{2,1,0:T(8,128)(2,1)}), bf16[16,32,128]{2,1,0:T(8,128)(2,1)S(1)}, u32[]{:S(2)}, u32[]{:S(2)}) %all-to-all-start.2) | async-done | bytes 131104 | tf_op jit(solution)/shard_map/all_to_all | solution.py:14
  75.4 0.4 fusion.3
  75.8 4.5 %all-gather.1 = bf16[512,256]{0,1:T(8,128)(2,1)S(1)} all-gather(bf16[256,256]{0,1:T(8,128)(2,1)S(1)} %fusion.3), channel_id=3, replica_groups=mesh['kv'=16,'z'=16,'c'=2] {'c'}, dimensions={0}, use_global_device_ids=true | all-gather | bytes 393216 | tf_op jit(solution)/shard_map/all_gather | solution.py:30
  80.5 15.0 %all_to_all.40 = bf16[16,8,256]{2,1,0:T(8,128)(2,1)S(1)} all-to-all(bf16[16,8,256]{2,1,0:T(8,128)(2,1)S(1)} %dynamic-slice_reduce_fusion.1), channel_id=1, replica_groups=mesh['kv'=16,'z'=16,'c'=2] {'z'}, dimensions={0} | all-to-all | bytes 131072 | tf_op jit(solution)/shard_map/all_to_all | solution.py:14
  95.7 15.3 %all_to_all.41 = bf16[16,8,256]{2,1,0:T(8,128)(2,1)S(1)} all-to-all(bf16[16,8,256]{2,1,0:T(8,128)(2,1)S(1)} %broadcast_in_dim.58), channel_id=1, replica_groups=mesh['kv'=16,'z'=16,'c'=2] {'z'}, dimensions={0} | all-to-all | bytes 131072 | tf_op jit(solution)/shard_map/all_to_all | solution.py:14
  110.9 3.8 %all-gather.2 = bf16[32,8,256]{2,1,0:T(8,128)(2,1)S(1)} all-gather(bf16[16,8,256]{2,1,0:T(8,128)(2,1)S(1)} %all_to_all.41), channel_id=4, replica_groups=mesh['kv'=16,'z'=16,'c'=2] {'c'}, dimensions={0}, use_global_device_ids=true | all-gather | bytes 196608 | tf_op jit(solution)/shard_map/all_gather | solution.py:22
  115.1 0.6 copy-done.9
  116.3 0.7 copy-done.2
  117.6 12.3 %all_to_all.42 = bf16[16,16,689]{2,1,0:T(8,128)(2,1)S(1)} all-to-all(bf16[16,16,689]{2,1,0:T(8,128)(2,1)S(1)} %pad_maximum_fusion), channel_id=1, replica_groups=mesh['kv'=16,'z'=16,'c'=2] {'kv'}, dimensions={0} | all-to-all | bytes 705536 | tf_op jit(solution)/shard_map/all_to_all | solution.py:14
  130.3 10.3 %all_to_all.43 = bf16[16,16,344]{2,1,0:T(8,128)(2,1)S(1)} all-to-all(bf16[16,16,344]{2,1,0:T(8,128)(2,1)S(1)} %broadcast_in_dim.59), channel_id=1, replica_groups=mesh['kv'=16,'z'=16,'c'=2] {'kv'}, dimensions={0} | all-to-all | bytes 352256 | tf_op jit(solution)/shard_map/all_to_all | solution.py:14
  140.8 4.2 %all-gather.3 = bf16[512,256]{0,1:T(8,128)(2,1)S(1)} all-gather(bf16[256,256]{0,1:T(8,128)(2,1)S(1)} %fusion.2), channel_id=5, replica_groups=mesh['kv'=16,'z'=16,'c'=2] {'c'}, dimensions={0}, use_global_device_ids=true | all-gather | bytes 393216 | tf_op jit(solution)/shard_map/all_gather | solution.py:30
  145.2 0.6 dynamic-slice_reduce_fusion
  145.8 3.5 %all-to-all-start.7 = ((bf16[16,8,256]{2,1,0:T(8,128)(2,1)}), bf16[16,8,256]{2,1,0:T(8,128)(2,1)S(1)}, u32[]{:S(2)}, u32[]{:S(2)}) async-start(bf16[16,8,256]{2,1,0:T(8,128)(2,1)} %dynamic-slice_reduce_fusion), calls=%async_computation.7 | async-start | bytes 131072 | tf_op jit(solution)/shard_map/all_to_all | solution.py:14
  149.6 1.1 fusion.1
  150.7 1.0 copy.173
  151.7 9.4 %all-to-all-done.7 = bf16[16,8,256]{2,1,0:T(8,128)(2,1)S(1)} async-done(((bf16[16,8,256]{2,1,0:T(8,128)(2,1)}), bf16[16,8,256]{2,1,0:T(8,128)(2,1)S(1)}, u32[]{:S(2)}, u32[]{:S(2)}) %all-to-all-start.7) | async-done | bytes 65568 | tf_op jit(solution)/shard_map/all_to_all | solution.py:14
  161.4 0.7 copy.172
  (99 shorter events, 7.6 us)
Async XLA Ops:
  0.6 115.2 %copy-start = (bf16[256,344]{0,1:T(8,128)(2,1)S(1)}, bf16[256,344]{0,1:T(8,128)(2,1)}, u32[]{:S(2)}) copy-start(bf16[256,344]{0,1:T(8,128)(2,1)} %param.32) | copy-start | bytes 528388
  2.3 27.7 %all-to-all-start = ((bf16[16,8,512]{2,1,0:T(8,128)(2,1)}), bf16[16,8,512]{2,1,0:T(8,128)(2,1)S(1)}, u32[]{:S(2)}, u32[]{:S(2)}) async-start(bf16[16,8,512]{2,1,0:T(8,128)(2,1)} %broadcast_in_dim.47), calls=%async_computation | async-start | bytes 262144 | tf_op jit(solution)/shard_map/all_to_all | solution.py:14
  18.8 0.8 copy-start.7
  35.8 0.7 copy-start.8
  36.7 0.8 copy-start.4
  37.6 0.8 copy-start.5
  38.4 0.8 copy-start.6
  40.5 17.5 %all-to-all-start.1 = ((bf16[16,32,387]{2,1,0:T(8,128)(2,1)}), bf16[16,32,387]{2,1,0:T(8,128)(2,1)S(1)}, u32[]{:S(2)}, u32[]{:S(2)}) async-start(bf16[16,32,387]{2,1,0:T(8,128)(2,1)} %concatenate.28), calls=%async_computation.1 | async-start | bytes 1048576 | tf_op jit(solution)/shard_map/all_to_all | solution.py:14
  47.3 0.7 copy-start.12
  48.0 0.7 copy-start.13
  50.6 11.0 %copy-start.1 = (f32[8,128,128]{2,1,0:T(8,128)S(1)}, f32[8,128,128]{2,1,0:T(8,128)}, u32[]{:S(2)}) copy-start(f32[8,128,128]{2,1,0:T(8,128)} %param.19) | copy-start | bytes 1572868
  63.5 0.7 copy-start.10
  64.9 10.5 %copy-start.11 = (bf16[128,256]{1,0:T(8,128)(2,1)S(1)}, bf16[128,256]{1,0:T(8,128)(2,1)}, u32[]{:S(2)}) copy-start(bf16[128,256]{1,0:T(8,128)(2,1)} %param.29) | copy-start | bytes 196612
  64.9 10.5 %all-to-all-start.2 = ((bf16[16,32,128]{2,1,0:T(8,128)(2,1)}), bf16[16,32,128]{2,1,0:T(8,128)(2,1)S(1)}, u32[]{:S(2)}, u32[]{:S(2)}) async-start(bf16[16,32,128]{2,1,0:T(8,128)(2,1)} %broadcast_in_dim.57), calls=%async_computation.2 | async-start | bytes 262144 | tf_op jit(solution)/shard_map/all_to_all | solution.py:14
  115.1 0.7 copy-start.9
  116.1 0.9 copy-start.2
  130.3 10.3 %copy-start.3 = (bf16[344,256]{1,0:T(8,128)(2,1)S(1)}, bf16[344,256]{1,0:T(8,128)(2,1)}, u32[]{:S(2)}) copy-start(bf16[344,256]{1,0:T(8,128)(2,1)} %param.33) | copy-start | bytes 528388
  145.8 15.2 %all-to-all-start.7 = ((bf16[16,8,256]{2,1,0:T(8,128)(2,1)}), bf16[16,8,256]{2,1,0:T(8,128)(2,1)S(1)}, u32[]{:S(2)}, u32[]{:S(2)}) async-start(bf16[16,8,256]{2,1,0:T(8,128)(2,1)} %dynamic-slice_reduce_fusion), calls=%async_computation.7 | async-start | bytes 131072 | tf_op jit(solution)/shard_map/all_to_all | solution.py:14

commit v2 on v1

v2 whole, which is shorter than its diff:
```python
import jax
import jax.numpy as jnp
from jax import lax
from jax.experimental import pallas as pl
from jax.experimental.pallas import tpu as pltpu
from jax.sharding import Mesh, PartitionSpec as P

D = 4096
HEAD_DIM = 128
EPSILON = 1e-06
F32 = jnp.float32
BF16 = jnp.bfloat16


def swap(tiles, axis):
    return lax.all_to_all(tiles, axis, split_axis=0, concat_axis=0, tiled=True)


def spread(shard, axis):
    return swap(jnp.broadcast_to(shard[None], (lax.axis_size(axis), *shard.shape)), axis)


def gather_features(shard):
    return lax.all_gather(spread(shard, "z"), "c", axis=0, tiled=False)


def sum_to_owner(part):
    feats, rows = part.shape
    z_count, c_count = lax.axis_size("z"), lax.axis_size("c")
    pair = lax.all_gather(part, "c", axis=0, tiled=False)
    pair = pair.reshape(c_count, z_count, c_count, -1, rows)
    mine = lax.dynamic_index_in_dim(pair, lax.axis_index("c"), 2, keepdims=False)
    both = mine.astype(F32).sum(axis=0).astype(BF16)
    return swap(both, "z").astype(F32).sum(axis=0)


def dot(a, b, dims):
    return lax.dot_general(a, b, ((dims[:1], dims[1:]), ((), ())), preferred_element_type=F32)


def split_high_low(x):
    high = x.astype(BF16)
    return high, (x - high.astype(F32)).astype(BF16)


def full(shape_of):
    return [pl.BlockSpec(memory_space=pltpu.VMEM)] * shape_of


def features_of(ref):
    c_count, z_count = ref.shape[:2]
    return jnp.concatenate(
        [ref[c, z].astype(F32) for z in range(z_count) for c in range(c_count)], axis=0
    )


def project_kernel(
    x_ref, gain_ref, wq_ref, wk_ref, wv_ref, wb_ref, wa_ref, out_ref, wb_rows, wa_rows, sems
):
    width = gain_ref.shape[0]
    first = lax.axis_index("kv") * width
    head = lax.axis_index("z") * lax.axis_size("c") + lax.axis_index("c")
    copies = [
        pltpu.make_async_copy(src.at[pl.ds(first, width)], dst, sems.at[k])
        for k, (src, dst) in enumerate(((wb_ref, wb_rows), (wa_ref, wa_rows)))
    ]
    for copy in copies:
        copy.start()
    kv_count, local_rows, _ = out_ref.shape
    x = features_of(x_ref)
    squared = (x * x).astype(BF16)
    normed = (x * gain_ref[...]).astype(BF16)

    def put(block, value):
        out_ref[:, :, block * 128 : (block + 1) * 128] = value.astype(BF16).reshape(
            kv_count, local_rows, 128
        )

    for block, w_ref in enumerate((wq_ref, wk_ref, wv_ref)):
        put(block, dot(normed, w_ref[...], (0, 0)))
    for copy in copies:
        copy.wait()
    heads = wb_rows.shape[1]
    row = lax.broadcasted_iota(jnp.int32, (heads, 128), 0)
    lane = lax.broadcasted_iota(jnp.int32, (heads, 128), 1)
    own = row == head
    small = dot(wb_rows[...], (own & (lane == 0)).astype(BF16), (1, 0))
    small = small + dot(wa_rows[...], (own & (lane == 1)).astype(BF16), (1, 0))
    ones = (lax.broadcasted_iota(jnp.int32, (width, 128), 1) == 2).astype(BF16)
    put(3, dot(normed, small.astype(BF16), (0, 0)) + dot(squared, ones, (0, 0)))


def project(x, gain, wq, wk, wv, wb, wa, kv_count):
    rows = x.shape[-1]
    width, heads = gain.shape[0], wb.shape[1]
    return pl.pallas_call(
        project_kernel,
        out_shape=jax.ShapeDtypeStruct((kv_count, rows // kv_count, 512), BF16),
        in_specs=full(5) + [pl.BlockSpec(memory_space=pl.ANY)] * 2,
        out_specs=pl.BlockSpec(memory_space=pltpu.VMEM),
        scratch_shapes=[
            pltpu.VMEM((width, heads), BF16),
            pltpu.VMEM((width, heads), BF16),
            pltpu.SemaphoreType.DMA((2,)),
        ],
        name="project",
    )(x, gain, wq, wk, wv, wb, wa)


def delta_kernel(
    recv_ref, state_ref, lengths_ref, rate_ref, bias_ref, gain_ref, head_ref, new_ref
):
    seq_count, size, _ = state_ref.shape
    rows = recv_ref.shape[1]
    span = rows // seq_count
    first = lax.axis_index("kv") * seq_count
    head = lax.axis_index("z") * lax.axis_size("c") + lax.axis_index("c")
    sums = recv_ref[0].astype(F32)
    for k in range(1, recv_ref.shape[0]):
        sums = sums + recv_ref[k].astype(F32)

    def lanes(column):
        return jnp.broadcast_to(column, (rows, size))

    row_scale = lanes(lax.rsqrt(sums[:, 386:387] / D + EPSILON))
    row = lax.broadcasted_iota(jnp.int32, (rows, size), 0)
    step = row % span
    seq = row // span
    limit = jnp.zeros((rows, size), jnp.int32)
    for n in range(seq_count):
        limit = jnp.where(seq == n, lengths_ref[first + n], limit)
    live = step < limit
    beta = jnp.where(live, jax.nn.sigmoid(lanes(sums[:, 384:385]) * row_scale), 0.0)
    pre = lanes(sums[:, 385:386]) * row_scale + bias_ref[head]
    soft = jnp.maximum(pre, 0.0) + jnp.log1p(jnp.exp(-jnp.abs(pre)))
    log_decay = jnp.where(live, -rate_ref[head] * soft, 0.0)

    def unit(block):
        v = sums[:, block * size : (block + 1) * size] * row_scale
        return v * lax.rsqrt(jnp.sum(v * v, axis=1, keepdims=True) + EPSILON)

    queries = unit(0) * HEAD_DIM ** (-0.5)
    keys = unit(1)
    values = sums[:, 2 * size : 3 * size] * row_scale

    def back(x, d):
        return pltpu.roll(x, d, 0)

    cumulative, tail = log_decay, jnp.zeros_like(log_decay)
    gaps = [jnp.zeros_like(log_decay)]
    for d in range(1, span):
        gaps.append(jnp.where(step >= d, log_decay + back(gaps[-1], 1), 0.0))
        cumulative = cumulative + jnp.where(step >= d, back(log_decay, d), 0.0)
        tail = tail + jnp.where(step < span - d, back(log_decay, rows - d), 0.0)
    decays = [jnp.exp(g) for g in gaps]
    grown = jnp.exp(cumulative)

    both = jnp.concatenate([keys, queries], axis=0)
    both_high, both_low = split_high_low(both)
    from_state = []
    for n in range(seq_count):
        s_high, s_low = split_high_low(state_ref[n])
        from_state.append(
            dot(both_high, s_high, (1, 0))
            + dot(both_low, s_high, (1, 0))
            + dot(both_high, s_low, (1, 0))
        )
    key_state = jnp.zeros_like(keys)
    query_state = jnp.zeros_like(keys)
    for n in range(seq_count):
        key_state = jnp.where(seq == n, from_state[n][:rows], key_state)
        query_state = jnp.where(seq == n, from_state[n][rows:], query_state)

    base = beta * (values - grown * key_state)
    lower, upper = [None], []
    for d in range(span):
        shifted = back(keys, d) if d else keys
        weight = jnp.where(step >= d, decays[d], 0.0)
        upper.append(weight * jnp.sum(queries * shifted, axis=1, keepdims=True))
        if d:
            lower.append(weight * beta * jnp.sum(keys * shifted, axis=1, keepdims=True))
    update = base
    for t in range(1, span):
        now = base
        for d in range(1, t + 1):
            now = now - lower[d] * back(update, d)
        update = jnp.where(step == t, now, update)
    attended = grown * query_state + upper[0] * update
    for d in range(1, span):
        attended = attended + upper[d] * back(update, d)
    out = attended * lax.rsqrt(jnp.mean(attended * attended, axis=1, keepdims=True) + EPSILON)
    out = (out * gain_ref[...]).astype(BF16)
    for k in range(head_ref.shape[0]):
        head_ref[k] = out

    k_high, k_low = split_high_low((keys * jnp.exp(tail)).T)
    k_all = jnp.concatenate([k_high, k_low, k_high], axis=1)
    for n in range(seq_count):
        u_high, u_low = split_high_low(jnp.where(seq == n, update, 0.0))
        u_all = jnp.concatenate([u_high, u_high, u_low], axis=0)
        last = n * span + span - 1
        new_ref[n] = state_ref[n] * grown[last : last + 1, :] + dot(k_all, u_all, (1, 0))


def delta_step(recv, state, lengths, rate, bias, gain):
    kv_count, rows, _ = recv.shape
    size = state.shape[1]
    smem = pl.BlockSpec(memory_space=pltpu.SMEM)
    return pl.pallas_call(
        delta_kernel,
        out_shape=(
            jax.ShapeDtypeStruct((kv_count, rows, size), BF16),
            jax.ShapeDtypeStruct(state.shape, F32),
        ),
        in_specs=full(2) + [smem] * 3 + full(1),
        out_specs=tuple(full(2)),
        name="delta",
    )(recv, state, lengths, rate, bias, gain)


def attend_kernel(heads_ref, lengths_ref, w_ref, flat_ref, part_ref, picker_ref, base_ref):
    rows, slots = picker_ref.shape
    batch = lengths_ref.shape[1]
    span = rows // batch
    lengths = jnp.broadcast_to(lengths_ref[...].astype(F32), (batch, batch)).astype(BF16)
    before = lax.broadcasted_iota(jnp.int32, (rows, batch), 1)
    row_seq = lax.broadcasted_iota(jnp.int32, (rows, batch), 0) // span
    ahead = dot((before < row_seq).astype(BF16), lengths, (1, 1))
    limit = dot((before == row_seq).astype(BF16), lengths, (1, 1))
    step = (lax.broadcasted_iota(jnp.int32, (rows, batch), 0) % span).astype(F32)
    target = jnp.where(step < limit, ahead + step, -1.0)
    target = jnp.concatenate([target] * (slots // batch), axis=1)
    slot = lax.broadcasted_iota(jnp.int32, (rows, slots), 1).astype(F32)
    picker = (target == slot).astype(BF16)
    picker_ref[...] = picker
    heads = heads_ref[...].reshape(rows, heads_ref.shape[2])
    packed = dot(picker, heads, (0, 0)).astype(BF16)
    part_ref[...] = dot(w_ref[...], packed, (0, 1)).astype(BF16)
    base_ref[...] = dot(flat_ref[...], picker, (1, 0)).astype(BF16)


def attend(heads, lengths, w_out, flat_t, slots):
    rows = flat_t.shape[1]
    return pl.pallas_call(
        attend_kernel,
        out_shape=(
            jax.ShapeDtypeStruct((w_out.shape[1], slots), BF16),
            jax.ShapeDtypeStruct((rows, slots), BF16),
            jax.ShapeDtypeStruct((flat_t.shape[0], slots), BF16),
        ),
        in_specs=full(4),
        out_specs=tuple(full(3)),
        name="attend",
    )(heads, lengths, w_out, flat_t)


def gate_kernel(x_ref, gain_ref, wg_ref, wu_ref, out_ref):
    kv_count, local, wide = out_ref.shape
    units = wg_ref.shape[1]
    x = features_of(x_ref)
    squared = (x * x).astype(BF16)
    normed = (x * gain_ref[...]).astype(BF16)
    ones = jnp.ones((x.shape[0], 128), BF16)

    def put(at, value):
        width = value.shape[1]
        out_ref[:, :, at : at + width] = value.astype(BF16).reshape(kv_count, local, width)

    half = wide // 2
    put(0, dot(normed, wg_ref[...], (0, 0)))
    put(half, dot(normed, wu_ref[...], (0, 0)))
    put(units, dot(squared, ones, (0, 0))[:, : half - units])


def gate(x, gain, w_gate, w_up, kv_count):
    rows = x.shape[-1]
    return pl.pallas_call(
        gate_kernel,
        out_shape=jax.ShapeDtypeStruct((kv_count, rows // kv_count, 768), BF16),
        in_specs=full(4),
        out_specs=pl.BlockSpec(memory_space=pltpu.VMEM),
        name="gate",
    )(x, gain, w_gate, w_up)


def body(
    tokens,
    lengths,
    state,
    attn_gain,
    w_query,
    w_key,
    w_value,
    w_beta,
    w_alpha,
    decay_rate,
    decay_bias,
    out_gain,
    w_out,
    mix_gain,
    w_gate,
    w_up,
    w_down,
):
    kv_count = lax.axis_size("kv")
    batch_all, span_len, own_cols = tokens.shape
    row_count = batch_all * span_len
    slots = 256

    flat_t = tokens.reshape(row_count, own_cols).T
    gathered = gather_features(flat_t)
    sent = project(
        gathered, attn_gain[:, None], w_query, w_key, w_value, w_beta, w_alpha, kv_count
    )
    heads, updated = delta_step(
        swap(sent, "kv"), state, lengths, decay_rate, decay_bias, out_gain[None, :]
    )
    attn_part, picker, base_rows = attend(
        swap(heads, "kv"), lengths[None, :], w_out, flat_t, slots
    )
    middle = (base_rows.astype(F32) + sum_to_owner(attn_part)).astype(BF16)
    share = gate(gather_features(middle), mix_gain[:, None], w_gate, w_up, kv_count)
    share = swap(share, "kv").astype(F32).sum(axis=0)
    units = w_gate.shape[1]
    share_scale = lax.rsqrt(share[:, units : units + 1] / D + EPSILON)
    hidden = (
        jax.nn.silu(share[:, :units] * share_scale)
        * (share[:, 384 : 384 + units] * share_scale)
    ).astype(BF16)
    hidden_every = spread(hidden, "kv").reshape(slots, units)
    down_part = dot(w_down, hidden_every, (0, 1)).astype(BF16)
    result = (middle.astype(F32) + sum_to_owner(down_part)).astype(BF16)
    mixed = dot(result, picker, (1, 1)).astype(BF16)
    return (mixed.T.reshape(batch_all, span_len, own_cols), updated)


def solution(mesh):
    split = Mesh(mesh.devices.reshape(mesh.shape["kv"], -1, 2), ("kv", "z", "c"))
    tp = ("z", "c")
    return jax.shard_map(
        body,
        mesh=split,
        in_specs=(
            P(None, None, ("kv", "z", "c")),
            P(),
            P("kv", None, tp),
            P("kv"),
            P("kv", tp),
            P("kv", tp),
            P("kv", tp),
            P(),
            P(),
            P(),
            P(),
            P(),
            P(tp, "kv"),
            P("kv"),
            P("kv", tp),
            P("kv", tp),
            P(tp, "kv"),
        ),
        out_specs=(P(None, None, ("kv", "z", "c")), P("kv", None, tp)),
        check_vma=False,
    )
```

time: 163 us -> 160 us (0.982)
  blocking collectives: 70.8 us -> 89.2 us
  Pallas kernels: 0 us -> 10.7 us
  waiting for transfers between devices: 33.3 us -> 23 us
  starting transfers between devices: 29.6 us -> 23.1 us
  matrix products: 5.84 us -> 0.38 us
  local copies, waits for them, and re-layouts: 17 us -> 12 us
  other arithmetic: 3.8 us -> 0.43 us
    all_to_all x4 -> x5, blocking collectives: 52.8 us -> 70.3 us  [swap(): return lax.all_to_all(tiles, axis, split_axis=0, concat_axis=0, tiled=True)]
    pallas_call x0 -> x4, Pallas kernels: none -> 10.7 us  [the longest x1 3.21 us: project(): pl.pallas_call(project_kernel, out_shape=jax.ShapeDtypeStruct((kv_count,...]
    all_to_all x4 -> x3, waiting for transfers between devices: 33.3 us -> 23 us  [swap(): return lax.all_to_all(tiles, axis, split_axis=0, concat_axis=0, tiled=True)]
    all_to_all x4 -> x3, starting transfers between devices: 29.6 us -> 23.1 us  [swap(): return lax.all_to_all(tiles, axis, split_axis=0, concat_axis=0, tiled=True)]
    dot_general x18 -> x2, matrix products: 5.84 us -> 0.38 us  [dot(): lax.dot_general(a, b, ((dims[:1], dims[1:]), ((), ())), preferred_element...]
    dynamic_slice x5 -> x0, local copies, waits for them, and re-layouts: 2.88 us -> none  [the longest x1 0.78 us: body(): alpha_col = lax.dynamic_slice_in_dim(alpha_rows, head, 1, 1)]
    unnamed x32 -> x28, local copies, waits for them, and re-layouts: 7.94 us -> 8.67 us
  transfers between devices with their start and end apart: 4 -> 3, of which waited for: 4 -> 3; matrix products, arithmetic and copies ran while one was open for 4% -> 4% of each run, Pallas kernels for 0% -> 0%
where the time goes in v2:
time: 160 us; the launch traced here: 159 us
  blocking collectives  89.2 us (56%)
  starting transfers between devices  23.1 us (14%)
  waiting for transfers between devices  23 us (14%)
  local copies, waits for them, and re-layouts  12 us (8%)
  Pallas kernels  10.7 us (7%)
    all_to_all x5, blocking collectives, swap(): return lax.all_to_all(tiles, axis, split_axis=0, concat_axis=0, tiled=True)  70.3 us
    all_to_all x3, starting transfers between devices, swap(): return lax.all_to_all(tiles, axis, split_axis=0, concat_axis=0, tiled=True)  23.1 us
    all_to_all x3, waiting for transfers between devices, swap(): return lax.all_to_all(tiles, axis, split_axis=0, concat_axis=0, tiled=True)  23 us
    all_gather x2, blocking collectives, gather_features(): return lax.all_gather(spread(shard, 'z'), 'c', axis=0, tiled=False)  10.1 us
    all_gather x2, blocking collectives, sum_to_owner(): pair = lax.all_gather(part, 'c', axis=0, tiled=False)  8.79 us
    unnamed x28, local copies, waits for them, and re-layouts  8.67 us
    pallas_call x1, Pallas kernels, project(): pl.pallas_call(project_kernel, out_shape=jax.ShapeDtypeStruct((kv_count,...  3.21 us
  transfers between devices with their start and end apart: 3, of which 3 were waited for; matrix products, arithmetic and copies ran while one was open for 4% of the time, Pallas kernels for 0%

profile of v2, /device:TPU:1, one launch (start us, length us, event | category | flops | bytes accessed | tf_op | source)
XLA Modules:
  0.0 159.5 jit_solution(4714683589452076228)
XLA Ops:
  0.6 0.0 copy-start
  0.6 0.9 copy.60
  1.5 0.1 copy.61
  1.6 0.7 broadcast_in_dim.14
  2.3 15.7 %all-to-all-start = ((bf16[16,8,512]{2,1,0:T(8,128)(2,1)}), bf16[16,8,512]{2,1,0:T(8,128)(2,1)S(1)}, u32[]{:S(2)}, u32[]{:S(2)}) async-start(bf16[16,8,512]{2,1,0:T(8,128)(2,1)} %broadcast_in_dim.14), calls=%async_computation | async-start | bytes 262144 | tf_op jit(solution)/shard_map/all_to_all | solution.py:16
  18.0 0.0 copy-start.9
  18.1 0.7 copy-done.9
  18.7 0.8 copy.62.gain_ref
  19.5 1.3 copy.63.wb_ref
  20.8 0.0 copy-done.3
  20.9 1.4 copy.64.wa_ref
  22.2 7.8 %all-to-all-done = bf16[16,8,512]{2,1,0:T(8,128)(2,1)S(1)} async-done(((bf16[16,8,512]{2,1,0:T(8,128)(2,1)}), bf16[16,8,512]{2,1,0:T(8,128)(2,1)S(1)}, u32[]{:S(2)}, u32[]{:S(2)}) %all-to-all-start) | async-done | bytes 131104 | tf_op jit(solution)/shard_map/all_to_all | solution.py:16
  30.0 5.5 %all-gather = bf16[32,8,512]{2,1,0:T(8,128)(2,1)} all-gather(bf16[16,8,512]{2,1,0:T(8,128)(2,1)S(1)} %all-to-all-done), channel_id=2, replica_groups=mesh['kv'=16,'z'=16,'c'=2] {'c'}, dimensions={0}, use_global_device_ids=true | all-gather | bytes 393216 | tf_op jit(solution)/shard_map/all_gather | solution.py:24
  35.5 3.2 %project.1 = bf16[16,32,512]{2,1,0:T(8,128)(2,1)} custom-call(bf16[2,16,8,512]{3,2,1,0:T(8,128)(2,1)} %bitcast.17, f32[256,1]{1,0:T(8,128)} %copy.62.gain_ref, bf16[256,128]{1,0:T(8,128)(2,1)} %wq_ref.1, bf16[256,128]{1,0:T(8,128)(2,1)} %wk_ref.1, bf16[256,128]{1,0:T(8,128)(2,1)} %wv_ref.1, bf16[4096,32]{1,0:T(8,128)(2,1)} %copy.63.wb_ref, ...), custom_call_target="tpu_custom_call" | custom-call | tf_op jit(solution)/shard_map/project/pallas_call | solution.py:96
  38.8 17.6 %all_to_all.40.recv_ref = bf16[16,32,512]{2,1,0:T(8,128)(2,1)} all-to-all(bf16[16,32,512]{2,1,0:T(8,128)(2,1)} %project.1), channel_id=1, replica_groups=mesh['kv'=16,'z'=16,'c'=2] {'kv'}, dimensions={0} | all-to-all | bytes 1048576 | tf_op jit(solution)/shard_map/all_to_all | solution.py:16
  56.4 2.8 %delta.1 = (bf16[16,32,128]{2,1,0:T(8,128)(2,1)}, f32[8,128,128]{2,1,0:T(8,128)}) custom-call(bf16[16,32,512]{2,1,0:T(8,128)(2,1)} %all_to_all.40.recv_ref, f32[8,128,128]{2,1,0:T(8,128)} %state_ref.1, s32[128]{0:T(128)} %lengths_ref.1, f32[32]{0:T(128)} %rate_ref.1, f32[32]{0:T(128)} %bias_ref.1, f32[1,128]{1,0:T(1,128)} %bitcast.29), custom_call_target="tpu_custom_call" | custom-call | tf_op jit(solution)/shard_map/delta/pallas_call | solution.py:209
  59.1 3.5 %all-to-all-start.2 = ((bf16[16,32,128]{2,1,0:T(8,128)(2,1)}), bf16[16,32,128]{2,1,0:T(8,128)(2,1)S(1)}, u32[]{:S(2)}, u32[]{:S(2)}) async-start(bf16[16,32,128]{2,1,0:T(8,128)(2,1)} %get-tuple-element.7), calls=%async_computation.2 | async-start | bytes 262144 | tf_op jit(solution)/shard_map/all_to_all | solution.py:16
  62.6 6.8 %all-to-all-done.2.heads_ref = bf16[16,32,128]{2,1,0:T(8,128)(2,1)S(1)} async-done(((bf16[16,32,128]{2,1,0:T(8,128)(2,1)}), bf16[16,32,128]{2,1,0:T(8,128)(2,1)S(1)}, u32[]{:S(2)}, u32[]{:S(2)}) %all-to-all-start.2) | async-done | bytes 131104 | tf_op jit(solution)/shard_map/all_to_all | solution.py:16
  69.5 0.6 copy-done.1
  70.1 2.3 %attend.1 = (bf16[256,256]{1,0:T(8,128)(2,1)}, bf16[512,256]{1,0:T(8,128)(2,1)}, bf16[8,256]{1,0:T(8,128)(2,1)}) custom-call(bf16[16,32,128]{2,1,0:T(8,128)(2,1)} %copy-done.1, s32[1,128]{1,0:T(1,128)} %bitcast.26, bf16[128,256]{1,0:T(8,128)(2,1)} %w_ref.1, bf16[8,512]{1,0:T(8,128)(2,1)} %bitcast.25), custom_call_target="tpu_custom_call" | custom-call | tf_op jit(solution)/shard_map/attend/pallas_call | solution.py:244
  72.4 4.7 %all-gather.1 = bf16[512,256]{1,0:T(8,128)(2,1)S(1)} all-gather(bf16[256,256]{1,0:T(8,128)(2,1)} %get-tuple-element.10), channel_id=3, replica_groups=mesh['kv'=16,'z'=16,'c'=2] {'c'}, dimensions={0}, use_global_device_ids=true | all-gather | bytes 393216 | tf_op jit(solution)/shard_map/all_gather | solution.py:30
  77.1 15.0 %all_to_all.41 = bf16[16,8,256]{2,1,0:T(8,128)(2,1)S(1)} all-to-all(bf16[16,8,256]{2,1,0:T(8,128)(2,1)S(1)} %dynamic-slice_reduce_fusion.1), channel_id=1, replica_groups=mesh['kv'=16,'z'=16,'c'=2] {'z'}, dimensions={0} | all-to-all | bytes 131072 | tf_op jit(solution)/shard_map/all_to_all | solution.py:16
  92.1 0.0 copy-start.5
  92.1 0.6 copy-done.8
  92.8 0.6 broadcast_in_dim.34
  93.4 3.9 %all-to-all-start.4 = ((bf16[16,8,256]{2,1,0:T(8,128)(2,1)}), bf16[16,8,256]{2,1,0:T(8,128)(2,1)S(1)}, u32[]{:S(2)}, u32[]{:S(2)}) async-start(bf16[16,8,256]{2,1,0:T(8,128)(2,1)} %broadcast_in_dim.34), calls=%async_computation.4 | async-start | bytes 131072 | tf_op jit(solution)/shard_map/all_to_all | solution.py:16
  97.2 0.0 copy-start.10
  97.3 0.7 copy-done.10
  97.9 0.8 copy.65.gain_ref
  98.7 0.0 copy-done.5
  98.7 0.8 copy.66.wg_ref
  99.5 0.1 copy-done.6
  99.6 0.8 copy.67.wu_ref
  100.5 8.4 %all-to-all-done.4 = bf16[16,8,256]{2,1,0:T(8,128)(2,1)S(1)} async-done(((bf16[16,8,256]{2,1,0:T(8,128)(2,1)}), bf16[16,8,256]{2,1,0:T(8,128)(2,1)S(1)}, u32[]{:S(2)}, u32[]{:S(2)}) %all-to-all-start.4) | async-done | bytes 65568 | tf_op jit(solution)/shard_map/all_to_all | solution.py:16
  108.8 4.6 %all-gather.2 = bf16[32,8,256]{2,1,0:T(8,128)(2,1)} all-gather(bf16[16,8,256]{2,1,0:T(8,128)(2,1)S(1)} %all-to-all-done.4), channel_id=4, replica_groups=mesh['kv'=16,'z'=16,'c'=2] {'c'}, dimensions={0}, use_global_device_ids=true | all-gather | bytes 196608 | tf_op jit(solution)/shard_map/all_gather | solution.py:24
  113.4 2.4 %gate.1 = bf16[16,16,768]{2,1,0:T(8,128)(2,1)} custom-call(bf16[2,16,8,256]{3,2,1,0:T(8,128)(2,1)} %bitcast.23, f32[256,1]{1,0:T(8,128)} %copy.65.gain_ref, bf16[256,344]{1,0:T(8,128)(2,1)} %copy.66.wg_ref, bf16[256,344]{1,0:T(8,128)(2,1)} %copy.67.wu_ref), custom_call_target="tpu_custom_call" | custom-call | tf_op jit(solution)/shard_map/gate/pallas_call | solution.py:277
  115.8 13.0 %all_to_all.42 = bf16[16,16,768]{2,1,0:T(8,128)(2,1)S(1)} all-to-all(bf16[16,16,768]{2,1,0:T(8,128)(2,1)} %gate.1), channel_id=1, replica_groups=mesh['kv'=16,'z'=16,'c'=2] {'kv'}, dimensions={0} | all-to-all | bytes 786432 | tf_op jit(solution)/shard_map/all_to_all | solution.py:16
  128.8 0.1 convert_reduce_fusion
  128.9 0.2 fusion.5
  129.1 0.1 fusion.2
  129.2 10.3 %all_to_all.43 = bf16[16,16,344]{2,1,0:T(8,128)(2,1)S(1)} all-to-all(bf16[16,16,344]{2,1,0:T(8,128)(2,1)S(1)} %broadcast_in_dim.36), channel_id=1, replica_groups=mesh['kv'=16,'z'=16,'c'=2] {'kv'}, dimensions={0} | all-to-all | bytes 352256 | tf_op jit(solution)/shard_map/all_to_all | solution.py:16
  139.5 0.2 fusion
  139.8 4.1 %all-gather.3 = bf16[512,256]{0,1:T(8,128)(2,1)S(1)} all-gather(bf16[256,256]{0,1:T(8,128)(2,1)S(1)} %fusion), channel_id=5, replica_groups=mesh['kv'=16,'z'=16,'c'=2] {'c'}, dimensions={0}, use_global_device_ids=true | all-gather | bytes 393216 | tf_op jit(solution)/shard_map/all_gather | solution.py:30
  143.8 0.1 copy.68
  144.0 14.4 %all_to_all.44 = bf16[16,8,256]{2,1,0:T(8,128)(2,1)S(1)} all-to-all(bf16[16,8,256]{2,1,0:T(8,128)(2,1)S(1)} %dynamic-slice_reduce_fusion), channel_id=1, replica_groups=mesh['kv'=16,'z'=16,'c'=2] {'z'}, dimensions={0} | all-to-all | bytes 131072 | tf_op jit(solution)/shard_map/all_to_all | solution.py:16
  158.4 0.2 convolution_convert_fusion.1
  158.6 0.2 copy.69
  158.8 0.7 copy.70
  (17 shorter events, 0.1 us)
Async XLA Ops:
  0.6 138.9 %copy-start = (bf16[344,256]{1,0:T(8,128)(2,1)S(1)}, bf16[344,256]{1,0:T(8,128)(2,1)}, u32[]{:S(2)}) copy-start(bf16[344,256]{1,0:T(8,128)(2,1)} %param.33) | copy-start | bytes 528388
  1.6 0.7 copy-start.7
  1.6 17.9 %copy-start.2 = (bf16[4096,32]{0,1:T(8,128)(2,1)S(1)}, bf16[4096,32]{0,1:T(8,128)(2,1)}, u32[]{:S(2)}) copy-start(bf16[4096,32]{0,1:T(8,128)(2,1)} %param.24) | copy-start | bytes 786436
  2.3 27.7 %all-to-all-start = ((bf16[16,8,512]{2,1,0:T(8,128)(2,1)}), bf16[16,8,512]{2,1,0:T(8,128)(2,1)S(1)}, u32[]{:S(2)}, u32[]{:S(2)}) async-start(bf16[16,8,512]{2,1,0:T(8,128)(2,1)} %broadcast_in_dim.14), calls=%async_computation | async-start | bytes 262144 | tf_op jit(solution)/shard_map/all_to_all | solution.py:16
  18.0 0.7 copy-start.9
  19.5 1.3 copy-start.3
  59.1 10.3 %all-to-all-start.2 = ((bf16[16,32,128]{2,1,0:T(8,128)(2,1)}), bf16[16,32,128]{2,1,0:T(8,128)(2,1)S(1)}, u32[]{:S(2)}, u32[]{:S(2)}) async-start(bf16[16,32,128]{2,1,0:T(8,128)(2,1)} %get-tuple-element.7), calls=%async_computation.2 | async-start | bytes 262144 | tf_op jit(solution)/shard_map/all_to_all | solution.py:16
  69.4 0.6 copy-start.1
  92.1 0.7 copy-start.8
  92.1 6.6 %copy-start.5 = (bf16[256,344]{0,1:T(8,128)(2,1)S(1)}, bf16[256,344]{0,1:T(8,128)(2,1)}, u32[]{:S(2)}) copy-start(bf16[256,344]{0,1:T(8,128)(2,1)} %param.31) | copy-start | bytes 528388
  93.4 15.4 %all-to-all-start.4 = ((bf16[16,8,256]{2,1,0:T(8,128)(2,1)}), bf16[16,8,256]{2,1,0:T(8,128)(2,1)S(1)}, u32[]{:S(2)}, u32[]{:S(2)}) async-start(bf16[16,8,256]{2,1,0:T(8,128)(2,1)} %broadcast_in_dim.34), calls=%async_computation.4 | async-start | bytes 131072 | tf_op jit(solution)/shard_map/all_to_all | solution.py:16
  97.2 0.7 copy-start.10
  98.7 0.9 copy-start.6
  144.0 14.5 %copy-start.4 = (bf16[512,256]{1,0:T(8,128)(2,1)S(1)}, bf16[512,256]{1,0:T(8,128)(2,1)}, u32[]{:S(2)}) copy-start(bf16[512,256]{1,0:T(8,128)(2,1)} %get-tuple-element.8) | copy-start | bytes 786436

commit v3 on v2

v3 whole, which is shorter than its diff:
```python
import jax
import jax.numpy as jnp
from jax import lax
from jax.experimental import pallas as pl
from jax.experimental.pallas import tpu as pltpu
from jax.sharding import Mesh, PartitionSpec as P

D = 4096
HEAD_DIM = 128
EPSILON = 1e-06
F32 = jnp.float32
BF16 = jnp.bfloat16
PARAMS = pltpu.CompilerParams(vmem_limit_bytes=12 * 1024 * 1024)


def swap(tiles, axis):
    return lax.all_to_all(tiles, axis, split_axis=0, concat_axis=0, tiled=True)


def spread(shard, axis):
    return swap(jnp.broadcast_to(shard[None], (lax.axis_size(axis), *shard.shape)), axis)


def gather_features(shard):
    return lax.all_gather(spread(shard, "z"), "c", axis=0, tiled=False)


def pair_sum(part, core):
    feats, rows = part.shape
    z_count, c_count = lax.axis_size("z"), lax.axis_size("c")
    pair = lax.all_gather(part, "c", axis=0, tiled=False)
    pair = pair.reshape(c_count, z_count, c_count, -1, rows)
    mine = lax.dynamic_index_in_dim(pair, core, 2, keepdims=False)
    return mine.astype(F32).sum(axis=0).astype(BF16)


def dot(a, b, dims):
    return lax.dot_general(a, b, ((dims[:1], dims[1:]), ((), ())), preferred_element_type=F32)


def split_high_low(x):
    high = x.astype(BF16)
    return high, (x - high.astype(F32)).astype(BF16)


def full(shape_of):
    return [pl.BlockSpec(memory_space=pltpu.VMEM)] * shape_of


def features_of(ref, *at):
    c_count, z_count = ref.shape[:2]
    tiles = [ref[(c, z, *at)].astype(F32) for z in range(z_count) for c in range(c_count)]
    return jnp.concatenate(tiles, axis=0).T


def normed_rows(x, gain_ref):
    return (x * gain_ref[...]).astype(BF16), jnp.sum(x * x, axis=1, keepdims=True)


def project_kernel(x_ref, gain_ref, wq_ref, wk_ref, wv_ref, wb_ref, wa_ref, out_ref):
    width = gain_ref.shape[1]
    first = pl.multiple_of(lax.axis_index("kv") * width, width)
    head = lax.axis_index("z") * lax.axis_size("c") + lax.axis_index("c")
    kv_count, local_rows, _ = out_ref.shape
    span = x_ref.shape[2]
    seqs = local_rows // span
    heads = wb_ref.shape[0]
    own = lax.broadcasted_iota(jnp.int32, (heads, width), 0) == head

    def own_row(ref):
        tile = ref[:, pl.ds(first, width)].astype(F32)
        return jnp.sum(jnp.where(own, tile, 0.0), axis=0, keepdims=True)

    row = lax.broadcasted_iota(jnp.int32, (128, width), 0)
    small = jnp.where(row == 0, own_row(wb_ref), jnp.where(row == 1, own_row(wa_ref), 0.0))
    small = small.astype(BF16)
    weights = jnp.concatenate([wq_ref[...], wk_ref[...], wv_ref[...]], axis=1)
    lane = lax.broadcasted_iota(jnp.int32, (x_ref.shape[4], 128), 1)
    for t in range(span):
        normed, squares = normed_rows(features_of(x_ref, t), gain_ref)
        at = slice(t * seqs, (t + 1) * seqs)
        wide = dot(normed, weights, (1, 0))
        extra = jnp.where(lane == 2, squares, dot(normed, small, (1, 1)))
        out_ref[:, at, :384] = wide.reshape(kv_count, seqs, 384).astype(BF16)
        out_ref[:, at, 384:] = extra.reshape(kv_count, seqs, 128).astype(BF16)


def project(x, gain, wq, wk, wv, wb, wa, kv_count):
    rows = x.shape[2] * x.shape[4]
    return pl.pallas_call(
        project_kernel,
        out_shape=jax.ShapeDtypeStruct((kv_count, rows // kv_count, 512), BF16),
        in_specs=full(7),
        out_specs=pl.BlockSpec(memory_space=pltpu.VMEM),
        compiler_params=PARAMS,
        name="project",
    )(x, gain, wq, wk, wv, wb, wa)


def delta_kernel(
    recv_ref, state_ref, lengths_ref, rate_ref, bias_ref, gain_ref, head_ref, new_ref
):
    seq_count, size, _ = state_ref.shape
    rows = recv_ref.shape[1]
    span = rows // seq_count
    first = lax.axis_index("kv") * seq_count
    head = lax.axis_index("z") * lax.axis_size("c") + lax.axis_index("c")
    sums = recv_ref[0].astype(F32)
    for k in range(1, recv_ref.shape[0]):
        sums = sums + recv_ref[k].astype(F32)

    def lanes(column):
        return jnp.broadcast_to(column, (rows, size))

    row_scale = lanes(lax.rsqrt(sums[:, 386:387] / D + EPSILON))
    row = lax.broadcasted_iota(jnp.int32, (rows, size), 0)
    step = row // seq_count
    seq = row % seq_count
    limit = jnp.zeros((rows, size), jnp.int32)
    for n in range(seq_count):
        limit = jnp.where(seq == n, lengths_ref[first + n], limit)
    live = step < limit
    beta = jnp.where(live, jax.nn.sigmoid(lanes(sums[:, 384:385]) * row_scale), 0.0)
    pre = lanes(sums[:, 385:386]) * row_scale + bias_ref[head]
    soft = jnp.maximum(pre, 0.0) + jnp.log1p(jnp.exp(-jnp.abs(pre)))
    log_decay = jnp.where(live, -rate_ref[head] * soft, 0.0)

    def unit(block):
        v = sums[:, block * size : (block + 1) * size] * row_scale
        return v * lax.rsqrt(jnp.sum(v * v, axis=1, keepdims=True) + EPSILON)

    queries = unit(0) * HEAD_DIM ** (-0.5)
    keys = unit(1)
    values = sums[:, 2 * size : 3 * size] * row_scale

    def back(x, d):
        return pltpu.roll(x, d * seq_count, 0)

    cumulative, tail = log_decay, jnp.zeros_like(log_decay)
    gaps = [jnp.zeros_like(log_decay)]
    for d in range(1, span):
        gaps.append(jnp.where(step >= d, log_decay + back(gaps[-1], 1), 0.0))
        cumulative = cumulative + jnp.where(step >= d, back(log_decay, d), 0.0)
        tail = tail + jnp.where(step < span - d, back(log_decay, span - d), 0.0)
    decays = [jnp.exp(g) for g in gaps]
    grown = jnp.exp(cumulative)

    both = jnp.concatenate([keys, queries], axis=0)
    both_high, both_low = split_high_low(both)
    from_state = []
    for n in range(seq_count):
        s_high, s_low = split_high_low(state_ref[n])
        from_state.append(
            dot(both_high, s_high, (1, 0))
            + dot(both_low, s_high, (1, 0))
            + dot(both_high, s_low, (1, 0))
        )
    key_state = jnp.zeros_like(keys)
    query_state = jnp.zeros_like(keys)
    for n in range(seq_count):
        key_state = jnp.where(seq == n, from_state[n][:rows], key_state)
        query_state = jnp.where(seq == n, from_state[n][rows:], query_state)

    base = beta * (values - grown * key_state)
    lower, upper = [None], []
    for d in range(span):
        shifted = back(keys, d) if d else keys
        weight = jnp.where(step >= d, decays[d], 0.0)
        upper.append(weight * jnp.sum(queries * shifted, axis=1, keepdims=True))
        if d:
            lower.append(weight * beta * jnp.sum(keys * shifted, axis=1, keepdims=True))
    update = base
    for t in range(1, span):
        now = base
        for d in range(1, t + 1):
            now = now - lower[d] * back(update, d)
        update = jnp.where(step == t, now, update)
    attended = grown * query_state + upper[0] * update
    for d in range(1, span):
        attended = attended + upper[d] * back(update, d)
    out = attended * lax.rsqrt(jnp.mean(attended * attended, axis=1, keepdims=True) + EPSILON)
    out = (out * gain_ref[...]).astype(BF16)
    for k in range(head_ref.shape[0]):
        head_ref[k] = out

    k_high, k_low = split_high_low((keys * jnp.exp(tail)).T)
    k_all = jnp.concatenate([k_high, k_low, k_high], axis=1)
    for n in range(seq_count):
        u_high, u_low = split_high_low(jnp.where(seq == n, update, 0.0))
        u_all = jnp.concatenate([u_high, u_high, u_low], axis=0)
        last = rows - seq_count + n
        new_ref[n] = state_ref[n] * grown[last : last + 1, :] + dot(k_all, u_all, (1, 0))


def delta_step(recv, state, lengths, rate, bias, gain):
    kv_count, rows, _ = recv.shape
    size = state.shape[1]
    smem = pl.BlockSpec(memory_space=pltpu.SMEM)
    return pl.pallas_call(
        delta_kernel,
        out_shape=(
            jax.ShapeDtypeStruct((kv_count, rows, size), BF16),
            jax.ShapeDtypeStruct(state.shape, F32),
        ),
        in_specs=full(2) + [smem] * 3 + full(1),
        out_specs=tuple(full(2)),
        compiler_params=PARAMS,
        name="delta",
    )(recv, state, lengths, rate, bias, gain)


def attend_kernel(heads_ref, lengths_ref, w_ref, flat_ref, part_ref, picker_ref, base_ref):
    slots, rows = picker_ref.shape
    span, _, batch = flat_ref.shape
    kv_count, local_rows, size = heads_ref.shape
    seqs = local_rows // span
    lengths = jnp.broadcast_to(lengths_ref[...].astype(F32), (8, batch))
    above = lax.broadcasted_iota(jnp.int32, (batch, batch), 0)
    across = lax.broadcasted_iota(jnp.int32, (batch, batch), 1)
    ahead = dot(lengths.astype(BF16), (above < across).astype(BF16), (1, 0))[:1]
    slot = lax.broadcasted_iota(jnp.int32, (slots, batch), 0).astype(F32)
    for t in range(span):
        target = jnp.where(lengths[:1] > t, ahead + t, -1.0)
        picker_ref[:, t * batch : (t + 1) * batch] = (slot == target).astype(BF16)
    picker = picker_ref[...]
    heads = heads_ref[...].astype(F32)
    heads = jnp.concatenate(
        [
            heads[:, t * seqs : (t + 1) * seqs].reshape(kv_count * seqs, size)
            for t in range(span)
        ],
        axis=0,
    ).astype(BF16)
    packed = dot(picker, heads, (1, 0)).astype(BF16)
    part_ref[...] = dot(packed, w_ref[...], (1, 0)).T.astype(BF16)
    flat = jnp.concatenate([flat_ref[t] for t in range(span)], axis=1)
    base_ref[...] = dot(flat, picker, (1, 1)).astype(BF16)


def attend(heads, lengths, w_out, flat, slots):
    span, own, batch = flat.shape
    return pl.pallas_call(
        attend_kernel,
        out_shape=(
            jax.ShapeDtypeStruct((w_out.shape[1], slots), BF16),
            jax.ShapeDtypeStruct((slots, span * batch), BF16),
            jax.ShapeDtypeStruct((own, slots), BF16),
        ),
        in_specs=full(4),
        out_specs=tuple(full(3)),
        compiler_params=PARAMS,
        name="attend",
    )(heads, lengths, w_out, flat)


def gate_kernel(x_ref, gain_ref, wg_ref, wu_ref, out_ref):
    kv_count, local, wide = out_ref.shape
    units = wg_ref.shape[0]
    normed, squares = normed_rows(features_of(x_ref), gain_ref)

    def put(at, value):
        width = value.shape[1]
        out_ref[:, :, at : at + width] = value.astype(BF16).reshape(kv_count, local, width)

    half = wide // 2
    put(0, dot(normed, wg_ref[...], (1, 1)))
    put(half, dot(normed, wu_ref[...], (1, 1)))
    put(units, jnp.broadcast_to(squares, (x_ref.shape[3], half - units)))


def gate(x, gain, w_gate, w_up, kv_count):
    rows = x.shape[-1]
    return pl.pallas_call(
        gate_kernel,
        out_shape=jax.ShapeDtypeStruct((kv_count, rows // kv_count, 768), BF16),
        in_specs=full(4),
        out_specs=pl.BlockSpec(memory_space=pltpu.VMEM),
        compiler_params=PARAMS,
        name="gate",
    )(x, gain, w_gate, w_up)


def finish_kernel(recv_ref, middle_ref, picker_ref, out_ref):
    total = middle_ref[...].astype(F32)
    for k in range(recv_ref.shape[0]):
        total = total + recv_ref[k].astype(F32)
    span, _, batch = out_ref.shape
    spread_out = dot(total.astype(BF16), picker_ref[...], (1, 0)).astype(BF16)
    for t in range(span):
        out_ref[t] = spread_out[:, t * batch : (t + 1) * batch]


def finish(recv, middle, picker, span):
    own = middle.shape[0]
    return pl.pallas_call(
        finish_kernel,
        out_shape=jax.ShapeDtypeStruct((span, own, picker.shape[1] // span), BF16),
        in_specs=full(3),
        out_specs=pl.BlockSpec(memory_space=pltpu.VMEM),
        compiler_params=PARAMS,
        name="finish",
    )(recv, middle, picker)


def body(
    tokens,
    lengths,
    state,
    attn_gain,
    w_query,
    w_key,
    w_value,
    w_beta,
    w_alpha,
    decay_rate,
    decay_bias,
    out_gain,
    w_out,
    mix_gain,
    w_gate,
    w_up,
    w_down,
):
    kv_count = lax.axis_size("kv")
    slots = 256

    core = lax.axis_index("c").astype(jnp.uint32)
    flat, core = lax.optimization_barrier((tokens.transpose(1, 2, 0), core))
    sent = project(
        gather_features(flat),
        attn_gain[None, :],
        w_query,
        w_key,
        w_value,
        w_beta.T,
        w_alpha.T,
        kv_count,
    )
    heads, updated = delta_step(
        swap(sent, "kv"), state, lengths, decay_rate, decay_bias, out_gain[None, :]
    )
    attn_part, picker, base_rows = attend(
        swap(heads, "kv"), lengths[None, :], w_out, flat, slots
    )
    attn_own = swap(pair_sum(attn_part, core), "z").astype(F32).sum(axis=0)
    middle = (base_rows.astype(F32) + attn_own).astype(BF16)
    share = gate(gather_features(middle), mix_gain[None, :], w_gate.T, w_up.T, kv_count)
    share = swap(share, "kv").astype(F32).sum(axis=0)
    units = w_gate.shape[1]
    share_scale = lax.rsqrt(share[:, units : units + 1] / D + EPSILON)
    hidden = (
        jax.nn.silu(share[:, :units] * share_scale)
        * (share[:, 384 : 384 + units] * share_scale)
    ).astype(BF16)
    hidden_every = spread(hidden, "kv").reshape(slots, units)
    down_part = dot(w_down, hidden_every, (0, 1)).astype(BF16)
    mixed = finish(swap(pair_sum(down_part, core), "z"), middle, picker, flat.shape[0])
    return (mixed.transpose(2, 0, 1), updated)


def solution(mesh):
    split = Mesh(mesh.devices.reshape(mesh.shape["kv"], -1, 2), ("kv", "z", "c"))
    tp = ("z", "c")
    return jax.shard_map(
        body,
        mesh=split,
        in_specs=(
            P(None, None, ("kv", "z", "c")),
            P(),
            P("kv", None, tp),
            P("kv"),
            P("kv", tp),
            P("kv", tp),
            P("kv", tp),
            P(),
            P(),
            P(),
            P(),
            P(),
            P(tp, "kv"),
            P("kv"),
            P("kv", tp),
            P("kv", tp),
            P(tp, "kv"),
        ),
        out_specs=(P(None, None, ("kv", "z", "c")), P("kv", None, tp)),
        check_vma=False,
    )
```

time: 160 us -> 149 us (0.931)
  blocking collectives: 89.2 us -> 140 us
  starting transfers between devices: 23.1 us -> 0 us
  waiting for transfers between devices: 23 us -> 0 us
  local copies, waits for them, and re-layouts: 12 us -> 2.95 us
  Pallas kernels: 10.7 us -> 4.22 us
    all_to_all x5 -> x8, blocking collectives: 70.3 us -> 122 us  [swap(): return lax.all_to_all(tiles, axis, split_axis=0, concat_axis=0, tiled=True)]
    all_to_all x3 -> x0, starting transfers between devices: 23.1 us -> none  [swap(): return lax.all_to_all(tiles, axis, split_axis=0, concat_axis=0, tiled=True)]
    all_to_all x3 -> x0, waiting for transfers between devices: 23 us -> none  [swap(): return lax.all_to_all(tiles, axis, split_axis=0, concat_axis=0, tiled=True)]
    unnamed x28 -> x34, local copies, waits for them, and re-layouts: 8.67 us -> 2.77 us
    pallas_call x1, Pallas kernels: 3.21 us -> 0.43 us  [project(): pl.pallas_call(project_kernel, out_shape=jax.ShapeDtypeStruct((kv_count,...]
    pallas_call x1, Pallas kernels: 2.42 us -> 0.37 us  [gate(): pl.pallas_call(gate_kernel, out_shape=jax.ShapeDtypeStruct((kv_count, row...]
    pallas_call x1, Pallas kernels: 2.27 us -> 0.57 us  [attend(): pl.pallas_call(attend_kernel, out_shape=(jax.ShapeDtypeStruct((w_out.shap...]
  transfers between devices with their start and end apart: 3 -> 0, of which waited for: 3 -> 0; matrix products, arithmetic and copies ran while one was open for 4% -> 0% of each run, Pallas kernels for 0% -> 0%
where the time goes in v3:
time: 149 us
  blocking collectives  140 us (94%)
  Pallas kernels  4.22 us (3%)
  local copies, waits for them, and re-layouts  2.95 us (2%)
    all_to_all x8, blocking collectives, swap(): return lax.all_to_all(tiles, axis, split_axis=0, concat_axis=0, tiled=True)  122 us
    all_gather x2, blocking collectives, gather_features(): return lax.all_gather(spread(shard, 'z'), 'c', axis=0, tiled=False)  9.32 us
    all_gather x2, blocking collectives, pair_sum(): pair = lax.all_gather(part, 'c', axis=0, tiled=False)  8.41 us

profile of v3, /device:TPU:1, one launch (start us, length us, event | category | flops | bytes accessed | tf_op | source)
XLA Modules:
  0.0 148.8 jit_solution(12289115240649734962)
XLA Ops:
  0.6 0.0 copy-start
  0.6 0.0 copy-start.10
  0.7 0.7 copy-done.10
  1.4 0.0 copy-start.8
  1.4 0.0 copy-start.3
  1.4 27.6 %all_to_all.40 = bf16[16,4,8,128]{3,2,1,0:T(8,128)(2,1)S(1)} all-to-all(bf16[16,4,8,128]{3,2,1,0:T(8,128)(2,1)S(1)} %broadcast_in_dim.14), channel_id=1, replica_groups=mesh['kv'=16,'z'=16,'c'=2] {'z'}, dimensions={0} | all-to-all | bytes 262144 | tf_op jit(solution)/shard_map/all_to_all | solution.py:17
  29.1 0.0 copy-start.2
  29.1 5.5 %all-gather = bf16[32,4,8,128]{3,2,1,0:T(8,128)(2,1)S(1)} all-gather(bf16[16,4,8,128]{3,2,1,0:T(8,128)(2,1)S(1)} %all_to_all.40), channel_id=2, replica_groups=mesh['kv'=16,'z'=16,'c'=2] {'c'}, dimensions={0}, use_global_device_ids=true | all-gather | bytes 393216 | tf_op jit(solution)/shard_map/all_gather | solution.py:25
  34.6 0.0 copy-done.8
  34.6 0.0 copy-done.3
  34.6 0.0 copy-done.2
  34.6 0.0 copy-done.6
  34.6 0.0 copy-done.7
  34.6 0.6 copy-done.12
  35.3 0.4 project.1
  35.7 0.0 copy-start.1
  35.7 0.0 copy-start.16
  35.7 17.4 %all_to_all.41.recv_ref = bf16[16,32,512]{2,1,0:T(8,128)(2,1)S(1)} all-to-all(bf16[16,32,512]{2,1,0:T(8,128)(2,1)S(1)} %project.1), channel_id=1, replica_groups=mesh['kv'=16,'z'=16,'c'=2] {'kv'}, dimensions={0} | all-to-all | bytes 1048576 | tf_op jit(solution)/shard_map/all_to_all | solution.py:17
  53.1 0.0 copy-done.1
  53.2 0.0 copy-done.16
  53.2 0.6 copy-done.11
  53.8 0.0 copy-done.14
  53.8 0.0 copy-done.15
  53.8 2.1 %delta.1 = (bf16[16,32,128]{2,1,0:T(8,128)(2,1)S(1)}, f32[8,128,128]{2,1,0:T(8,128)}) custom-call(bf16[16,32,512]{2,1,0:T(8,128)(2,1)S(1)} %all_to_all.41.recv_ref, f32[8,128,128]{2,1,0:T(8,128)S(1)} %copy-done.1, s32[128]{0:T(128)S(1)} %copy-done.11, f32[32]{0:T(128)S(1)} %copy-done.14, f32[32]{0:T(128)S(1)} %copy-done.15, f32[1,128]{1,0:T(1,128)S(1)} %bitcast.30), custom_call_target="tpu_custom_call" | custom-call | tf_op jit(solution)/shard_map/delta/pallas_call | solution.py:199
  55.9 10.2 %all_to_all.42.heads_ref = bf16[16,32,128]{2,1,0:T(8,128)(2,1)S(1)} all-to-all(bf16[16,32,128]{2,1,0:T(8,128)(2,1)S(1)} %get-tuple-element.10), channel_id=1, replica_groups=mesh['kv'=16,'z'=16,'c'=2] {'kv'}, dimensions={0} | all-to-all | bytes 262144 | tf_op jit(solution)/shard_map/all_to_all | solution.py:17
  66.2 0.0 copy-done.9
  66.2 0.6 attend.1
  66.8 4.2 %all-gather.1 = bf16[512,256]{1,0:T(8,128)(2,1)S(1)} all-gather(bf16[256,256]{1,0:T(8,128)(2,1)S(1)} %get-tuple-element.12), channel_id=3, replica_groups=mesh['kv'=16,'z'=16,'c'=2] {'c'}, dimensions={0}, use_global_device_ids=true | all-gather | bytes 393216 | tf_op jit(solution)/shard_map/all_gather | solution.py:31
  71.0 15.0 %all_to_all.43 = bf16[16,8,256]{2,1,0:T(8,128)(2,1)S(1)} all-to-all(bf16[16,8,256]{2,1,0:T(8,128)(2,1)S(1)} %dynamic-slice_reduce_fusion.1), channel_id=1, replica_groups=mesh['kv'=16,'z'=16,'c'=2] {'z'}, dimensions={0} | all-to-all | bytes 131072 | tf_op jit(solution)/shard_map/all_to_all | solution.py:17
  86.0 0.0 copy-start.5
  86.0 0.0 copy-start.4
  86.0 15.4 %all_to_all.44 = bf16[16,8,256]{2,1,0:T(8,128)(2,1)S(1)} all-to-all(bf16[16,8,256]{2,1,0:T(8,128)(2,1)S(1)} %broadcast_in_dim.34), channel_id=1, replica_groups=mesh['kv'=16,'z'=16,'c'=2] {'z'}, dimensions={0} | all-to-all | bytes 131072 | tf_op jit(solution)/shard_map/all_to_all | solution.py:17
  101.4 3.8 %all-gather.2 = bf16[32,8,256]{2,1,0:T(8,128)(2,1)S(1)} all-gather(bf16[16,8,256]{2,1,0:T(8,128)(2,1)S(1)} %all_to_all.44), channel_id=4, replica_groups=mesh['kv'=16,'z'=16,'c'=2] {'c'}, dimensions={0}, use_global_device_ids=true | all-gather | bytes 196608 | tf_op jit(solution)/shard_map/all_gather | solution.py:25
  105.2 0.0 copy-done.5
  105.2 0.0 copy-done.4
  105.2 0.7 copy-done.13
  105.9 0.4 gate.1
  106.2 12.3 %all_to_all.45 = bf16[16,16,768]{2,1,0:T(8,128)(2,1)S(1)} all-to-all(bf16[16,16,768]{2,1,0:T(8,128)(2,1)S(1)} %gate.1), channel_id=1, replica_groups=mesh['kv'=16,'z'=16,'c'=2] {'kv'}, dimensions={0} | all-to-all | bytes 786432 | tf_op jit(solution)/shard_map/all_to_all | solution.py:17
  118.6 0.1 convert_reduce_fusion
  118.6 0.2 fusion.5
  118.8 0.1 fusion.2
  119.0 10.1 %all_to_all.46 = bf16[16,16,344]{2,1,0:T(8,128)(2,1)S(1)} all-to-all(bf16[16,16,344]{2,1,0:T(8,128)(2,1)S(1)} %broadcast_in_dim.36), channel_id=1, replica_groups=mesh['kv'=16,'z'=16,'c'=2] {'kv'}, dimensions={0} | all-to-all | bytes 352256 | tf_op jit(solution)/shard_map/all_to_all | solution.py:17
  129.1 0.0 copy-done
  129.1 0.2 fusion
  129.3 4.2 %all-gather.3 = bf16[512,256]{0,1:T(8,128)(2,1)S(1)} all-gather(bf16[256,256]{0,1:T(8,128)(2,1)S(1)} %fusion), channel_id=5, replica_groups=mesh['kv'=16,'z'=16,'c'=2] {'c'}, dimensions={0}, use_global_device_ids=true | all-gather | bytes 393216 | tf_op jit(solution)/shard_map/all_gather | solution.py:31
  133.5 0.1 copy.24
  133.7 14.3 %all_to_all.47.recv_ref = bf16[16,8,256]{2,1,0:T(8,128)(2,1)S(1)} all-to-all(bf16[16,8,256]{2,1,0:T(8,128)(2,1)S(1)} %dynamic-slice_reduce_fusion), channel_id=1, replica_groups=mesh['kv'=16,'z'=16,'c'=2] {'z'}, dimensions={0} | all-to-all | bytes 131072 | tf_op jit(solution)/shard_map/all_to_all | solution.py:17
  148.0 0.8 finish.1
  (15 shorter events, 0.1 us)
Async XLA Ops:
  0.6 128.5 %copy-start = (bf16[344,256]{1,0:T(8,128)(2,1)S(1)}, bf16[344,256]{1,0:T(8,128)(2,1)}, u32[]{:S(2)}) copy-start(bf16[344,256]{1,0:T(8,128)(2,1)} %param.33) | copy-start | bytes 528388
  0.6 0.7 copy-start.10
  1.4 33.2 %copy-start.8 = (bf16[256,128]{1,0:T(8,128)(2,1)S(1)}, bf16[256,128]{1,0:T(8,128)(2,1)}, u32[]{:S(2)}) copy-start(bf16[256,128]{1,0:T(8,128)(2,1)} %wv_ref.1) | copy-start | bytes 196612
  1.4 33.2 %copy-start.3 = (bf16[4096,32]{0,1:T(8,128)(2,1)S(1)}, bf16[4096,32]{0,1:T(8,128)(2,1)}, u32[]{:S(2)}) copy-start(bf16[4096,32]{0,1:T(8,128)(2,1)} %param.25) | copy-start | bytes 786436
  29.1 5.5 %copy-start.2 = (bf16[4096,32]{0,1:T(8,128)(2,1)S(1)}, bf16[4096,32]{0,1:T(8,128)(2,1)}, u32[]{:S(2)}) copy-start(bf16[4096,32]{0,1:T(8,128)(2,1)} %param.24) | copy-start | bytes 786436
  29.1 5.5 %copy-start.6 = (bf16[256,128]{1,0:T(8,128)(2,1)S(1)}, bf16[256,128]{1,0:T(8,128)(2,1)}, u32[]{:S(2)}) copy-start(bf16[256,128]{1,0:T(8,128)(2,1)} %wq_ref.1) | copy-start | bytes 196612
  29.1 5.5 %copy-start.7 = (bf16[256,128]{1,0:T(8,128)(2,1)S(1)}, bf16[256,128]{1,0:T(8,128)(2,1)}, u32[]{:S(2)}) copy-start(bf16[256,128]{1,0:T(8,128)(2,1)} %wk_ref.1) | copy-start | bytes 196612
  34.6 0.7 copy-start.12
  35.7 17.5 %copy-start.1 = (f32[8,128,128]{2,1,0:T(8,128)S(1)}, f32[8,128,128]{2,1,0:T(8,128)}, u32[]{:S(2)}) copy-start(f32[8,128,128]{2,1,0:T(8,128)} %state_ref.1) | copy-start | bytes 1572868
  35.7 17.5 %copy-start.16 = (f32[128]{0:T(128)S(1)}, f32[128]{0:T(128)}, u32[]{:S(2)}) copy-start(f32[128]{0:T(128)} %param.28) | copy-start | bytes 1540
  53.1 0.7 copy-start.11
  53.1 0.7 copy-start.14
  53.1 0.7 copy-start.15
  55.9 10.3 %copy-start.9 = (bf16[128,256]{1,0:T(8,128)(2,1)S(1)}, bf16[128,256]{1,0:T(8,128)(2,1)}, u32[]{:S(2)}) copy-start(bf16[128,256]{1,0:T(8,128)(2,1)} %w_ref.1) | copy-start | bytes 196612
  86.0 19.2 %copy-start.5 = (bf16[256,344]{0,1:T(8,128)(2,1)S(1)}, bf16[256,344]{0,1:T(8,128)(2,1)}, u32[]{:S(2)}) copy-start(bf16[256,344]{0,1:T(8,128)(2,1)} %param.32) | copy-start | bytes 528388
  86.0 19.2 %copy-start.4 = (bf16[256,344]{0,1:T(8,128)(2,1)S(1)}, bf16[256,344]{0,1:T(8,128)(2,1)}, u32[]{:S(2)}) copy-start(bf16[256,344]{0,1:T(8,128)(2,1)} %param.31) | copy-start | bytes 528388
  105.2 0.7 copy-start.13

commit v4 on v3

--- a/solution.py
+++ b/solution.py
@@ -53,23 +53,72 @@
     return jnp.concatenate(tiles, axis=0).T
 
 
-def normed_rows(x, gain_ref):
-    return (x * gain_ref[...]).astype(BF16), jnp.sum(x * x, axis=1, keepdims=True)
+def normed_rows(x, gain):
+    return (x * gain).astype(BF16), jnp.sum(x * x, axis=1, keepdims=True)
+
+
+def prepare_kernel(
+    flat_ref,
+    lengths_ref,
+    rate_ref,
+    bias_ref,
+    gain_ref,
+    sent_ref,
+    gain_rows_ref,
+    table_ref,
+):
+    seqs, batch = table_ref.shape[1:]
+    heads = rate_ref.shape[1]
+    first = lax.axis_index("kv") * seqs
+    head = lax.axis_index("z") * lax.axis_size("c") + lax.axis_index("c")
+    flat = flat_ref[...]
+    for k in range(sent_ref.shape[0]):
+        sent_ref[k] = flat
+    gain_rows_ref[...] = jnp.broadcast_to(gain_ref[...], gain_rows_ref.shape)
+    lengths = jnp.broadcast_to(lengths_ref[...].astype(F32), (seqs, batch))
+    own = lax.broadcasted_iota(jnp.int32, (seqs, batch), 1)
+    own = own == first + lax.broadcasted_iota(jnp.int32, (seqs, batch), 0)
+    mine = lax.broadcasted_iota(jnp.int32, (seqs, heads), 1) == head
+
+    def chosen(mask, values):
+        column = jnp.sum(jnp.where(mask, values, 0.0), axis=1, keepdims=True)
+        return jnp.broadcast_to(column, (seqs, batch))
+
+    table_ref[0] = lengths
+    table_ref[1] = chosen(own, lengths)
+    table_ref[2] = chosen(mine, jnp.broadcast_to(rate_ref[...], (seqs, heads)))
+    table_ref[3] = chosen(mine, jnp.broadcast_to(bias_ref[...], (seqs, heads)))
+
+
+def prepare(seqs, *arrays):
+    flat, gain = arrays[0], arrays[4]
+    return pl.pallas_call(
+        prepare_kernel,
+        out_shape=(
+            jax.ShapeDtypeStruct((lax.axis_size("z"), *flat.shape), BF16),
+            jax.ShapeDtypeStruct((8, gain.shape[1]), F32),
+            jax.ShapeDtypeStruct((4, seqs, flat.shape[2]), F32),
+        ),
+        in_specs=full(len(arrays)),
+        out_specs=tuple(full(3)),
+        compiler_params=PARAMS,
+        name="prepare",
+    )(*arrays)
 
 
 def project_kernel(x_ref, gain_ref, wq_ref, wk_ref, wv_ref, wb_ref, wa_ref, out_ref):
-    width = gain_ref.shape[1]
-    first = pl.multiple_of(lax.axis_index("kv") * width, width)
-    head = lax.axis_index("z") * lax.axis_size("c") + lax.axis_index("c")
     kv_count, local_rows, _ = out_ref.shape
     span = x_ref.shape[2]
     seqs = local_rows // span
     heads = wb_ref.shape[0]
-    own = lax.broadcasted_iota(jnp.int32, (heads, width), 0) == head
+    head = lax.axis_index("z") * lax.axis_size("c") + lax.axis_index("c")
+    width = gain_ref.shape[1]
+    start = pl.multiple_of(lax.axis_index("kv") * width, width)
+    own_head = lax.broadcasted_iota(jnp.int32, (heads, width), 0) == head
 
     def own_row(ref):
-        tile = ref[:, pl.ds(first, width)].astype(F32)
-        return jnp.sum(jnp.where(own, tile, 0.0), axis=0, keepdims=True)
+        tile = ref[:, pl.ds(start, width)].astype(F32)
+        return jnp.sum(jnp.where(own_head, tile, 0.0), axis=0, keepdims=True)
 
     row = lax.broadcasted_iota(jnp.int32, (128, width), 0)
     small = jnp.where(row == 0, own_row(wb_ref), jnp.where(row == 1, own_row(wa_ref), 0.0))
@@ -77,7 +126,7 @@
     weights = jnp.concatenate([wq_ref[...], wk_ref[...], wv_ref[...]], axis=1)
     lane = lax.broadcasted_iota(jnp.int32, (x_ref.shape[4], 128), 1)
     for t in range(span):
-        normed, squares = normed_rows(features_of(x_ref, t), gain_ref)
+        normed, squares = normed_rows(features_of(x_ref, t), gain_ref[0:1])
         at = slice(t * seqs, (t + 1) * seqs)
         wide = dot(normed, weights, (1, 0))
         extra = jnp.where(lane == 2, squares, dot(normed, small, (1, 1)))
@@ -97,14 +146,10 @@
     )(x, gain, wq, wk, wv, wb, wa)
 
 
-def delta_kernel(
-    recv_ref, state_ref, lengths_ref, rate_ref, bias_ref, gain_ref, head_ref, new_ref
-):
+def delta_kernel(recv_ref, state_ref, table_ref, gain_ref, head_ref, new_ref):
     seq_count, size, _ = state_ref.shape
     rows = recv_ref.shape[1]
     span = rows // seq_count
-    first = lax.axis_index("kv") * seq_count
-    head = lax.axis_index("z") * lax.axis_size("c") + lax.axis_index("c")
     sums = recv_ref[0].astype(F32)
     for k in range(1, recv_ref.shape[0]):
         sums = sums + recv_ref[k].astype(F32)
@@ -116,14 +161,15 @@
     row = lax.broadcasted_iota(jnp.int32, (rows, size), 0)
     step = row // seq_count
     seq = row % seq_count
-    limit = jnp.zeros((rows, size), jnp.int32)
-    for n in range(seq_count):
-        limit = jnp.where(seq == n, lengths_ref[first + n], limit)
-    live = step < limit
+
+    def every_step(k):
+        return jnp.concatenate([table_ref[k]] * span, axis=0)
+
+    live = step.astype(F32) < every_step(1)
     beta = jnp.where(live, jax.nn.sigmoid(lanes(sums[:, 384:385]) * row_scale), 0.0)
-    pre = lanes(sums[:, 385:386]) * row_scale + bias_ref[head]
+    pre = lanes(sums[:, 385:386]) * row_scale + every_step(3)
     soft = jnp.maximum(pre, 0.0) + jnp.log1p(jnp.exp(-jnp.abs(pre)))
-    log_decay = jnp.where(live, -rate_ref[head] * soft, 0.0)
+    log_decay = jnp.where(live, -every_step(2) * soft, 0.0)
 
     def unit(block):
         v = sums[:, block * size : (block + 1) * size] * row_scale
@@ -145,21 +191,24 @@
     decays = [jnp.exp(g) for g in gaps]
     grown = jnp.exp(cumulative)
 
-    both = jnp.concatenate([keys, queries], axis=0)
-    both_high, both_low = split_high_low(both)
-    from_state = []
-    for n in range(seq_count):
-        s_high, s_low = split_high_low(state_ref[n])
-        from_state.append(
-            dot(both_high, s_high, (1, 0))
-            + dot(both_low, s_high, (1, 0))
-            + dot(both_high, s_low, (1, 0))
-        )
+    both_high, both_low = split_high_low(jnp.concatenate([keys, queries], axis=0))
+    both_rows = jnp.concatenate(
+        [
+            jnp.concatenate([both_high, both_high], axis=1),
+            jnp.concatenate([both_low, jnp.zeros_like(both_low)], axis=1),
+        ],
+        axis=0,
+    )
     key_state = jnp.zeros_like(keys)
     query_state = jnp.zeros_like(keys)
-    for n in range(seq_count):
-        key_state = jnp.where(seq == n, from_state[n][:rows], key_state)
-        query_state = jnp.where(seq == n, from_state[n][rows:], query_state)
+    for n in range(0, seq_count, 2):
+        halves = split_high_low(jnp.concatenate([state_ref[n], state_ref[n + 1]], axis=1))
+        terms = dot(both_rows, jnp.concatenate(halves, axis=0), (1, 0))
+        terms = terms[: 2 * rows] + terms[2 * rows :]
+        for k in range(2):
+            at = slice(k * size, (k + 1) * size)
+            key_state = jnp.where(seq == n + k, terms[:rows, at], key_state)
+            query_state = jnp.where(seq == n + k, terms[rows:, at], query_state)
 
     base = beta * (values - grown * key_state)
     lower, upper = [None], []
@@ -185,36 +234,41 @@
 
     k_high, k_low = split_high_low((keys * jnp.exp(tail)).T)
     k_all = jnp.concatenate([k_high, k_low, k_high], axis=1)
-    for n in range(seq_count):
-        u_high, u_low = split_high_low(jnp.where(seq == n, update, 0.0))
-        u_all = jnp.concatenate([u_high, u_high, u_low], axis=0)
-        last = rows - seq_count + n
-        new_ref[n] = state_ref[n] * grown[last : last + 1, :] + dot(k_all, u_all, (1, 0))
-
-
-def delta_step(recv, state, lengths, rate, bias, gain):
+    for n in range(0, seq_count, 2):
+        pair = [jnp.where(seq == n + k, update, 0.0) for k in range(2)]
+        u_high, u_low = split_high_low(jnp.concatenate(pair, axis=1))
+        added = dot(k_all, jnp.concatenate([u_high, u_high, u_low], axis=0), (1, 0))
+        for k in range(2):
+            last = rows - seq_count + n + k
+            kept = state_ref[n + k] * grown[last : last + 1, :]
+            new_ref[n + k] = kept + added[:, k * size : (k + 1) * size]
+
+
+def delta_step(recv, state, table, gain):
     kv_count, rows, _ = recv.shape
     size = state.shape[1]
-    smem = pl.BlockSpec(memory_space=pltpu.SMEM)
     return pl.pallas_call(
         delta_kernel,
         out_shape=(
             jax.ShapeDtypeStruct((kv_count, rows, size), BF16),
             jax.ShapeDtypeStruct(state.shape, F32),
         ),
-        in_specs=full(2) + [smem] * 3 + full(1),
+        in_specs=full(4),
         out_specs=tuple(full(2)),
         compiler_params=PARAMS,
         name="delta",
-    )(recv, state, lengths, rate, bias, gain)
-
-
-def attend_kernel(heads_ref, lengths_ref, w_ref, flat_ref, part_ref, picker_ref, base_ref):
+    )(recv, state, table, gain)
+
+
+def attend_kernel(
+    heads_ref, table_ref, w_ref, flat_ref, gain_ref, part_ref, picker_ref, base_ref, gain_rows_ref
+):
+    gain_rows_ref[...] = jnp.broadcast_to(gain_ref[...], gain_rows_ref.shape)
     slots, rows = picker_ref.shape
     span, _, batch = flat_ref.shape
     kv_count, local_rows, size = heads_ref.shape
     seqs = local_rows // span
-    lengths = jnp.broadcast_to(lengths_ref[...].astype(F32), (8, batch))
+    lengths = table_ref[0]
     above = lax.broadcasted_iota(jnp.int32, (batch, batch), 0)
     across = lax.broadcasted_iota(jnp.int32, (batch, batch), 1)
     ahead = dot(lengths.astype(BF16), (above < across).astype(BF16), (1, 0))[:1]
@@ -237,7 +291,7 @@
     base_ref[...] = dot(flat, picker, (1, 1)).astype(BF16)
 
 
-def attend(heads, lengths, w_out, flat, slots):
+def attend(heads, table, w_out, flat, gain, slots):
     span, own, batch = flat.shape
     return pl.pallas_call(
         attend_kernel,
@@ -245,18 +299,19 @@
             jax.ShapeDtypeStruct((w_out.shape[1], slots), BF16),
             jax.ShapeDtypeStruct((slots, span * batch), BF16),
             jax.ShapeDtypeStruct((own, slots), BF16),
+            jax.ShapeDtypeStruct((8, gain.shape[1]), F32),
         ),
-        in_specs=full(4),
-        out_specs=tuple(full(3)),
+        in_specs=full(5),
+        out_specs=tuple(full(4)),
         compiler_params=PARAMS,
         name="attend",
-    )(heads, lengths, w_out, flat)
+    )(heads, table, w_out, flat, gain)
 
 
 def gate_kernel(x_ref, gain_ref, wg_ref, wu_ref, out_ref):
     kv_count, local, wide = out_ref.shape
     units = wg_ref.shape[0]
-    normed, squares = normed_rows(features_of(x_ref), gain_ref)
+    normed, squares = normed_rows(features_of(x_ref), gain_ref[0:1])
 
     def put(at, value):
         width = value.shape[1]
@@ -326,25 +381,23 @@
 
     core = lax.axis_index("c").astype(jnp.uint32)
     flat, core = lax.optimization_barrier((tokens.transpose(1, 2, 0), core))
-    sent = project(
-        gather_features(flat),
+    sent, gain_in, table = prepare(
+        state.shape[0],
+        flat,
+        lengths[None, :],
+        decay_rate[None, :],
+        decay_bias[None, :],
         attn_gain[None, :],
-        w_query,
-        w_key,
-        w_value,
-        w_beta.T,
-        w_alpha.T,
-        kv_count,
     )
-    heads, updated = delta_step(
-        swap(sent, "kv"), state, lengths, decay_rate, decay_bias, out_gain[None, :]
-    )
-    attn_part, picker, base_rows = attend(
-        swap(heads, "kv"), lengths[None, :], w_out, flat, slots
+    every = lax.all_gather(swap(sent, "z"), "c", axis=0, tiled=False)
+    sums = project(every, gain_in, w_query, w_key, w_value, w_beta.T, w_alpha.T, kv_count)
+    heads, updated = delta_step(swap(sums, "kv"), state, table, out_gain[None, :])
+    attn_part, picker, base_rows, gain_mid = attend(
+        swap(heads, "kv"), table, w_out, flat, mix_gain[None, :], slots
     )
     attn_own = swap(pair_sum(attn_part, core), "z").astype(F32).sum(axis=0)
     middle = (base_rows.astype(F32) + attn_own).astype(BF16)
-    share = gate(gather_features(middle), mix_gain[None, :], w_gate.T, w_up.T, kv_count)
+    share = gate(gather_features(middle), gain_mid, w_gate.T, w_up.T, kv_count)
     share = swap(share, "kv").astype(F32).sum(axis=0)
     units = w_gate.shape[1]
     share_scale = lax.rsqrt(share[:, units : units + 1] / D + EPSILON)

time: 149 us -> 149 us (level)
    all_gather x0 -> x1, blocking collectives: none -> 5.51 us  [body(): every = lax.all_gather(swap(sent, 'z'), 'c', axis=0, tiled=False)]
    all_gather x2 -> x1, blocking collectives: 9.32 us -> 3.8 us  [gather_features(): return lax.all_gather(spread(shard, 'z'), 'c', axis=0, tiled=False)]
where the time goes in v4:
time: 149 us; the launch traced here: 148 us
  blocking collectives  140 us (94%)
  Pallas kernels  3.62 us (2%)
  local copies, waits for them, and re-layouts  3.09 us (2%)
    all_to_all x8, blocking collectives, swap(): return lax.all_to_all(tiles, axis, split_axis=0, concat_axis=0, tiled=True)  122 us
    all_gather x2, blocking collectives, pair_sum(): pair = lax.all_gather(part, 'c', axis=0, tiled=False)  8.42 us
    all_gather x1, blocking collectives, body(): every = lax.all_gather(swap(sent, 'z'), 'c', axis=0, tiled=False)  5.51 us
    all_gather x1, blocking collectives, gather_features(): return lax.all_gather(spread(shard, 'z'), 'c', axis=0, tiled=False)  3.8 us

profile of v4, /device:TPU:1, one launch (start us, length us, event | category | flops | bytes accessed | tf_op | source)
XLA Modules:
  0.0 148.3 jit_solution(9951507559911384260)
XLA Ops:
  0.6 0.0 copy-start
  0.7 0.0 copy-start.10
  0.7 0.0 copy-start.15
  0.7 0.0 copy-start.16
  0.7 0.0 copy-start.12
  0.7 0.0 copy-start.14
  0.7 0.7 copy-done.10
  1.4 0.0 copy-done.15
  1.4 0.0 copy-done.16
  1.4 0.0 copy-done.12
  1.4 0.0 copy-done.14
  1.4 0.1 prepare.1
  1.5 27.6 %all_to_all.40 = bf16[16,4,8,128]{3,2,1,0:T(8,128)(2,1)S(1)} all-to-all(bf16[16,4,8,128]{3,2,1,0:T(8,128)(2,1)S(1)} %get-tuple-element.14), channel_id=1, replica_groups=mesh['kv'=16,'z'=16,'c'=2] {'z'}, dimensions={0} | all-to-all | bytes 262144 | tf_op jit(solution)/shard_map/all_to_all | solution.py:17
  29.1 5.5 %all-gather = bf16[32,4,8,128]{3,2,1,0:T(8,128)(2,1)S(1)} all-gather(bf16[16,4,8,128]{3,2,1,0:T(8,128)(2,1)S(1)} %all_to_all.40), channel_id=2, replica_groups=mesh['kv'=16,'z'=16,'c'=2] {'c'}, dimensions={0}, use_global_device_ids=true | all-gather | bytes 393216 | tf_op jit(solution)/shard_map/all_gather | solution.py:392
  34.7 0.0 copy-done.3
  34.7 0.0 copy-done.2
  34.7 0.0 copy-done.6
  34.7 0.0 copy-done.7
  34.7 0.0 copy-start.8
  34.7 0.8 copy-done.8
  35.5 0.4 project.1
  35.9 0.0 copy-start.1
  36.0 17.4 %all_to_all.41.recv_ref = bf16[16,32,512]{2,1,0:T(8,128)(2,1)S(1)} all-to-all(bf16[16,32,512]{2,1,0:T(8,128)(2,1)S(1)} %project.1), channel_id=1, replica_groups=mesh['kv'=16,'z'=16,'c'=2] {'kv'}, dimensions={0} | all-to-all | bytes 1048576 | tf_op jit(solution)/shard_map/all_to_all | solution.py:17
  53.4 0.0 copy-done.1
  53.4 0.7 copy-done.13
  54.0 1.4 delta.1
  55.5 10.3 %all_to_all.42.heads_ref = bf16[16,32,128]{2,1,0:T(8,128)(2,1)S(1)} all-to-all(bf16[16,32,128]{2,1,0:T(8,128)(2,1)S(1)} %get-tuple-element.17), channel_id=1, replica_groups=mesh['kv'=16,'z'=16,'c'=2] {'kv'}, dimensions={0} | all-to-all | bytes 262144 | tf_op jit(solution)/shard_map/all_to_all | solution.py:17
  65.7 0.0 copy-done.9
  65.7 0.7 copy-done.11
  66.4 0.6 attend.1
  67.0 4.2 %all-gather.1 = bf16[512,256]{1,0:T(8,128)(2,1)S(1)} all-gather(bf16[256,256]{1,0:T(8,128)(2,1)S(1)} %get-tuple-element.19), channel_id=3, replica_groups=mesh['kv'=16,'z'=16,'c'=2] {'c'}, dimensions={0}, use_global_device_ids=true | all-gather | bytes 393216 | tf_op jit(solution)/shard_map/all_gather | solution.py:31
  71.2 15.0 %all_to_all.43 = bf16[16,8,256]{2,1,0:T(8,128)(2,1)S(1)} all-to-all(bf16[16,8,256]{2,1,0:T(8,128)(2,1)S(1)} %dynamic-slice_reduce_fusion.1), channel_id=1, replica_groups=mesh['kv'=16,'z'=16,'c'=2] {'z'}, dimensions={0} | all-to-all | bytes 131072 | tf_op jit(solution)/shard_map/all_to_all | solution.py:17
  86.2 0.0 copy-start.5
  86.2 0.0 copy-start.4
  86.2 15.4 %all_to_all.44 = bf16[16,8,256]{2,1,0:T(8,128)(2,1)S(1)} all-to-all(bf16[16,8,256]{2,1,0:T(8,128)(2,1)S(1)} %broadcast_in_dim.36), channel_id=1, replica_groups=mesh['kv'=16,'z'=16,'c'=2] {'z'}, dimensions={0} | all-to-all | bytes 131072 | tf_op jit(solution)/shard_map/all_to_all | solution.py:17
  101.6 3.8 %all-gather.2 = bf16[32,8,256]{2,1,0:T(8,128)(2,1)S(1)} all-gather(bf16[16,8,256]{2,1,0:T(8,128)(2,1)S(1)} %all_to_all.44), channel_id=4, replica_groups=mesh['kv'=16,'z'=16,'c'=2] {'c'}, dimensions={0}, use_global_device_ids=true | all-gather | bytes 196608 | tf_op jit(solution)/shard_map/all_gather | solution.py:25
  105.4 0.0 copy-done.5
  105.4 0.4 gate.1
  105.8 12.3 %all_to_all.45 = bf16[16,16,768]{2,1,0:T(8,128)(2,1)S(1)} all-to-all(bf16[16,16,768]{2,1,0:T(8,128)(2,1)S(1)} %gate.1), channel_id=1, replica_groups=mesh['kv'=16,'z'=16,'c'=2] {'kv'}, dimensions={0} | all-to-all | bytes 786432 | tf_op jit(solution)/shard_map/all_to_all | solution.py:17
  118.1 0.1 convert_reduce_fusion
  118.2 0.2 fusion.5
  118.4 0.1 fusion.2
  118.5 10.1 %all_to_all.46 = bf16[16,16,344]{2,1,0:T(8,128)(2,1)S(1)} all-to-all(bf16[16,16,344]{2,1,0:T(8,128)(2,1)S(1)} %broadcast_in_dim.37), channel_id=1, replica_groups=mesh['kv'=16,'z'=16,'c'=2] {'kv'}, dimensions={0} | all-to-all | bytes 352256 | tf_op jit(solution)/shard_map/all_to_all | solution.py:17
  128.6 0.2 fusion
  128.9 4.2 %all-gather.3 = bf16[512,256]{0,1:T(8,128)(2,1)S(1)} all-gather(bf16[256,256]{0,1:T(8,128)(2,1)S(1)} %fusion), channel_id=5, replica_groups=mesh['kv'=16,'z'=16,'c'=2] {'c'}, dimensions={0}, use_global_device_ids=true | all-gather | bytes 393216 | tf_op jit(solution)/shard_map/all_gather | solution.py:31
  133.1 0.1 copy.24
  133.2 14.3 %all_to_all.47.recv_ref = bf16[16,8,256]{2,1,0:T(8,128)(2,1)S(1)} all-to-all(bf16[16,8,256]{2,1,0:T(8,128)(2,1)S(1)} %dynamic-slice_reduce_fusion), channel_id=1, replica_groups=mesh['kv'=16,'z'=16,'c'=2] {'z'}, dimensions={0} | all-to-all | bytes 131072 | tf_op jit(solution)/shard_map/all_to_all | solution.py:17
  147.5 0.8 finish.1
  (15 shorter events, 0.1 us)
Async XLA Ops:
  0.6 128.0 %copy-start = (bf16[344,256]{1,0:T(8,128)(2,1)S(1)}, bf16[344,256]{1,0:T(8,128)(2,1)}, u32[]{:S(2)}) copy-start(bf16[344,256]{1,0:T(8,128)(2,1)} %param.33) | copy-start | bytes 528388
  0.7 0.7 copy-start.10
  0.7 0.7 copy-start.15
  0.7 0.7 copy-start.16
  0.7 0.7 copy-start.12
  0.7 0.7 copy-start.14
  1.5 33.2 %copy-start.3 = (bf16[4096,32]{0,1:T(8,128)(2,1)S(1)}, bf16[4096,32]{0,1:T(8,128)(2,1)}, u32[]{:S(2)}) copy-start(bf16[4096,32]{0,1:T(8,128)(2,1)} %param.25) | copy-start | bytes 786436
  29.1 5.5 %copy-start.2 = (bf16[4096,32]{0,1:T(8,128)(2,1)S(1)}, bf16[4096,32]{0,1:T(8,128)(2,1)}, u32[]{:S(2)}) copy-start(bf16[4096,32]{0,1:T(8,128)(2,1)} %param.24) | copy-start | bytes 786436
  29.1 5.5 %copy-start.6 = (bf16[256,128]{1,0:T(8,128)(2,1)S(1)}, bf16[256,128]{1,0:T(8,128)(2,1)}, u32[]{:S(2)}) copy-start(bf16[256,128]{1,0:T(8,128)(2,1)} %wq_ref.1) | copy-start | bytes 196612
  29.1 5.5 %copy-start.7 = (bf16[256,128]{1,0:T(8,128)(2,1)S(1)}, bf16[256,128]{1,0:T(8,128)(2,1)}, u32[]{:S(2)}) copy-start(bf16[256,128]{1,0:T(8,128)(2,1)} %wk_ref.1) | copy-start | bytes 196612
  34.7 0.8 copy-start.8
  35.9 17.4 %copy-start.1 = (f32[8,128,128]{2,1,0:T(8,128)S(1)}, f32[8,128,128]{2,1,0:T(8,128)}, u32[]{:S(2)}) copy-start(f32[8,128,128]{2,1,0:T(8,128)} %state_ref.1) | copy-start | bytes 1572868
  53.4 0.7 copy-start.13
  55.5 10.3 %copy-start.9 = (bf16[128,256]{1,0:T(8,128)(2,1)S(1)}, bf16[128,256]{1,0:T(8,128)(2,1)}, u32[]{:S(2)}) copy-start(bf16[128,256]{1,0:T(8,128)(2,1)} %w_ref.1) | copy-start | bytes 196612
  65.7 0.7 copy-start.11
  86.2 19.2 %copy-start.5 = (bf16[256,344]{0,1:T(8,128)(2,1)S(1)}, bf16[256,344]{0,1:T(8,128)(2,1)}, u32[]{:S(2)}) copy-start(bf16[256,344]{0,1:T(8,128)(2,1)} %param.32) | copy-start | bytes 528388
  86.2 19.2 %copy-start.4 = (bf16[256,344]{0,1:T(8,128)(2,1)S(1)}, bf16[256,344]{0,1:T(8,128)(2,1)}, u32[]{:S(2)}) copy-start(bf16[256,344]{0,1:T(8,128)(2,1)} %param.31) | copy-start | bytes 528388

commit v5 on v4

--- a/solution.py
+++ b/solution.py
@@ -10,6 +10,8 @@
 EPSILON = 1e-06
 F32 = jnp.float32
 BF16 = jnp.bfloat16
+Z = ("zh", "zl")
+NEAR = ("zl", "c")
 PARAMS = pltpu.CompilerParams(vmem_limit_bytes=12 * 1024 * 1024)
 
 
@@ -21,13 +23,9 @@
     return swap(jnp.broadcast_to(shard[None], (lax.axis_size(axis), *shard.shape)), axis)
 
 
-def gather_features(shard):
-    return lax.all_gather(spread(shard, "z"), "c", axis=0, tiled=False)
-
-
 def pair_sum(part, core):
     feats, rows = part.shape
-    z_count, c_count = lax.axis_size("z"), lax.axis_size("c")
+    z_count, c_count = lax.axis_size(Z), lax.axis_size("c")
     pair = lax.all_gather(part, "c", axis=0, tiled=False)
     pair = pair.reshape(c_count, z_count, c_count, -1, rows)
     mine = lax.dynamic_index_in_dim(pair, core, 2, keepdims=False)
@@ -62,19 +60,22 @@
     lengths_ref,
     rate_ref,
     bias_ref,
-    gain_ref,
+    gain_in_ref,
+    gain_mid_ref,
+    gain_out_ref,
     sent_ref,
-    gain_rows_ref,
+    gains_ref,
     table_ref,
 ):
     seqs, batch = table_ref.shape[1:]
     heads = rate_ref.shape[1]
     first = lax.axis_index("kv") * seqs
-    head = lax.axis_index("z") * lax.axis_size("c") + lax.axis_index("c")
+    head = lax.axis_index(Z) * lax.axis_size("c") + lax.axis_index("c")
     flat = flat_ref[...]
     for k in range(sent_ref.shape[0]):
         sent_ref[k] = flat
-    gain_rows_ref[...] = jnp.broadcast_to(gain_ref[...], gain_rows_ref.shape)
+    gains_ref[0:1] = gain_in_ref[...]
+    gains_ref[1:2] = gain_mid_ref[...]
     lengths = jnp.broadcast_to(lengths_ref[...].astype(F32), (seqs, batch))
     own = lax.broadcasted_iota(jnp.int32, (seqs, batch), 1)
     own = own == first + lax.broadcasted_iota(jnp.int32, (seqs, batch), 0)
@@ -88,6 +89,7 @@
     table_ref[1] = chosen(own, lengths)
     table_ref[2] = chosen(mine, jnp.broadcast_to(rate_ref[...], (seqs, heads)))
     table_ref[3] = chosen(mine, jnp.broadcast_to(bias_ref[...], (seqs, heads)))
+    table_ref[4] = jnp.broadcast_to(gain_out_ref[...], (seqs, batch))
 
 
 def prepare(seqs, *arrays):
@@ -95,9 +97,9 @@
     return pl.pallas_call(
         prepare_kernel,
         out_shape=(
-            jax.ShapeDtypeStruct((lax.axis_size("z"), *flat.shape), BF16),
+            jax.ShapeDtypeStruct((lax.axis_size(Z), *flat.shape), BF16),
             jax.ShapeDtypeStruct((8, gain.shape[1]), F32),
-            jax.ShapeDtypeStruct((4, seqs, flat.shape[2]), F32),
+            jax.ShapeDtypeStruct((5, seqs, flat.shape[2]), F32),
         ),
         in_specs=full(len(arrays)),
         out_specs=tuple(full(3)),
@@ -111,7 +113,7 @@
     span = x_ref.shape[2]
     seqs = local_rows // span
     heads = wb_ref.shape[0]
-    head = lax.axis_index("z") * lax.axis_size("c") + lax.axis_index("c")
+    head = lax.axis_index(Z) * lax.axis_size("c") + lax.axis_index("c")
     width = gain_ref.shape[1]
     start = pl.multiple_of(lax.axis_index("kv") * width, width)
     own_head = lax.broadcasted_iota(jnp.int32, (heads, width), 0) == head
@@ -146,7 +148,7 @@
     )(x, gain, wq, wk, wv, wb, wa)
 
 
-def delta_kernel(recv_ref, state_ref, table_ref, gain_ref, head_ref, new_ref):
+def delta_kernel(recv_ref, state_ref, table_ref, head_ref, new_ref):
     seq_count, size, _ = state_ref.shape
     rows = recv_ref.shape[1]
     span = rows // seq_count
@@ -228,7 +230,7 @@
     for d in range(1, span):
         attended = attended + upper[d] * back(update, d)
     out = attended * lax.rsqrt(jnp.mean(attended * attended, axis=1, keepdims=True) + EPSILON)
-    out = (out * gain_ref[...]).astype(BF16)
+    out = (out * every_step(4)).astype(BF16)
     for k in range(head_ref.shape[0]):
         head_ref[k] = out
 
@@ -244,7 +246,7 @@
             new_ref[n + k] = kept + added[:, k * size : (k + 1) * size]
 
 
-def delta_step(recv, state, table, gain):
+def delta_step(recv, state, table):
     kv_count, rows, _ = recv.shape
     size = state.shape[1]
     return pl.pallas_call(
@@ -253,19 +255,16 @@
             jax.ShapeDtypeStruct((kv_count, rows, size), BF16),
             jax.ShapeDtypeStruct(state.shape, F32),
         ),
-        in_specs=full(4),
+        in_specs=full(3),
         out_specs=tuple(full(2)),
         compiler_params=PARAMS,
         name="delta",
-    )(recv, state, table, gain)
-
-
-def attend_kernel(
-    heads_ref, table_ref, w_ref, flat_ref, gain_ref, part_ref, picker_ref, base_ref, gain_rows_ref
-):
-    gain_rows_ref[...] = jnp.broadcast_to(gain_ref[...], gain_rows_ref.shape)
+    )(recv, state, table)
+
+
+def attend_kernel(heads_ref, table_ref, w_ref, every_ref, part_ref, picker_ref, base_ref):
     slots, rows = picker_ref.shape
-    span, _, batch = flat_ref.shape
+    c_count, _, span, own, batch = every_ref.shape
     kv_count, local_rows, size = heads_ref.shape
     seqs = local_rows // span
     lengths = table_ref[0]
@@ -287,31 +286,46 @@
     ).astype(BF16)
     packed = dot(picker, heads, (1, 0)).astype(BF16)
     part_ref[...] = dot(packed, w_ref[...], (1, 0)).T.astype(BF16)
-    flat = jnp.concatenate([flat_ref[t] for t in range(span)], axis=1)
-    base_ref[...] = dot(flat, picker, (1, 1)).astype(BF16)
-
-
-def attend(heads, table, w_out, flat, gain, slots):
-    span, own, batch = flat.shape
+    near = lax.axis_index("zl") * c_count + lax.axis_index("c")
+    chips = base_ref.shape[0] // (own * c_count)
+    tiles = [
+        jnp.concatenate([every_ref[c, near * chips + k, t] for t in range(span)], axis=1)
+        for k in range(chips)
+        for c in range(c_count)
+    ]
+    tiles = jnp.concatenate([tile.astype(F32) for tile in tiles], axis=0).astype(BF16)
+    base_ref[...] = dot(tiles, picker, (1, 1)).astype(BF16)
+
+
+def attend(heads, table, w_out, every, slots, near_feats):
+    _, _, span, _, batch = every.shape
     return pl.pallas_call(
         attend_kernel,
         out_shape=(
             jax.ShapeDtypeStruct((w_out.shape[1], slots), BF16),
             jax.ShapeDtypeStruct((slots, span * batch), BF16),
-            jax.ShapeDtypeStruct((own, slots), BF16),
-            jax.ShapeDtypeStruct((8, gain.shape[1]), F32),
+            jax.ShapeDtypeStruct((near_feats, slots), BF16),
         ),
-        in_specs=full(5),
-        out_specs=tuple(full(4)),
+        in_specs=full(4),
+        out_specs=tuple(full(3)),
         compiler_params=PARAMS,
         name="attend",
-    )(heads, table, w_out, flat, gain)
-
-
-def gate_kernel(x_ref, gain_ref, wg_ref, wu_ref, out_ref):
+    )(heads, table, w_out, every)
+
+
+def gate_kernel(x_ref, gain_ref, wg_ref, wu_ref, out_ref, own_ref):
     kv_count, local, wide = out_ref.shape
     units = wg_ref.shape[0]
-    normed, squares = normed_rows(features_of(x_ref), gain_ref[0:1])
+    near_count, feats, slots = x_ref.shape
+    x = x_ref[...].astype(F32).reshape(near_count * feats, slots)
+    own = own_ref.shape[0]
+    first = ((lax.axis_index(Z)) * lax.axis_size("c") + lax.axis_index("c")) * own
+    chunk = x_ref[first // feats].astype(F32)
+    mine = chunk[:own]
+    for k in range(1, feats // own):
+        mine = jnp.where(first % feats == k * own, chunk[k * own : (k + 1) * own], mine)
+    own_ref[...] = mine.astype(BF16)
+    normed, squares = normed_rows(x.T, gain_ref[1:2])
 
     def put(at, value):
         width = value.shape[1]
@@ -320,16 +334,19 @@
     half = wide // 2
     put(0, dot(normed, wg_ref[...], (1, 1)))
     put(half, dot(normed, wu_ref[...], (1, 1)))
-    put(units, jnp.broadcast_to(squares, (x_ref.shape[3], half - units)))
-
-
-def gate(x, gain, w_gate, w_up, kv_count):
+    put(units, jnp.broadcast_to(squares, (slots, half - units)))
+
+
+def gate(x, gain, w_gate, w_up, kv_count, own):
     rows = x.shape[-1]
     return pl.pallas_call(
         gate_kernel,
-        out_shape=jax.ShapeDtypeStruct((kv_count, rows // kv_count, 768), BF16),
+        out_shape=(
+            jax.ShapeDtypeStruct((kv_count, rows // kv_count, 768), BF16),
+            jax.ShapeDtypeStruct((own, rows), BF16),
+        ),
         in_specs=full(4),
-        out_specs=pl.BlockSpec(memory_space=pltpu.VMEM),
+        out_specs=tuple(full(2)),
         compiler_params=PARAMS,
         name="gate",
     )(x, gain, w_gate, w_up)
@@ -381,23 +398,27 @@
 
     core = lax.axis_index("c").astype(jnp.uint32)
     flat, core = lax.optimization_barrier((tokens.transpose(1, 2, 0), core))
-    sent, gain_in, table = prepare(
+    sent, gains, table = prepare(
         state.shape[0],
         flat,
         lengths[None, :],
         decay_rate[None, :],
         decay_bias[None, :],
         attn_gain[None, :],
+        mix_gain[None, :],
+        out_gain[None, :],
     )
-    every = lax.all_gather(swap(sent, "z"), "c", axis=0, tiled=False)
-    sums = project(every, gain_in, w_query, w_key, w_value, w_beta.T, w_alpha.T, kv_count)
-    heads, updated = delta_step(swap(sums, "kv"), state, table, out_gain[None, :])
-    attn_part, picker, base_rows, gain_mid = attend(
-        swap(heads, "kv"), table, w_out, flat, mix_gain[None, :], slots
+    every = lax.all_gather(swap(sent, Z), "c", axis=0, tiled=False)
+    sums = project(every, gains, w_query, w_key, w_value, w_beta.T, w_alpha.T, kv_count)
+    heads, updated = delta_step(swap(sums, "kv"), state, table)
+    near_count = lax.axis_size(NEAR)
+    attn_part, picker, base_rows = attend(
+        swap(heads, "kv"), table, w_out, every, slots, w_out.shape[1] // near_count
     )
-    attn_own = swap(pair_sum(attn_part, core), "z").astype(F32).sum(axis=0)
-    middle = (base_rows.astype(F32) + attn_own).astype(BF16)
-    share = gate(gather_features(middle), gain_mid, w_gate.T, w_up.T, kv_count)
+    near_sum = swap(attn_part.reshape(near_count, -1, slots), NEAR).astype(F32).sum(axis=0)
+    far_terms = spread(near_sum.astype(BF16), "zh").astype(F32).sum(axis=0)
+    middle_rows = spread((base_rows.astype(F32) + far_terms).astype(BF16), NEAR)
+    share, middle = gate(middle_rows, gains, w_gate.T, w_up.T, kv_count, flat.shape[1])
     share = swap(share, "kv").astype(F32).sum(axis=0)
     units = w_gate.shape[1]
     share_scale = lax.rsqrt(share[:, units : units + 1] / D + EPSILON)
@@ -407,18 +428,18 @@
     ).astype(BF16)
     hidden_every = spread(hidden, "kv").reshape(slots, units)
     down_part = dot(w_down, hidden_every, (0, 1)).astype(BF16)
-    mixed = finish(swap(pair_sum(down_part, core), "z"), middle, picker, flat.shape[0])
+    mixed = finish(swap(pair_sum(down_part, core), Z), middle, picker, flat.shape[0])
     return (mixed.transpose(2, 0, 1), updated)
 
 
 def solution(mesh):
-    split = Mesh(mesh.devices.reshape(mesh.shape["kv"], -1, 2), ("kv", "z", "c"))
-    tp = ("z", "c")
+    tp = ("zh", "zl", "c")
+    split = Mesh(mesh.devices.reshape(mesh.shape["kv"], -1, 4, 2), ("kv", *tp))
     return jax.shard_map(
         body,
         mesh=split,
         in_specs=(
-            P(None, None, ("kv", "z", "c")),
+            P(None, None, ("kv", *tp)),
             P(),
             P("kv", None, tp),
             P("kv"),
@@ -436,6 +457,6 @@
             P("kv", tp),
             P(tp, "kv"),
         ),
-        out_specs=(P(None, None, ("kv", "z", "c")), P("kv", None, tp)),
+        out_specs=(P(None, None, ("kv", *tp)), P("kv", None, tp)),
         check_vma=False,
     )

time: 149 us -> 148 us (level)
    all_to_all x8 -> x9, blocking collectives: 122 us -> 130 us  [swap(): return lax.all_to_all(tiles, axis, split_axis=0, concat_axis=0, tiled=True)]
    all_gather x2 -> x1, blocking collectives: 9.32 us -> 5.51 us  [body(): every = lax.all_gather(swap(sent, Z), 'c', axis=0, tiled=False)]
    all_gather x2 -> x1, blocking collectives: 8.42 us -> 4.9 us  [pair_sum(): pair = lax.all_gather(part, 'c', axis=0, tiled=False)]
where the time goes in v5:
time: 148 us
  blocking collectives  141 us (95%)
  Pallas kernels  3.62 us (2%)
  local copies, waits for them, and re-layouts  1.79 us (1%)
    all_to_all x9, blocking collectives, swap(): return lax.all_to_all(tiles, axis, split_axis=0, concat_axis=0, tiled=True)  130 us
    all_gather x1, blocking collectives, body(): every = lax.all_gather(swap(sent, Z), 'c', axis=0, tiled=False)  5.51 us
    all_gather x1, blocking collectives, pair_sum(): pair = lax.all_gather(part, 'c', axis=0, tiled=False)  4.9 us

profile of v5, /device:TPU:1, one launch (start us, length us, event | category | flops | bytes accessed | tf_op | source)
XLA Modules:
  0.0 147.5 jit_solution(7170748756671766474)
XLA Ops:
  0.6 0.0 copy-start
  0.7 0.0 copy-start.10
  0.7 0.0 copy-start.16
  0.7 0.0 copy-start.12
  0.7 0.0 copy-start.14
  0.7 0.0 copy-start.15
  0.7 0.0 copy-start.11
  0.7 0.0 copy-start.13
  0.7 0.7 copy-done.10
  1.4 0.0 copy-done.16
  1.4 0.0 copy-done.12
  1.4 0.0 copy-done.14
  1.4 0.0 copy-done.15
  1.4 0.0 copy-done.11
  1.4 0.0 copy-done.13
  1.5 0.1 prepare.1
  1.5 27.6 %all_to_all.45 = bf16[16,4,8,128]{3,2,1,0:T(8,128)(2,1)S(1)} all-to-all(bf16[16,4,8,128]{3,2,1,0:T(8,128)(2,1)S(1)} %get-tuple-element.15), channel_id=1, replica_groups=mesh['kv'=16,'zh'=4,'zl'=4,'c'=2] {'zh','zl'}, dimensions={0} | all-to-all | bytes 262144 | tf_op jit(solution)/shard_map/all_to_all | solution.py:19
  29.2 5.5 %all-gather = bf16[32,4,8,128]{3,2,1,0:T(8,128)(2,1)S(1)} all-gather(bf16[16,4,8,128]{3,2,1,0:T(8,128)(2,1)S(1)} %all_to_all.45), channel_id=2, replica_groups=mesh['kv'=16,'zh'=4,'zl'=4,'c'=2] {'c'}, dimensions={0}, use_global_device_ids=true | all-gather | bytes 393216 | tf_op jit(solution)/shard_map/all_gather | solution.py:411
  34.7 0.0 copy-done.3
  34.7 0.0 copy-done.2
  34.7 0.0 copy-done.6
  34.7 0.0 copy-done.7
  34.7 0.0 copy-start.8
  34.7 0.8 copy-done.8
  35.6 0.4 project.1
  36.0 0.0 copy-start.1
  36.0 17.4 %all_to_all.46.recv_ref = bf16[16,32,512]{2,1,0:T(8,128)(2,1)S(1)} all-to-all(bf16[16,32,512]{2,1,0:T(8,128)(2,1)S(1)} %project.1), channel_id=1, replica_groups=mesh['kv'=16,'zh'=4,'zl'=4,'c'=2] {'kv'}, dimensions={0} | all-to-all | bytes 1048576 | tf_op jit(solution)/shard_map/all_to_all | solution.py:19
  53.4 0.0 copy-done.1
  53.4 1.4 delta.1
  54.8 10.3 %all_to_all.47.heads_ref = bf16[16,32,128]{2,1,0:T(8,128)(2,1)S(1)} all-to-all(bf16[16,32,128]{2,1,0:T(8,128)(2,1)S(1)} %get-tuple-element.18), channel_id=1, replica_groups=mesh['kv'=16,'zh'=4,'zl'=4,'c'=2] {'kv'}, dimensions={0} | all-to-all | bytes 262144 | tf_op jit(solution)/shard_map/all_to_all | solution.py:19
  65.1 0.6 attend.1
  65.7 11.4 %all_to_all.48 = bf16[8,32,256]{2,1,0:T(8,128)(2,1)S(1)} all-to-all(bf16[8,32,256]{2,1,0:T(8,128)(2,1)S(1)} %bitcast.26), channel_id=1, replica_groups=mesh['kv'=16,'zh'=4,'zl'=4,'c'=2] {'zl','c'}, dimensions={0} | all-to-all | bytes 262144 | tf_op jit(solution)/shard_map/all_to_all | solution.py:19
  77.1 16.7 %all_to_all.49 = bf16[4,32,256]{2,1,0:T(8,128)(2,1)S(1)} all-to-all(bf16[4,32,256]{2,1,0:T(8,128)(2,1)S(1)} %broadcast_in_dim.42), channel_id=1, replica_groups=mesh['kv'=16,'zh'=4,'zl'=4,'c'=2] {'zh'}, dimensions={0} | all-to-all | bytes 131072 | tf_op jit(solution)/shard_map/all_to_all | solution.py:19
  93.8 0.0 copy-start.4
  93.8 0.0 copy-start.5
  93.9 10.7 %all_to_all.50.x_ref = bf16[8,32,256]{2,1,0:T(8,128)(2,1)S(1)} all-to-all(bf16[8,32,256]{2,1,0:T(8,128)(2,1)S(1)} %broadcast_in_dim.43), channel_id=1, replica_groups=mesh['kv'=16,'zh'=4,'zl'=4,'c'=2] {'zl','c'}, dimensions={0} | all-to-all | bytes 262144 | tf_op jit(solution)/shard_map/all_to_all | solution.py:19
  104.6 0.0 copy-done.5
  104.6 0.4 gate.1
  105.0 11.7 %all_to_all.51 = bf16[16,16,768]{2,1,0:T(8,128)(2,1)S(1)} all-to-all(bf16[16,16,768]{2,1,0:T(8,128)(2,1)S(1)} %get-tuple-element.21), channel_id=1, replica_groups=mesh['kv'=16,'zh'=4,'zl'=4,'c'=2] {'kv'}, dimensions={0} | all-to-all | bytes 786432 | tf_op jit(solution)/shard_map/all_to_all | solution.py:19
  116.7 0.1 convert_reduce_fusion
  116.8 0.2 fusion.5
  117.0 0.1 fusion.2
  117.1 10.1 %all_to_all.52 = bf16[16,16,344]{2,1,0:T(8,128)(2,1)S(1)} all-to-all(bf16[16,16,344]{2,1,0:T(8,128)(2,1)S(1)} %broadcast_in_dim.44), channel_id=1, replica_groups=mesh['kv'=16,'zh'=4,'zl'=4,'c'=2] {'kv'}, dimensions={0} | all-to-all | bytes 352256 | tf_op jit(solution)/shard_map/all_to_all | solution.py:19
  127.2 0.2 fusion
  127.4 4.9 %all-gather.1 = bf16[512,256]{0,1:T(8,128)(2,1)S(1)} all-gather(bf16[256,256]{0,1:T(8,128)(2,1)S(1)} %fusion), channel_id=3, replica_groups=mesh['kv'=16,'zh'=4,'zl'=4,'c'=2] {'c'}, dimensions={0}, use_global_device_ids=true | all-gather | bytes 393216 | tf_op jit(solution)/shard_map/all_gather | solution.py:29
  132.3 0.1 copy.24
  132.5 14.3 %all_to_all.53.recv_ref = bf16[16,8,256]{2,1,0:T(8,128)(2,1)S(1)} all-to-all(bf16[16,8,256]{2,1,0:T(8,128)(2,1)S(1)} %dynamic-slice_reduce_fusion), channel_id=1, replica_groups=mesh['kv'=16,'zh'=4,'zl'=4,'c'=2] {'zh','zl'}, dimensions={0} | all-to-all | bytes 131072 | tf_op jit(solution)/shard_map/all_to_all | solution.py:19
  146.8 0.8 finish.1
  (15 shorter events, 0.1 us)
Async XLA Ops:
  0.6 126.5 %copy-start = (bf16[344,256]{1,0:T(8,128)(2,1)S(1)}, bf16[344,256]{1,0:T(8,128)(2,1)}, u32[]{:S(2)}) copy-start(bf16[344,256]{1,0:T(8,128)(2,1)} %param.33) | copy-start | bytes 528388
  0.7 0.7 copy-start.10
  0.7 0.7 copy-start.16
  0.7 0.7 copy-start.12
  0.7 0.7 copy-start.14
  0.7 0.7 copy-start.15
  0.7 0.7 copy-start.11
  0.7 0.7 copy-start.13
  1.5 33.2 %copy-start.3 = (bf16[4096,32]{0,1:T(8,128)(2,1)S(1)}, bf16[4096,32]{0,1:T(8,128)(2,1)}, u32[]{:S(2)}) copy-start(bf16[4096,32]{0,1:T(8,128)(2,1)} %param.25) | copy-start | bytes 786436
  29.2 5.5 %copy-start.2 = (bf16[4096,32]{0,1:T(8,128)(2,1)S(1)}, bf16[4096,32]{0,1:T(8,128)(2,1)}, u32[]{:S(2)}) copy-start(bf16[4096,32]{0,1:T(8,128)(2,1)} %param.24) | copy-start | bytes 786436
  29.2 5.5 %copy-start.6 = (bf16[256,128]{1,0:T(8,128)(2,1)S(1)}, bf16[256,128]{1,0:T(8,128)(2,1)}, u32[]{:S(2)}) copy-start(bf16[256,128]{1,0:T(8,128)(2,1)} %wq_ref.1) | copy-start | bytes 196612
  29.2 5.5 %copy-start.7 = (bf16[256,128]{1,0:T(8,128)(2,1)S(1)}, bf16[256,128]{1,0:T(8,128)(2,1)}, u32[]{:S(2)}) copy-start(bf16[256,128]{1,0:T(8,128)(2,1)} %wk_ref.1) | copy-start | bytes 196612
  34.7 0.8 copy-start.8
  36.0 17.4 %copy-start.1 = (f32[8,128,128]{2,1,0:T(8,128)S(1)}, f32[8,128,128]{2,1,0:T(8,128)}, u32[]{:S(2)}) copy-start(f32[8,128,128]{2,1,0:T(8,128)} %state_ref.1) | copy-start | bytes 1572868
  54.8 10.3 %copy-start.9 = (bf16[128,256]{1,0:T(8,128)(2,1)S(1)}, bf16[128,256]{1,0:T(8,128)(2,1)}, u32[]{:S(2)}) copy-start(bf16[128,256]{1,0:T(8,128)(2,1)} %w_ref.1) | copy-start | bytes 196612
  93.8 10.8 %copy-start.4 = (bf16[256,344]{0,1:T(8,128)(2,1)S(1)}, bf16[256,344]{0,1:T(8,128)(2,1)}, u32[]{:S(2)}) copy-start(bf16[256,344]{0,1:T(8,128)(2,1)} %param.31) | copy-start | bytes 528388
  93.8 10.8 %copy-start.5 = (bf16[256,344]{0,1:T(8,128)(2,1)S(1)}, bf16[256,344]{0,1:T(8,128)(2,1)}, u32[]{:S(2)}) copy-start(bf16[256,344]{0,1:T(8,128)(2,1)} %param.32) | copy-start | bytes 528388

commit v6 on v5

--- a/solution.py
+++ b/solution.py
@@ -10,8 +10,8 @@
 EPSILON = 1e-06
 F32 = jnp.float32
 BF16 = jnp.bfloat16
-Z = ("zh", "zl")
-NEAR = ("zl", "c")
+Z = "z"
+COST = pl.CostEstimate(flops=1 << 28, bytes_accessed=1 << 21, transcendentals=0)
 PARAMS = pltpu.CompilerParams(vmem_limit_bytes=12 * 1024 * 1024)
 
 
@@ -104,6 +104,7 @@
         in_specs=full(len(arrays)),
         out_specs=tuple(full(3)),
         compiler_params=PARAMS,
+        cost_estimate=COST,
         name="prepare",
     )(*arrays)
 
@@ -262,9 +263,9 @@
     )(recv, state, table)
 
 
-def attend_kernel(heads_ref, table_ref, w_ref, every_ref, part_ref, picker_ref, base_ref):
+def attend_kernel(heads_ref, table_ref, w_ref, flat_ref, part_ref, picker_ref, base_ref):
     slots, rows = picker_ref.shape
-    c_count, _, span, own, batch = every_ref.shape
+    span, _, batch = flat_ref.shape
     kv_count, local_rows, size = heads_ref.shape
     seqs = local_rows // span
     lengths = table_ref[0]
@@ -286,46 +287,30 @@
     ).astype(BF16)
     packed = dot(picker, heads, (1, 0)).astype(BF16)
     part_ref[...] = dot(packed, w_ref[...], (1, 0)).T.astype(BF16)
-    near = lax.axis_index("zl") * c_count + lax.axis_index("c")
-    chips = base_ref.shape[0] // (own * c_count)
-    tiles = [
-        jnp.concatenate([every_ref[c, near * chips + k, t] for t in range(span)], axis=1)
-        for k in range(chips)
-        for c in range(c_count)
-    ]
-    tiles = jnp.concatenate([tile.astype(F32) for tile in tiles], axis=0).astype(BF16)
-    base_ref[...] = dot(tiles, picker, (1, 1)).astype(BF16)
-
-
-def attend(heads, table, w_out, every, slots, near_feats):
-    _, _, span, _, batch = every.shape
+    flat = jnp.concatenate([flat_ref[t] for t in range(span)], axis=1)
+    base_ref[...] = dot(flat, picker, (1, 1)).astype(BF16)
+
+
+def attend(heads, table, w_out, flat, slots):
+    span, own, batch = flat.shape
     return pl.pallas_call(
         attend_kernel,
         out_shape=(
             jax.ShapeDtypeStruct((w_out.shape[1], slots), BF16),
             jax.ShapeDtypeStruct((slots, span * batch), BF16),
-            jax.ShapeDtypeStruct((near_feats, slots), BF16),
+            jax.ShapeDtypeStruct((own, slots), BF16),
         ),
         in_specs=full(4),
         out_specs=tuple(full(3)),
         compiler_params=PARAMS,
         name="attend",
-    )(heads, table, w_out, every)
-
-
-def gate_kernel(x_ref, gain_ref, wg_ref, wu_ref, out_ref, own_ref):
+    )(heads, table, w_out, flat)
+
+
+def gate_kernel(x_ref, gain_ref, wg_ref, wu_ref, out_ref):
     kv_count, local, wide = out_ref.shape
     units = wg_ref.shape[0]
-    near_count, feats, slots = x_ref.shape
-    x = x_ref[...].astype(F32).reshape(near_count * feats, slots)
-    own = own_ref.shape[0]
-    first = ((lax.axis_index(Z)) * lax.axis_size("c") + lax.axis_index("c")) * own
-    chunk = x_ref[first // feats].astype(F32)
-    mine = chunk[:own]
-    for k in range(1, feats // own):
-        mine = jnp.where(first % feats == k * own, chunk[k * own : (k + 1) * own], mine)
-    own_ref[...] = mine.astype(BF16)
-    normed, squares = normed_rows(x.T, gain_ref[1:2])
+    normed, squares = normed_rows(features_of(x_ref), gain_ref[1:2])
 
     def put(at, value):
         width = value.shape[1]
@@ -334,19 +319,16 @@
     half = wide // 2
     put(0, dot(normed, wg_ref[...], (1, 1)))
     put(half, dot(normed, wu_ref[...], (1, 1)))
-    put(units, jnp.broadcast_to(squares, (slots, half - units)))
-
-
-def gate(x, gain, w_gate, w_up, kv_count, own):
+    put(units, jnp.broadcast_to(squares, (x_ref.shape[3], half - units)))
+
+
+def gate(x, gain, w_gate, w_up, kv_count):
     rows = x.shape[-1]
     return pl.pallas_call(
         gate_kernel,
-        out_shape=(
-            jax.ShapeDtypeStruct((kv_count, rows // kv_count, 768), BF16),
-            jax.ShapeDtypeStruct((own, rows), BF16),
-        ),
+        out_shape=jax.ShapeDtypeStruct((kv_count, rows // kv_count, 768), BF16),
         in_specs=full(4),
-        out_specs=tuple(full(2)),
+        out_specs=pl.BlockSpec(memory_space=pltpu.VMEM),
         compiler_params=PARAMS,
         name="gate",
     )(x, gain, w_gate, w_up)
@@ -411,14 +393,11 @@
     every = lax.all_gather(swap(sent, Z), "c", axis=0, tiled=False)
     sums = project(every, gains, w_query, w_key, w_value, w_beta.T, w_alpha.T, kv_count)
     heads, updated = delta_step(swap(sums, "kv"), state, table)
-    near_count = lax.axis_size(NEAR)
-    attn_part, picker, base_rows = attend(
-        swap(heads, "kv"), table, w_out, every, slots, w_out.shape[1] // near_count
-    )
-    near_sum = swap(attn_part.reshape(near_count, -1, slots), NEAR).astype(F32).sum(axis=0)
-    far_terms = spread(near_sum.astype(BF16), "zh").astype(F32).sum(axis=0)
-    middle_rows = spread((base_rows.astype(F32) + far_terms).astype(BF16), NEAR)
-    share, middle = gate(middle_rows, gains, w_gate.T, w_up.T, kv_count, flat.shape[1])
+    attn_part, picker, base_rows = attend(swap(heads, "kv"), table, w_out, flat, slots)
+    attn_own = swap(pair_sum(attn_part, core), Z).astype(F32).sum(axis=0)
+    middle = (base_rows.astype(F32) + attn_own).astype(BF16)
+    middle_rows = lax.all_gather(spread(middle, Z), "c", axis=0, tiled=False)
+    share = gate(middle_rows, gains, w_gate.T, w_up.T, kv_count)
     share = swap(share, "kv").astype(F32).sum(axis=0)
     units = w_gate.shape[1]
     share_scale = lax.rsqrt(share[:, units : units + 1] / D + EPSILON)
@@ -433,8 +412,8 @@
 
 
 def solution(mesh):
-    tp = ("zh", "zl", "c")
-    split = Mesh(mesh.devices.reshape(mesh.shape["kv"], -1, 4, 2), ("kv", *tp))
+    tp = ("z", "c")
+    split = Mesh(mesh.devices.reshape(mesh.shape["kv"], -1, 2), ("kv", *tp))
     return jax.shard_map(
         body,
         mesh=split,

time: 148 us -> 147 us (level)
    all_to_all x9 -> x8, blocking collectives: 130 us -> 122 us  [swap(): return lax.all_to_all(tiles, axis, split_axis=0, concat_axis=0, tiled=True)]
    all_gather x0 -> x1, blocking collectives: none -> 3.8 us  [body(): middle_rows = lax.all_gather(spread(middle, Z), 'c', axis=0, tiled=False)]
    all_gather x1 -> x2, blocking collectives: 4.9 us -> 8.41 us  [pair_sum(): pair = lax.all_gather(part, 'c', axis=0, tiled=False)]
where the time goes in v6:
time: 147 us; the launch traced here: 146 us
  blocking collectives  140 us (95%)
  Pallas kernels  3.63 us (2%)
    all_to_all x8, blocking collectives, swap(): return lax.all_to_all(tiles, axis, split_axis=0, concat_axis=0, tiled=True)  122 us
    all_gather x2, blocking collectives, pair_sum(): pair = lax.all_gather(part, 'c', axis=0, tiled=False)  8.41 us
    all_gather x1, blocking collectives, body(): every = lax.all_gather(swap(sent, Z), 'c', axis=0, tiled=False)  5.51 us
    all_gather x1, blocking collectives, body(): middle_rows = lax.all_gather(spread(middle, Z), 'c', axis=0, tiled=False)  3.8 us

profile of v6, /device:TPU:1, one launch (start us, length us, event | category | flops | bytes accessed | tf_op | source)
XLA Modules:
  0.0 146.2 jit_solution(5687866553443448103)
XLA Ops:
  0.6 0.0 copy-start
  0.7 0.0 copy-start.10
  0.7 0.0 copy-start.16
  0.7 0.0 copy-start.12
  0.7 0.0 copy-start.14
  0.7 0.0 copy-start.15
  0.7 0.0 copy-start.11
  0.7 0.0 copy-start.13
  0.7 0.7 copy-done.10
  1.4 0.0 copy-done.16
  1.4 0.0 copy-done.12
  1.4 0.0 copy-done.14
  1.4 0.0 copy-done.15
  1.4 0.0 copy-done.11
  1.4 0.0 copy-done.13
  1.5 0.1 prepare.1
  1.5 27.6 %all_to_all.40 = bf16[16,4,8,128]{3,2,1,0:T(8,128)(2,1)S(1)} all-to-all(bf16[16,4,8,128]{3,2,1,0:T(8,128)(2,1)S(1)} %get-tuple-element.13), channel_id=1, replica_groups=mesh['kv'=16,'z'=16,'c'=2] {'z'}, dimensions={0} | all-to-all | bytes 262144 | tf_op jit(solution)/shard_map/all_to_all | solution.py:19
  29.2 5.5 %all-gather = bf16[32,4,8,128]{3,2,1,0:T(8,128)(2,1)S(1)} all-gather(bf16[16,4,8,128]{3,2,1,0:T(8,128)(2,1)S(1)} %all_to_all.40), channel_id=2, replica_groups=mesh['kv'=16,'z'=16,'c'=2] {'c'}, dimensions={0}, use_global_device_ids=true | all-gather | bytes 393216 | tf_op jit(solution)/shard_map/all_gather | solution.py:393
  34.7 0.0 copy-done.8
  34.7 0.0 copy-done.3
  34.7 0.0 copy-done.2
  34.7 0.0 copy-done.6
  34.7 0.0 copy-done.7
  34.7 0.4 project.1
  35.2 0.0 copy-start.1
  35.2 17.4 %all_to_all.41.recv_ref = bf16[16,32,512]{2,1,0:T(8,128)(2,1)S(1)} all-to-all(bf16[16,32,512]{2,1,0:T(8,128)(2,1)S(1)} %project.1), channel_id=1, replica_groups=mesh['kv'=16,'z'=16,'c'=2] {'kv'}, dimensions={0} | all-to-all | bytes 1048576 | tf_op jit(solution)/shard_map/all_to_all | solution.py:19
  52.6 0.0 copy-done.1
  52.6 1.4 delta.1
  54.0 10.3 %all_to_all.42.heads_ref = bf16[16,32,128]{2,1,0:T(8,128)(2,1)S(1)} all-to-all(bf16[16,32,128]{2,1,0:T(8,128)(2,1)S(1)} %get-tuple-element.16), channel_id=1, replica_groups=mesh['kv'=16,'z'=16,'c'=2] {'kv'}, dimensions={0} | all-to-all | bytes 262144 | tf_op jit(solution)/shard_map/all_to_all | solution.py:19
  64.3 0.0 copy-done.9
  64.3 0.6 attend.1
  64.8 4.2 %all-gather.1 = bf16[512,256]{1,0:T(8,128)(2,1)S(1)} all-gather(bf16[256,256]{1,0:T(8,128)(2,1)S(1)} %get-tuple-element.18), channel_id=3, replica_groups=mesh['kv'=16,'z'=16,'c'=2] {'c'}, dimensions={0}, use_global_device_ids=true | all-gather | bytes 393216 | tf_op jit(solution)/shard_map/all_gather | solution.py:29
  69.0 15.0 %all_to_all.43 = bf16[16,8,256]{2,1,0:T(8,128)(2,1)S(1)} all-to-all(bf16[16,8,256]{2,1,0:T(8,128)(2,1)S(1)} %dynamic-slice_reduce_fusion.1), channel_id=1, replica_groups=mesh['kv'=16,'z'=16,'c'=2] {'z'}, dimensions={0} | all-to-all | bytes 131072 | tf_op jit(solution)/shard_map/all_to_all | solution.py:19
  84.0 0.0 copy-start.5
  84.1 0.0 copy-start.4
  84.1 15.4 %all_to_all.44 = bf16[16,8,256]{2,1,0:T(8,128)(2,1)S(1)} all-to-all(bf16[16,8,256]{2,1,0:T(8,128)(2,1)S(1)} %broadcast_in_dim.36), channel_id=1, replica_groups=mesh['kv'=16,'z'=16,'c'=2] {'z'}, dimensions={0} | all-to-all | bytes 131072 | tf_op jit(solution)/shard_map/all_to_all | solution.py:19
  99.5 3.8 %all-gather.2 = bf16[32,8,256]{2,1,0:T(8,128)(2,1)S(1)} all-gather(bf16[16,8,256]{2,1,0:T(8,128)(2,1)S(1)} %all_to_all.44), channel_id=4, replica_groups=mesh['kv'=16,'z'=16,'c'=2] {'c'}, dimensions={0}, use_global_device_ids=true | all-gather | bytes 196608 | tf_op jit(solution)/shard_map/all_gather | solution.py:399
  103.3 0.4 gate.1
  103.6 12.3 %all_to_all.45 = bf16[16,16,768]{2,1,0:T(8,128)(2,1)S(1)} all-to-all(bf16[16,16,768]{2,1,0:T(8,128)(2,1)S(1)} %gate.1), channel_id=1, replica_groups=mesh['kv'=16,'z'=16,'c'=2] {'kv'}, dimensions={0} | all-to-all | bytes 786432 | tf_op jit(solution)/shard_map/all_to_all | solution.py:19
  116.0 0.1 convert_reduce_fusion
  116.0 0.2 fusion.5
  116.2 0.1 fusion.2
  116.4 10.1 %all_to_all.46 = bf16[16,16,344]{2,1,0:T(8,128)(2,1)S(1)} all-to-all(bf16[16,16,344]{2,1,0:T(8,128)(2,1)S(1)} %broadcast_in_dim.37), channel_id=1, replica_groups=mesh['kv'=16,'z'=16,'c'=2] {'kv'}, dimensions={0} | all-to-all | bytes 352256 | tf_op jit(solution)/shard_map/all_to_all | solution.py:19
  126.5 0.2 fusion
  126.7 4.2 %all-gather.3 = bf16[512,256]{0,1:T(8,128)(2,1)S(1)} all-gather(bf16[256,256]{0,1:T(8,128)(2,1)S(1)} %fusion), channel_id=5, replica_groups=mesh['kv'=16,'z'=16,'c'=2] {'c'}, dimensions={0}, use_global_device_ids=true | all-gather | bytes 393216 | tf_op jit(solution)/shard_map/all_gather | solution.py:29
  131.0 0.1 copy.24
  131.1 14.3 %all_to_all.47.recv_ref = bf16[16,8,256]{2,1,0:T(8,128)(2,1)S(1)} all-to-all(bf16[16,8,256]{2,1,0:T(8,128)(2,1)S(1)} %dynamic-slice_reduce_fusion), channel_id=1, replica_groups=mesh['kv'=16,'z'=16,'c'=2] {'z'}, dimensions={0} | all-to-all | bytes 131072 | tf_op jit(solution)/shard_map/all_to_all | solution.py:19
  145.4 0.8 finish.1
  (15 shorter events, 0.1 us)
Async XLA Ops:
  0.6 125.9 %copy-start = (bf16[344,256]{1,0:T(8,128)(2,1)S(1)}, bf16[344,256]{1,0:T(8,128)(2,1)}, u32[]{:S(2)}) copy-start(bf16[344,256]{1,0:T(8,128)(2,1)} %param.33) | copy-start | bytes 528388
  0.7 0.7 copy-start.10
  0.7 0.7 copy-start.16
  0.7 0.7 copy-start.12
  0.7 0.7 copy-start.14
  0.7 0.7 copy-start.15
  0.7 0.7 copy-start.11
  0.7 0.7 copy-start.13
  1.5 33.2 %copy-start.8 = (bf16[256,128]{1,0:T(8,128)(2,1)S(1)}, bf16[256,128]{1,0:T(8,128)(2,1)}, u32[]{:S(2)}) copy-start(bf16[256,128]{1,0:T(8,128)(2,1)} %wv_ref.1) | copy-start | bytes 196612
  1.5 33.2 %copy-start.3 = (bf16[4096,32]{0,1:T(8,128)(2,1)S(1)}, bf16[4096,32]{0,1:T(8,128)(2,1)}, u32[]{:S(2)}) copy-start(bf16[4096,32]{0,1:T(8,128)(2,1)} %param.25) | copy-start | bytes 786436
  29.2 5.5 %copy-start.2 = (bf16[4096,32]{0,1:T(8,128)(2,1)S(1)}, bf16[4096,32]{0,1:T(8,128)(2,1)}, u32[]{:S(2)}) copy-start(bf16[4096,32]{0,1:T(8,128)(2,1)} %param.24) | copy-start | bytes 786436
  29.2 5.5 %copy-start.6 = (bf16[256,128]{1,0:T(8,128)(2,1)S(1)}, bf16[256,128]{1,0:T(8,128)(2,1)}, u32[]{:S(2)}) copy-start(bf16[256,128]{1,0:T(8,128)(2,1)} %wq_ref.1) | copy-start | bytes 196612
  29.2 5.5 %copy-start.7 = (bf16[256,128]{1,0:T(8,128)(2,1)S(1)}, bf16[256,128]{1,0:T(8,128)(2,1)}, u32[]{:S(2)}) copy-start(bf16[256,128]{1,0:T(8,128)(2,1)} %wk_ref.1) | copy-start | bytes 196612
  35.2 17.4 %copy-start.1 = (f32[8,128,128]{2,1,0:T(8,128)S(1)}, f32[8,128,128]{2,1,0:T(8,128)}, u32[]{:S(2)}) copy-start(f32[8,128,128]{2,1,0:T(8,128)} %state_ref.1) | copy-start | bytes 1572868
  54.0 10.3 %copy-start.9 = (bf16[128,256]{1,0:T(8,128)(2,1)S(1)}, bf16[128,256]{1,0:T(8,128)(2,1)}, u32[]{:S(2)}) copy-start(bf16[128,256]{1,0:T(8,128)(2,1)} %w_ref.1) | copy-start | bytes 196612
  84.0 19.2 %copy-start.5 = (bf16[256,344]{0,1:T(8,128)(2,1)S(1)}, bf16[256,344]{0,1:T(8,128)(2,1)}, u32[]{:S(2)}) copy-start(bf16[256,344]{0,1:T(8,128)(2,1)} %param.32) | copy-start | bytes 528388
  84.1 19.2 %copy-start.4 = (bf16[256,344]{0,1:T(8,128)(2,1)S(1)}, bf16[256,344]{0,1:T(8,128)(2,1)}, u32[]{:S(2)}) copy-start(bf16[256,344]{0,1:T(8,128)(2,1)} %param.31) | copy-start | bytes 528388

commit v7 on v6

--- a/solution.py
+++ b/solution.py
@@ -66,14 +66,14 @@
     sent_ref,
     gains_ref,
     table_ref,
+    picker_ref,
 ):
     seqs, batch = table_ref.shape[1:]
+    span = flat_ref.shape[0]
+    slots = picker_ref.shape[0]
     heads = rate_ref.shape[1]
     first = lax.axis_index("kv") * seqs
     head = lax.axis_index(Z) * lax.axis_size("c") + lax.axis_index("c")
-    flat = flat_ref[...]
-    for k in range(sent_ref.shape[0]):
-        sent_ref[k] = flat
     gains_ref[0:1] = gain_in_ref[...]
     gains_ref[1:2] = gain_mid_ref[...]
     lengths = jnp.broadcast_to(lengths_ref[...].astype(F32), (seqs, batch))
@@ -85,6 +85,17 @@
         column = jnp.sum(jnp.where(mask, values, 0.0), axis=1, keepdims=True)
         return jnp.broadcast_to(column, (seqs, batch))
 
+    above = lax.broadcasted_iota(jnp.int32, (batch, batch), 0)
+    across = lax.broadcasted_iota(jnp.int32, (batch, batch), 1)
+    ahead = dot(lengths.astype(BF16), (above < across).astype(BF16), (1, 0))[:1]
+    slot = lax.broadcasted_iota(jnp.int32, (slots, batch), 0).astype(F32)
+    for t in range(span):
+        target = jnp.where(lengths[:1] > t, ahead + t, -1.0)
+        picker_ref[:, t * batch : (t + 1) * batch] = (slot == target).astype(BF16)
+    flat = jnp.concatenate([flat_ref[t] for t in range(span)], axis=1)
+    packed = dot(flat, picker_ref[...], (1, 1)).astype(BF16)
+    for k in range(sent_ref.shape[0]):
+        sent_ref[k] = packed
     table_ref[0] = lengths
     table_ref[1] = chosen(own, lengths)
     table_ref[2] = chosen(mine, jnp.broadcast_to(rate_ref[...], (seqs, heads)))
@@ -92,26 +103,32 @@
     table_ref[4] = jnp.broadcast_to(gain_out_ref[...], (seqs, batch))
 
 
-def prepare(seqs, *arrays):
+def prepare(seqs, slots, *arrays):
     flat, gain = arrays[0], arrays[4]
+    span, own, batch = flat.shape
     return pl.pallas_call(
         prepare_kernel,
         out_shape=(
-            jax.ShapeDtypeStruct((lax.axis_size(Z), *flat.shape), BF16),
+            jax.ShapeDtypeStruct((lax.axis_size(Z), own, slots), BF16),
             jax.ShapeDtypeStruct((8, gain.shape[1]), F32),
-            jax.ShapeDtypeStruct((5, seqs, flat.shape[2]), F32),
+            jax.ShapeDtypeStruct((5, seqs, batch), F32),
+            jax.ShapeDtypeStruct((slots, span * batch), BF16),
         ),
         in_specs=full(len(arrays)),
-        out_specs=tuple(full(3)),
+        out_specs=tuple(full(4)),
         compiler_params=PARAMS,
         cost_estimate=COST,
         name="prepare",
     )(*arrays)
 
 
-def project_kernel(x_ref, gain_ref, wq_ref, wk_ref, wv_ref, wb_ref, wa_ref, out_ref):
+def project_kernel(
+    x_ref, gain_ref, picker_ref, wq_ref, wk_ref, wv_ref, wb_ref, wa_ref, out_ref
+):
     kv_count, local_rows, _ = out_ref.shape
-    span = x_ref.shape[2]
+    slots, rows = picker_ref.shape
+    batch = 128
+    span = rows // batch
     seqs = local_rows // span
     heads = wb_ref.shape[0]
     head = lax.axis_index(Z) * lax.axis_size("c") + lax.axis_index("c")
@@ -127,26 +144,26 @@
     small = jnp.where(row == 0, own_row(wb_ref), jnp.where(row == 1, own_row(wa_ref), 0.0))
     small = small.astype(BF16)
     weights = jnp.concatenate([wq_ref[...], wk_ref[...], wv_ref[...]], axis=1)
-    lane = lax.broadcasted_iota(jnp.int32, (x_ref.shape[4], 128), 1)
+    lane = lax.broadcasted_iota(jnp.int32, (slots, 128), 1)
+    normed, squares = normed_rows(features_of(x_ref), gain_ref[0:1])
+    extra = jnp.where(lane == 2, squares, dot(normed, small, (1, 1))).astype(BF16)
+    packed = jnp.concatenate([dot(normed, weights, (1, 0)).astype(BF16), extra], axis=1)
+    placed = dot(picker_ref[...], packed, (0, 0))
     for t in range(span):
-        normed, squares = normed_rows(features_of(x_ref, t), gain_ref[0:1])
-        at = slice(t * seqs, (t + 1) * seqs)
-        wide = dot(normed, weights, (1, 0))
-        extra = jnp.where(lane == 2, squares, dot(normed, small, (1, 1)))
-        out_ref[:, at, :384] = wide.reshape(kv_count, seqs, 384).astype(BF16)
-        out_ref[:, at, 384:] = extra.reshape(kv_count, seqs, 128).astype(BF16)
-
-
-def project(x, gain, wq, wk, wv, wb, wa, kv_count):
-    rows = x.shape[2] * x.shape[4]
+        block = placed[t * batch : (t + 1) * batch].reshape(kv_count, seqs, -1)
+        out_ref[:, t * seqs : (t + 1) * seqs] = block.astype(BF16)
+
+
+def project(x, gain, picker, wq, wk, wv, wb, wa, kv_count):
+    rows = picker.shape[1]
     return pl.pallas_call(
         project_kernel,
         out_shape=jax.ShapeDtypeStruct((kv_count, rows // kv_count, 512), BF16),
-        in_specs=full(7),
+        in_specs=full(8),
         out_specs=pl.BlockSpec(memory_space=pltpu.VMEM),
         compiler_params=PARAMS,
         name="project",
-    )(x, gain, wq, wk, wv, wb, wa)
+    )(x, gain, picker, wq, wk, wv, wb, wa)
 
 
 def delta_kernel(recv_ref, state_ref, table_ref, head_ref, new_ref):
@@ -263,20 +280,10 @@
     )(recv, state, table)
 
 
-def attend_kernel(heads_ref, table_ref, w_ref, flat_ref, part_ref, picker_ref, base_ref):
-    slots, rows = picker_ref.shape
-    span, _, batch = flat_ref.shape
+def attend_kernel(heads_ref, picker_ref, w_ref, part_ref):
     kv_count, local_rows, size = heads_ref.shape
+    span = picker_ref.shape[1] // 128
     seqs = local_rows // span
-    lengths = table_ref[0]
-    above = lax.broadcasted_iota(jnp.int32, (batch, batch), 0)
-    across = lax.broadcasted_iota(jnp.int32, (batch, batch), 1)
-    ahead = dot(lengths.astype(BF16), (above < across).astype(BF16), (1, 0))[:1]
-    slot = lax.broadcasted_iota(jnp.int32, (slots, batch), 0).astype(F32)
-    for t in range(span):
-        target = jnp.where(lengths[:1] > t, ahead + t, -1.0)
-        picker_ref[:, t * batch : (t + 1) * batch] = (slot == target).astype(BF16)
-    picker = picker_ref[...]
     heads = heads_ref[...].astype(F32)
     heads = jnp.concatenate(
         [
@@ -285,26 +292,19 @@
         ],
         axis=0,
     ).astype(BF16)
-    packed = dot(picker, heads, (1, 0)).astype(BF16)
+    packed = dot(picker_ref[...], heads, (1, 0)).astype(BF16)
     part_ref[...] = dot(packed, w_ref[...], (1, 0)).T.astype(BF16)
-    flat = jnp.concatenate([flat_ref[t] for t in range(span)], axis=1)
-    base_ref[...] = dot(flat, picker, (1, 1)).astype(BF16)
-
-
-def attend(heads, table, w_out, flat, slots):
-    span, own, batch = flat.shape
+
+
+def attend(heads, picker, w_out):
     return pl.pallas_call(
         attend_kernel,
-        out_shape=(
-            jax.ShapeDtypeStruct((w_out.shape[1], slots), BF16),
-            jax.ShapeDtypeStruct((slots, span * batch), BF16),
-            jax.ShapeDtypeStruct((own, slots), BF16),
-        ),
-        in_specs=full(4),
-        out_specs=tuple(full(3)),
+        out_shape=jax.ShapeDtypeStruct((w_out.shape[1], picker.shape[0]), BF16),
+        in_specs=full(3),
+        out_specs=pl.BlockSpec(memory_space=pltpu.VMEM),
         compiler_params=PARAMS,
         name="attend",
-    )(heads, table, w_out, flat)
+    )(heads, picker, w_out)
 
 
 def gate_kernel(x_ref, gain_ref, wg_ref, wu_ref, out_ref):
@@ -334,7 +334,9 @@
     )(x, gain, w_gate, w_up)
 
 
-def finish_kernel(recv_ref, middle_ref, picker_ref, out_ref):
+def finish_kernel(recv_ref, middle_ref, picker_ref, state_ref, out_ref, new_ref, sem):
+    copy = pltpu.make_async_copy(state_ref, new_ref, sem)
+    copy.start()
     total = middle_ref[...].astype(F32)
     for k in range(recv_ref.shape[0]):
         total = total + recv_ref[k].astype(F32)
@@ -342,18 +344,23 @@
     spread_out = dot(total.astype(BF16), picker_ref[...], (1, 0)).astype(BF16)
     for t in range(span):
         out_ref[t] = spread_out[:, t * batch : (t + 1) * batch]
-
-
-def finish(recv, middle, picker, span):
+    copy.wait()
+
+
+def finish(recv, middle, picker, state, span):
     own = middle.shape[0]
     return pl.pallas_call(
         finish_kernel,
-        out_shape=jax.ShapeDtypeStruct((span, own, picker.shape[1] // span), BF16),
-        in_specs=full(3),
-        out_specs=pl.BlockSpec(memory_space=pltpu.VMEM),
+        out_shape=(
+            jax.ShapeDtypeStruct((span, own, picker.shape[1] // span), BF16),
+            jax.ShapeDtypeStruct(state.shape, F32),
+        ),
+        in_specs=full(4),
+        out_specs=(pl.BlockSpec(memory_space=pltpu.VMEM), pl.BlockSpec(memory_space=pl.ANY)),
+        scratch_shapes=[pltpu.SemaphoreType.DMA],
         compiler_params=PARAMS,
         name="finish",
-    )(recv, middle, picker)
+    )(recv, middle, picker, state)
 
 
 def body(
@@ -380,8 +387,9 @@
 
     core = lax.axis_index("c").astype(jnp.uint32)
     flat, core = lax.optimization_barrier((tokens.transpose(1, 2, 0), core))
-    sent, gains, table = prepare(
+    sent, gains, table, picker = prepare(
         state.shape[0],
+        slots,
         flat,
         lengths[None, :],
         decay_rate[None, :],
@@ -391,11 +399,13 @@
         out_gain[None, :],
     )
     every = lax.all_gather(swap(sent, Z), "c", axis=0, tiled=False)
-    sums = project(every, gains, w_query, w_key, w_value, w_beta.T, w_alpha.T, kv_count)
+    sums = project(
+        every, gains, picker, w_query, w_key, w_value, w_beta.T, w_alpha.T, kv_count
+    )
     heads, updated = delta_step(swap(sums, "kv"), state, table)
-    attn_part, picker, base_rows = attend(swap(heads, "kv"), table, w_out, flat, slots)
+    attn_part = attend(swap(heads, "kv"), picker, w_out)
     attn_own = swap(pair_sum(attn_part, core), Z).astype(F32).sum(axis=0)
-    middle = (base_rows.astype(F32) + attn_own).astype(BF16)
+    middle = lax.optimization_barrier((sent[0].astype(F32) + attn_own).astype(BF16))
     middle_rows = lax.all_gather(spread(middle, Z), "c", axis=0, tiled=False)
     share = gate(middle_rows, gains, w_gate.T, w_up.T, kv_count)
     share = swap(share, "kv").astype(F32).sum(axis=0)
@@ -407,8 +417,10 @@
     ).astype(BF16)
     hidden_every = spread(hidden, "kv").reshape(slots, units)
     down_part = dot(w_down, hidden_every, (0, 1)).astype(BF16)
-    mixed = finish(swap(pair_sum(down_part, core), Z), middle, picker, flat.shape[0])
-    return (mixed.transpose(2, 0, 1), updated)
+    mixed, new_state = finish(
+        swap(pair_sum(down_part, core), Z), middle, picker, updated, flat.shape[0]
+    )
+    return (mixed.transpose(2, 0, 1), new_state)
 
 
 def solution(mesh):

time: 147 us -> 144 us (0.980)
  blocking collectives: 140 us -> 137 us
    all_gather x1, blocking collectives: 5.51 us -> 3.78 us  [body(): every = lax.all_gather(swap(sent, Z), 'c', axis=0, tiled=False)]
where the time goes in v7:
time: 144 us
  blocking collectives  137 us (95%)
  Pallas kernels  3.77 us (3%)
    all_to_all x8, blocking collectives, swap(): return lax.all_to_all(tiles, axis, split_axis=0, concat_axis=0, tiled=True)  121 us
    all_gather x2, blocking collectives, pair_sum(): pair = lax.all_gather(part, 'c', axis=0, tiled=False)  8.41 us
    all_gather x1, blocking collectives, body(): middle_rows = lax.all_gather(spread(middle, Z), 'c', axis=0, tiled=False)  3.92 us
    all_gather x1, blocking collectives, body(): every = lax.all_gather(swap(sent, Z), 'c', axis=0, tiled=False)  3.78 us

profile of v7, /device:TPU:1, one launch (start us, length us, event | category | flops | bytes accessed | tf_op | source)
XLA Modules:
  0.0 143.5 jit_solution(5699274796021449759)
XLA Ops:
  0.6 0.0 copy-start
  0.7 0.0 copy-start.10
  0.7 0.0 copy-start.16
  0.7 0.0 copy-start.12
  0.7 0.0 copy-start.14
  0.7 0.0 copy-start.15
  0.7 0.0 copy-start.11
  0.7 0.0 copy-start.13
  0.7 0.7 copy-done.10
  1.4 0.0 copy-done.16
  1.4 0.0 copy-done.12
  1.4 0.0 copy-done.14
  1.4 0.0 copy-done.15
  1.4 0.0 copy-done.11
  1.5 0.0 copy-done.13
  1.5 0.3 prepare.1
  1.8 27.2 %all_to_all.40 = bf16[16,8,256]{2,1,0:T(8,128)(2,1)S(1)} all-to-all(bf16[16,8,256]{2,1,0:T(8,128)(2,1)S(1)} %get-tuple-element.13), channel_id=1, replica_groups=mesh['kv'=16,'z'=16,'c'=2] {'z'}, dimensions={0} | all-to-all | bytes 131072 | tf_op jit(solution)/shard_map/all_to_all | solution.py:19
  29.1 3.8 %all-gather = bf16[32,8,256]{2,1,0:T(8,128)(2,1)S(1)} all-gather(bf16[16,8,256]{2,1,0:T(8,128)(2,1)S(1)} %all_to_all.40), channel_id=2, replica_groups=mesh['kv'=16,'z'=16,'c'=2] {'c'}, dimensions={0}, use_global_device_ids=true | all-gather | bytes 196608 | tf_op jit(solution)/shard_map/all_gather | solution.py:401
  32.8 0.0 copy-done.3
  32.8 0.0 copy-done.7
  32.8 0.0 copy-done.8
  32.8 0.0 copy-done.2
  32.9 0.0 copy-done.6
  32.9 0.6 project.1
  33.5 0.0 copy-start.1
  33.5 17.4 %all_to_all.41.recv_ref = bf16[16,32,512]{2,1,0:T(8,128)(2,1)S(1)} all-to-all(bf16[16,32,512]{2,1,0:T(8,128)(2,1)S(1)} %project.1), channel_id=1, replica_groups=mesh['kv'=16,'z'=16,'c'=2] {'kv'}, dimensions={0} | all-to-all | bytes 1048576 | tf_op jit(solution)/shard_map/all_to_all | solution.py:19
  50.9 0.6 delta.1
  51.5 0.0 copy-start.9
  51.5 10.3 %all_to_all.42.heads_ref = bf16[16,32,128]{2,1,0:T(8,128)(2,1)S(1)} all-to-all(bf16[16,32,128]{2,1,0:T(8,128)(2,1)S(1)} %get-tuple-element.17), channel_id=1, replica_groups=mesh['kv'=16,'z'=16,'c'=2] {'kv'}, dimensions={0} | all-to-all | bytes 262144 | tf_op jit(solution)/shard_map/all_to_all | solution.py:19
  61.8 0.4 attend.1
  62.2 4.2 %all-gather.1 = bf16[512,256]{1,0:T(8,128)(2,1)S(1)} all-gather(bf16[256,256]{1,0:T(8,128)(2,1)S(1)} %attend.1), channel_id=3, replica_groups=mesh['kv'=16,'z'=16,'c'=2] {'c'}, dimensions={0}, use_global_device_ids=true | all-gather | bytes 393216 | tf_op jit(solution)/shard_map/all_gather | solution.py:29
  66.4 14.2 %all_to_all.43 = bf16[16,8,256]{2,1,0:T(8,128)(2,1)S(1)} all-to-all(bf16[16,8,256]{2,1,0:T(8,128)(2,1)S(1)} %dynamic-slice_reduce_fusion.1), channel_id=1, replica_groups=mesh['kv'=16,'z'=16,'c'=2] {'z'}, dimensions={0} | all-to-all | bytes 131072 | tf_op jit(solution)/shard_map/all_to_all | solution.py:19
  80.7 0.0 copy-start.5
  80.7 0.0 copy-start.4
  80.8 15.3 %all_to_all.44 = bf16[16,8,256]{2,1,0:T(8,128)(2,1)S(1)} all-to-all(bf16[16,8,256]{2,1,0:T(8,128)(2,1)S(1)} %broadcast_in_dim.36), channel_id=1, replica_groups=mesh['kv'=16,'z'=16,'c'=2] {'z'}, dimensions={0} | all-to-all | bytes 131072 | tf_op jit(solution)/shard_map/all_to_all | solution.py:19
  96.0 3.9 %all-gather.2 = bf16[32,8,256]{2,1,0:T(8,128)(2,1)S(1)} all-gather(bf16[16,8,256]{2,1,0:T(8,128)(2,1)S(1)} %all_to_all.44), channel_id=4, replica_groups=mesh['kv'=16,'z'=16,'c'=2] {'c'}, dimensions={0}, use_global_device_ids=true | all-gather | bytes 196608 | tf_op jit(solution)/shard_map/all_gather | solution.py:409
  99.9 0.0 copy-done.4
  99.9 0.4 gate.1
  100.3 12.3 %all_to_all.45 = bf16[16,16,768]{2,1,0:T(8,128)(2,1)S(1)} all-to-all(bf16[16,16,768]{2,1,0:T(8,128)(2,1)S(1)} %gate.1), channel_id=1, replica_groups=mesh['kv'=16,'z'=16,'c'=2] {'kv'}, dimensions={0} | all-to-all | bytes 786432 | tf_op jit(solution)/shard_map/all_to_all | solution.py:19
  112.7 0.1 convert_reduce_fusion
  112.7 0.2 fusion.5
  112.9 0.1 fusion.2
  113.0 10.1 %all_to_all.46 = bf16[16,16,344]{2,1,0:T(8,128)(2,1)S(1)} all-to-all(bf16[16,16,344]{2,1,0:T(8,128)(2,1)S(1)} %broadcast_in_dim.37), channel_id=1, replica_groups=mesh['kv'=16,'z'=16,'c'=2] {'kv'}, dimensions={0} | all-to-all | bytes 352256 | tf_op jit(solution)/shard_map/all_to_all | solution.py:19
  123.2 0.2 fusion
  123.4 4.2 %all-gather.3 = bf16[512,256]{0,1:T(8,128)(2,1)S(1)} all-gather(bf16[256,256]{0,1:T(8,128)(2,1)S(1)} %fusion), channel_id=5, replica_groups=mesh['kv'=16,'z'=16,'c'=2] {'c'}, dimensions={0}, use_global_device_ids=true | all-gather | bytes 393216 | tf_op jit(solution)/shard_map/all_gather | solution.py:29
  127.6 0.1 copy.24
  127.8 14.3 %all_to_all.47.recv_ref = bf16[16,8,256]{2,1,0:T(8,128)(2,1)S(1)} all-to-all(bf16[16,8,256]{2,1,0:T(8,128)(2,1)S(1)} %dynamic-slice_reduce_fusion), channel_id=1, replica_groups=mesh['kv'=16,'z'=16,'c'=2] {'z'}, dimensions={0} | all-to-all | bytes 131072 | tf_op jit(solution)/shard_map/all_to_all | solution.py:19
  142.1 1.4 finish.1
  (15 shorter events, 0.1 us)
Async XLA Ops:
  0.6 122.6 %copy-start = (bf16[344,256]{1,0:T(8,128)(2,1)S(1)}, bf16[344,256]{1,0:T(8,128)(2,1)}, u32[]{:S(2)}) copy-start(bf16[344,256]{1,0:T(8,128)(2,1)} %param.33) | copy-start | bytes 528388
  0.7 0.7 copy-start.10
  0.7 0.7 copy-start.16
  0.7 0.7 copy-start.12
  0.7 0.7 copy-start.14
  0.7 0.7 copy-start.15
  0.7 0.7 copy-start.11
  0.7 0.7 copy-start.13
  1.5 31.4 %copy-start.3 = (bf16[4096,32]{0,1:T(8,128)(2,1)S(1)}, bf16[4096,32]{0,1:T(8,128)(2,1)}, u32[]{:S(2)}) copy-start(bf16[4096,32]{0,1:T(8,128)(2,1)} %param.25) | copy-start | bytes 786436
  1.5 31.4 %copy-start.7 = (bf16[256,128]{1,0:T(8,128)(2,1)S(1)}, bf16[256,128]{1,0:T(8,128)(2,1)}, u32[]{:S(2)}) copy-start(bf16[256,128]{1,0:T(8,128)(2,1)} %wk_ref.1) | copy-start | bytes 196612
  1.5 31.4 %copy-start.8 = (bf16[256,128]{1,0:T(8,128)(2,1)S(1)}, bf16[256,128]{1,0:T(8,128)(2,1)}, u32[]{:S(2)}) copy-start(bf16[256,128]{1,0:T(8,128)(2,1)} %wv_ref.1) | copy-start | bytes 196612
  1.8 31.0 %copy-start.2 = (bf16[4096,32]{0,1:T(8,128)(2,1)S(1)}, bf16[4096,32]{0,1:T(8,128)(2,1)}, u32[]{:S(2)}) copy-start(bf16[4096,32]{0,1:T(8,128)(2,1)} %param.24) | copy-start | bytes 786436
  29.1 3.8 %copy-start.6 = (bf16[256,128]{1,0:T(8,128)(2,1)S(1)}, bf16[256,128]{1,0:T(8,128)(2,1)}, u32[]{:S(2)}) copy-start(bf16[256,128]{1,0:T(8,128)(2,1)} %wq_ref.1) | copy-start | bytes 196612
  33.5 17.4 %copy-start.1 = (f32[8,128,128]{2,1,0:T(8,128)S(1)}, f32[8,128,128]{2,1,0:T(8,128)}, u32[]{:S(2)}) copy-start(f32[8,128,128]{2,1,0:T(8,128)} %state_ref.1) | copy-start | bytes 1572868
  51.5 10.3 %copy-start.9 = (bf16[128,256]{1,0:T(8,128)(2,1)S(1)}, bf16[128,256]{1,0:T(8,128)(2,1)}, u32[]{:S(2)}) copy-start(bf16[128,256]{1,0:T(8,128)(2,1)} %w_ref.1) | copy-start | bytes 196612
  80.7 19.2 %copy-start.5 = (bf16[256,344]{0,1:T(8,128)(2,1)S(1)}, bf16[256,344]{0,1:T(8,128)(2,1)}, u32[]{:S(2)}) copy-start(bf16[256,344]{0,1:T(8,128)(2,1)} %param.32) | copy-start | bytes 528388
  80.7 19.2 %copy-start.4 = (bf16[256,344]{0,1:T(8,128)(2,1)S(1)}, bf16[256,344]{0,1:T(8,128)(2,1)}, u32[]{:S(2)}) copy-start(bf16[256,344]{0,1:T(8,128)(2,1)} %param.31) | copy-start | bytes 528388

commit v8 on v7

--- a/solution.py
+++ b/solution.py
@@ -67,6 +67,7 @@
     gains_ref,
     table_ref,
     picker_ref,
+    own_picker_ref,
 ):
     seqs, batch = table_ref.shape[1:]
     span = flat_ref.shape[0]
@@ -92,6 +93,17 @@
     for t in range(span):
         target = jnp.where(lengths[:1] > t, ahead + t, -1.0)
         picker_ref[:, t * batch : (t + 1) * batch] = (slot == target).astype(BF16)
+    rows = own_picker_ref.shape[1]
+    place = lax.broadcasted_iota(jnp.int32, (batch, rows), 1)
+    place_seq = place // (span * seqs) * seqs + place % seqs
+    other = lax.broadcasted_iota(jnp.int32, (batch, rows), 0)
+    sizes = lengths.astype(BF16)
+    ahead = dot(sizes, (other < place_seq).astype(BF16), (1, 0))[:1]
+    limit = dot(sizes, (other == place_seq).astype(BF16), (1, 0))[:1]
+    step = (place[:1] // seqs % span).astype(F32)
+    target = jnp.where(limit > step, ahead + step, -1.0)
+    slot = lax.broadcasted_iota(jnp.int32, (slots, rows), 0).astype(F32)
+    own_picker_ref[...] = (slot == target).astype(BF16)
     flat = jnp.concatenate([flat_ref[t] for t in range(span)], axis=1)
     packed = dot(flat, picker_ref[...], (1, 1)).astype(BF16)
     for k in range(sent_ref.shape[0]):
@@ -113,9 +125,10 @@
             jax.ShapeDtypeStruct((8, gain.shape[1]), F32),
             jax.ShapeDtypeStruct((5, seqs, batch), F32),
             jax.ShapeDtypeStruct((slots, span * batch), BF16),
+            jax.ShapeDtypeStruct((slots, span * batch), BF16),
         ),
         in_specs=full(len(arrays)),
-        out_specs=tuple(full(4)),
+        out_specs=tuple(full(5)),
         compiler_params=PARAMS,
         cost_estimate=COST,
         name="prepare",
@@ -125,11 +138,8 @@
 def project_kernel(
     x_ref, gain_ref, picker_ref, wq_ref, wk_ref, wv_ref, wb_ref, wa_ref, out_ref
 ):
-    kv_count, local_rows, _ = out_ref.shape
-    slots, rows = picker_ref.shape
-    batch = 128
-    span = rows // batch
-    seqs = local_rows // span
+    kv_count = out_ref.shape[0]
+    rows = picker_ref.shape[1]
     heads = wb_ref.shape[0]
     head = lax.axis_index(Z) * lax.axis_size("c") + lax.axis_index("c")
     width = gain_ref.shape[1]
@@ -140,25 +150,30 @@
         tile = ref[:, pl.ds(start, width)].astype(F32)
         return jnp.sum(jnp.where(own_head, tile, 0.0), axis=0, keepdims=True)
 
-    row = lax.broadcasted_iota(jnp.int32, (128, width), 0)
+    row = lax.broadcasted_iota(jnp.int32, (8, width), 0)
     small = jnp.where(row == 0, own_row(wb_ref), jnp.where(row == 1, own_row(wa_ref), 0.0))
     small = small.astype(BF16)
     weights = jnp.concatenate([wq_ref[...], wk_ref[...], wv_ref[...]], axis=1)
-    lane = lax.broadcasted_iota(jnp.int32, (slots, 128), 1)
-    normed, squares = normed_rows(features_of(x_ref), gain_ref[0:1])
-    extra = jnp.where(lane == 2, squares, dot(normed, small, (1, 1))).astype(BF16)
-    packed = jnp.concatenate([dot(normed, weights, (1, 0)).astype(BF16), extra], axis=1)
-    placed = dot(picker_ref[...], packed, (0, 0))
-    for t in range(span):
-        block = placed[t * batch : (t + 1) * batch].reshape(kv_count, seqs, -1)
-        out_ref[:, t * seqs : (t + 1) * seqs] = block.astype(BF16)
+    x = features_of(x_ref)
+    normed = (x * gain_ref[0:1]).astype(BF16)
+    ones = (row == 2).astype(BF16)
+    extra = dot(small, normed, (1, 1)) + dot(ones, (x * x).astype(BF16), (1, 1))
+    extra = dot(extra.astype(BF16), picker_ref[...], (1, 0)).astype(BF16)
+    placed = dot(picker_ref[...], dot(normed, weights, (1, 0)).astype(BF16), (0, 0))
+    local = rows // kv_count
+    for k in range(3):
+        block = placed[:, k * 128 : (k + 1) * 128].reshape(kv_count, local, 128)
+        out_ref[:, k * local : (k + 1) * local] = block.astype(BF16)
+    for k in range(kv_count):
+        tile = k * local // 128
+        out_ref[k, 3 * local :] = extra[:, tile * 128 : (tile + 1) * 128]
 
 
 def project(x, gain, picker, wq, wk, wv, wb, wa, kv_count):
     rows = picker.shape[1]
     return pl.pallas_call(
         project_kernel,
-        out_shape=jax.ShapeDtypeStruct((kv_count, rows // kv_count, 512), BF16),
+        out_shape=jax.ShapeDtypeStruct((kv_count, 3 * rows // kv_count + 8, 128), BF16),
         in_specs=full(8),
         out_specs=pl.BlockSpec(memory_space=pltpu.VMEM),
         compiler_params=PARAMS,
@@ -166,9 +181,9 @@
     )(x, gain, picker, wq, wk, wv, wb, wa)
 
 
-def delta_kernel(recv_ref, state_ref, table_ref, head_ref, new_ref):
+def delta_kernel(recv_ref, state_ref, table_ref, head_ref, new_ref, extra_ref):
     seq_count, size, _ = state_ref.shape
-    rows = recv_ref.shape[1]
+    rows = head_ref.shape[1]
     span = rows // seq_count
     sums = recv_ref[0].astype(F32)
     for k in range(1, recv_ref.shape[0]):
@@ -177,7 +192,11 @@
     def lanes(column):
         return jnp.broadcast_to(column, (rows, size))
 
-    row_scale = lanes(lax.rsqrt(sums[:, 386:387] / D + EPSILON))
+    extra_ref[...] = sums[3 * rows :].T
+    per_tile = extra_ref.shape[0] // rows
+    start = pl.multiple_of(lax.axis_index("kv") % per_tile * rows, rows)
+    extra = extra_ref[pl.ds(start, rows)]
+    row_scale = lanes(lax.rsqrt(extra[:, 2:3] / D + EPSILON))
     row = lax.broadcasted_iota(jnp.int32, (rows, size), 0)
     step = row // seq_count
     seq = row % seq_count
@@ -186,18 +205,18 @@
         return jnp.concatenate([table_ref[k]] * span, axis=0)
 
     live = step.astype(F32) < every_step(1)
-    beta = jnp.where(live, jax.nn.sigmoid(lanes(sums[:, 384:385]) * row_scale), 0.0)
-    pre = lanes(sums[:, 385:386]) * row_scale + every_step(3)
+    beta = jnp.where(live, jax.nn.sigmoid(lanes(extra[:, 0:1]) * row_scale), 0.0)
+    pre = lanes(extra[:, 1:2]) * row_scale + every_step(3)
     soft = jnp.maximum(pre, 0.0) + jnp.log1p(jnp.exp(-jnp.abs(pre)))
     log_decay = jnp.where(live, -every_step(2) * soft, 0.0)
 
     def unit(block):
-        v = sums[:, block * size : (block + 1) * size] * row_scale
+        v = sums[block * rows : (block + 1) * rows] * row_scale
         return v * lax.rsqrt(jnp.sum(v * v, axis=1, keepdims=True) + EPSILON)
 
     queries = unit(0) * HEAD_DIM ** (-0.5)
     keys = unit(1)
-    values = sums[:, 2 * size : 3 * size] * row_scale
+    values = sums[2 * rows : 3 * rows] * row_scale
 
     def back(x, d):
         return pltpu.roll(x, d * seq_count, 0)
@@ -265,33 +284,23 @@
 
 
 def delta_step(recv, state, table):
-    kv_count, rows, _ = recv.shape
-    size = state.shape[1]
+    kv_count, sent_rows, size = recv.shape
     return pl.pallas_call(
         delta_kernel,
         out_shape=(
-            jax.ShapeDtypeStruct((kv_count, rows, size), BF16),
+            jax.ShapeDtypeStruct((kv_count, (sent_rows - 8) // 3, size), BF16),
             jax.ShapeDtypeStruct(state.shape, F32),
         ),
         in_specs=full(3),
         out_specs=tuple(full(2)),
+        scratch_shapes=[pltpu.VMEM((size, 8), F32)],
         compiler_params=PARAMS,
         name="delta",
     )(recv, state, table)
 
 
 def attend_kernel(heads_ref, picker_ref, w_ref, part_ref):
-    kv_count, local_rows, size = heads_ref.shape
-    span = picker_ref.shape[1] // 128
-    seqs = local_rows // span
-    heads = heads_ref[...].astype(F32)
-    heads = jnp.concatenate(
-        [
-            heads[:, t * seqs : (t + 1) * seqs].reshape(kv_count * seqs, size)
-            for t in range(span)
-        ],
-        axis=0,
-    ).astype(BF16)
+    heads = heads_ref[...].reshape(picker_ref.shape[1], heads_ref.shape[2])
     packed = dot(picker_ref[...], heads, (1, 0)).astype(BF16)
     part_ref[...] = dot(packed, w_ref[...], (1, 0)).T.astype(BF16)
 
@@ -334,30 +343,39 @@
     )(x, gain, w_gate, w_up)
 
 
-def finish_kernel(recv_ref, middle_ref, picker_ref, state_ref, out_ref, new_ref, sem):
-    copy = pltpu.make_async_copy(state_ref, new_ref, sem)
-    copy.start()
+def finish_kernel(
+    recv_ref, middle_ref, picker_ref, state_ref, out_ref, new_ref, local, sem_out, sem_new
+):
+    state_copy = pltpu.make_async_copy(state_ref, new_ref, sem_new)
+    state_copy.start()
     total = middle_ref[...].astype(F32)
     for k in range(recv_ref.shape[0]):
         total = total + recv_ref[k].astype(F32)
-    span, _, batch = out_ref.shape
+    span, _, batch = local.shape
     spread_out = dot(total.astype(BF16), picker_ref[...], (1, 0)).astype(BF16)
     for t in range(span):
-        out_ref[t] = spread_out[:, t * batch : (t + 1) * batch]
-    copy.wait()
+        local[t] = spread_out[:, t * batch : (t + 1) * batch]
+    out_copy = pltpu.make_async_copy(local, out_ref, sem_out)
+    out_copy.start()
+    out_copy.wait()
+    state_copy.wait()
 
 
 def finish(recv, middle, picker, state, span):
-    own = middle.shape[0]
+    mixed = (span, middle.shape[0], picker.shape[1] // span)
     return pl.pallas_call(
         finish_kernel,
         out_shape=(
-            jax.ShapeDtypeStruct((span, own, picker.shape[1] // span), BF16),
+            jax.ShapeDtypeStruct(mixed, BF16),
             jax.ShapeDtypeStruct(state.shape, F32),
         ),
         in_specs=full(4),
-        out_specs=(pl.BlockSpec(memory_space=pltpu.VMEM), pl.BlockSpec(memory_space=pl.ANY)),
-        scratch_shapes=[pltpu.SemaphoreType.DMA],
+        out_specs=(pl.BlockSpec(memory_space=pl.ANY),) * 2,
+        scratch_shapes=[
+            pltpu.VMEM(mixed, BF16),
+            pltpu.SemaphoreType.DMA,
+            pltpu.SemaphoreType.DMA,
+        ],
         compiler_params=PARAMS,
         name="finish",
     )(recv, middle, picker, state)
@@ -387,7 +405,7 @@
 
     core = lax.axis_index("c").astype(jnp.uint32)
     flat, core = lax.optimization_barrier((tokens.transpose(1, 2, 0), core))
-    sent, gains, table, picker = prepare(
+    sent, gains, table, picker, own_picker = prepare(
         state.shape[0],
         slots,
         flat,
@@ -400,10 +418,10 @@
     )
     every = lax.all_gather(swap(sent, Z), "c", axis=0, tiled=False)
     sums = project(
-        every, gains, picker, w_query, w_key, w_value, w_beta.T, w_alpha.T, kv_count
+        every, gains, own_picker, w_query, w_key, w_value, w_beta.T, w_alpha.T, kv_count
     )
     heads, updated = delta_step(swap(sums, "kv"), state, table)
-    attn_part = attend(swap(heads, "kv"), picker, w_out)
+    attn_part = attend(swap(heads, "kv"), own_picker, w_out)
     attn_own = swap(pair_sum(attn_part, core), Z).astype(F32).sum(axis=0)
     middle = lax.optimization_barrier((sent[0].astype(F32) + attn_own).astype(BF16))
     middle_rows = lax.all_gather(spread(middle, Z), "c", axis=0, tiled=False)

time: 144 us -> 143 us (level)
  no operation moved by 1% of the time
where the time goes in v8:
time: 143 us; the launch traced here: 142 us
  blocking collectives  136 us (95%)
  Pallas kernels  3.52 us (2%)
    all_to_all x8, blocking collectives, swap(): return lax.all_to_all(tiles, axis, split_axis=0, concat_axis=0, tiled=True)  120 us
    all_gather x2, blocking collectives, pair_sum(): pair = lax.all_gather(part, 'c', axis=0, tiled=False)  8.5 us
    all_gather x1, blocking collectives, body(): middle_rows = lax.all_gather(spread(middle, Z), 'c', axis=0, tiled=False)  3.85 us
    all_gather x1, blocking collectives, body(): every = lax.all_gather(swap(sent, Z), 'c', axis=0, tiled=False)  3.78 us

profile of v8, /device:TPU:1, one launch (start us, length us, event | category | flops | bytes accessed | tf_op | source)
XLA Modules:
  0.0 142.1 jit_solution(14849008096488161249)
XLA Ops:
  0.6 0.0 copy-start
  0.7 0.0 copy-start.10
  0.7 0.0 copy-start.16
  0.7 0.0 copy-start.12
  0.7 0.0 copy-start.14
  0.7 0.0 copy-start.15
  0.7 0.0 copy-start.11
  0.7 0.0 copy-start.13
  0.7 0.7 copy-done.10
  1.4 0.0 copy-done.16
  1.4 0.0 copy-done.12
  1.4 0.0 copy-done.14
  1.4 0.0 copy-done.15
  1.4 0.0 copy-done.11
  1.5 0.0 copy-done.13
  1.5 0.3 prepare.1
  1.8 27.2 %all_to_all.40 = bf16[16,8,256]{2,1,0:T(8,128)(2,1)S(1)} all-to-all(bf16[16,8,256]{2,1,0:T(8,128)(2,1)S(1)} %get-tuple-element.14), channel_id=1, replica_groups=mesh['kv'=16,'z'=16,'c'=2] {'z'}, dimensions={0} | all-to-all | bytes 131072 | tf_op jit(solution)/shard_map/all_to_all | solution.py:19
  29.0 3.8 %all-gather = bf16[32,8,256]{2,1,0:T(8,128)(2,1)S(1)} all-gather(bf16[16,8,256]{2,1,0:T(8,128)(2,1)S(1)} %all_to_all.40), channel_id=2, replica_groups=mesh['kv'=16,'z'=16,'c'=2] {'c'}, dimensions={0}, use_global_device_ids=true | all-gather | bytes 196608 | tf_op jit(solution)/shard_map/all_gather | solution.py:419
  32.8 0.0 copy-done.3
  32.8 0.0 copy-done.7
  32.8 0.0 copy-done.8
  32.8 0.0 copy-done.2
  32.8 0.0 copy-done.6
  32.8 0.9 project.1
  33.7 0.0 copy-start.1
  33.7 16.4 %all_to_all.41.recv_ref = bf16[16,104,128]{2,1,0:T(8,128)(2,1)S(1)} all-to-all(bf16[16,104,128]{2,1,0:T(8,128)(2,1)S(1)} %project.1), channel_id=1, replica_groups=mesh['kv'=16,'z'=16,'c'=2] {'kv'}, dimensions={0} | all-to-all | bytes 851968 | tf_op jit(solution)/shard_map/all_to_all | solution.py:19
  50.1 0.0 copy-done.1
  50.1 0.7 delta.1
  50.8 0.0 copy-start.9
  50.9 10.1 %all_to_all.42.heads_ref = bf16[16,32,128]{2,1,0:T(8,128)(2,1)S(1)} all-to-all(bf16[16,32,128]{2,1,0:T(8,128)(2,1)S(1)} %get-tuple-element.18), channel_id=1, replica_groups=mesh['kv'=16,'z'=16,'c'=2] {'kv'}, dimensions={0} | all-to-all | bytes 262144 | tf_op jit(solution)/shard_map/all_to_all | solution.py:19
  60.9 0.4 attend.1
  61.4 4.3 %all-gather.1 = bf16[512,256]{1,0:T(8,128)(2,1)S(1)} all-gather(bf16[256,256]{1,0:T(8,128)(2,1)S(1)} %attend.1), channel_id=3, replica_groups=mesh['kv'=16,'z'=16,'c'=2] {'c'}, dimensions={0}, use_global_device_ids=true | all-gather | bytes 393216 | tf_op jit(solution)/shard_map/all_gather | solution.py:29
  65.7 14.4 %all_to_all.43 = bf16[16,8,256]{2,1,0:T(8,128)(2,1)S(1)} all-to-all(bf16[16,8,256]{2,1,0:T(8,128)(2,1)S(1)} %dynamic-slice_reduce_fusion.1), channel_id=1, replica_groups=mesh['kv'=16,'z'=16,'c'=2] {'z'}, dimensions={0} | all-to-all | bytes 131072 | tf_op jit(solution)/shard_map/all_to_all | solution.py:19
  80.1 0.0 copy-start.5
  80.1 0.0 copy-start.4
  80.1 15.2 %all_to_all.44 = bf16[16,8,256]{2,1,0:T(8,128)(2,1)S(1)} all-to-all(bf16[16,8,256]{2,1,0:T(8,128)(2,1)S(1)} %broadcast_in_dim.36), channel_id=1, replica_groups=mesh['kv'=16,'z'=16,'c'=2] {'z'}, dimensions={0} | all-to-all | bytes 131072 | tf_op jit(solution)/shard_map/all_to_all | solution.py:19
  95.3 3.8 %all-gather.2 = bf16[32,8,256]{2,1,0:T(8,128)(2,1)S(1)} all-gather(bf16[16,8,256]{2,1,0:T(8,128)(2,1)S(1)} %all_to_all.44), channel_id=4, replica_groups=mesh['kv'=16,'z'=16,'c'=2] {'c'}, dimensions={0}, use_global_device_ids=true | all-gather | bytes 196608 | tf_op jit(solution)/shard_map/all_gather | solution.py:427
  99.2 0.4 gate.1
  99.5 12.3 %all_to_all.45 = bf16[16,16,768]{2,1,0:T(8,128)(2,1)S(1)} all-to-all(bf16[16,16,768]{2,1,0:T(8,128)(2,1)S(1)} %gate.1), channel_id=1, replica_groups=mesh['kv'=16,'z'=16,'c'=2] {'kv'}, dimensions={0} | all-to-all | bytes 786432 | tf_op jit(solution)/shard_map/all_to_all | solution.py:19
  111.9 0.1 convert_reduce_fusion
  111.9 0.2 fusion.5
  112.1 0.1 fusion.2
  112.3 10.1 %all_to_all.46 = bf16[16,16,344]{2,1,0:T(8,128)(2,1)S(1)} all-to-all(bf16[16,16,344]{2,1,0:T(8,128)(2,1)S(1)} %broadcast_in_dim.37), channel_id=1, replica_groups=mesh['kv'=16,'z'=16,'c'=2] {'kv'}, dimensions={0} | all-to-all | bytes 352256 | tf_op jit(solution)/shard_map/all_to_all | solution.py:19
  122.4 0.2 fusion
  122.6 4.2 %all-gather.3 = bf16[512,256]{0,1:T(8,128)(2,1)S(1)} all-gather(bf16[256,256]{0,1:T(8,128)(2,1)S(1)} %fusion), channel_id=5, replica_groups=mesh['kv'=16,'z'=16,'c'=2] {'c'}, dimensions={0}, use_global_device_ids=true | all-gather | bytes 393216 | tf_op jit(solution)/shard_map/all_gather | solution.py:29
  126.9 0.1 copy.24
  127.0 14.3 %all_to_all.47.recv_ref = bf16[16,8,256]{2,1,0:T(8,128)(2,1)S(1)} all-to-all(bf16[16,8,256]{2,1,0:T(8,128)(2,1)S(1)} %dynamic-slice_reduce_fusion), channel_id=1, replica_groups=mesh['kv'=16,'z'=16,'c'=2] {'z'}, dimensions={0} | all-to-all | bytes 131072 | tf_op jit(solution)/shard_map/all_to_all | solution.py:19
  141.3 0.8 finish.1
  (15 shorter events, 0.1 us)
Async XLA Ops:
  0.6 121.8 %copy-start = (bf16[344,256]{1,0:T(8,128)(2,1)S(1)}, bf16[344,256]{1,0:T(8,128)(2,1)}, u32[]{:S(2)}) copy-start(bf16[344,256]{1,0:T(8,128)(2,1)} %param.33) | copy-start | bytes 528388
  0.7 0.7 copy-start.10
  0.7 0.7 copy-start.16
  0.7 0.7 copy-start.12
  0.7 0.7 copy-start.14
  0.7 0.7 copy-start.15
  0.7 0.7 copy-start.11
  0.7 0.7 copy-start.13
  1.5 31.4 %copy-start.3 = (bf16[4096,32]{0,1:T(8,128)(2,1)S(1)}, bf16[4096,32]{0,1:T(8,128)(2,1)}, u32[]{:S(2)}) copy-start(bf16[4096,32]{0,1:T(8,128)(2,1)} %param.25) | copy-start | bytes 786436
  1.5 31.4 %copy-start.7 = (bf16[256,128]{1,0:T(8,128)(2,1)S(1)}, bf16[256,128]{1,0:T(8,128)(2,1)}, u32[]{:S(2)}) copy-start(bf16[256,128]{1,0:T(8,128)(2,1)} %wk_ref.1) | copy-start | bytes 196612
  1.5 31.4 %copy-start.8 = (bf16[256,128]{1,0:T(8,128)(2,1)S(1)}, bf16[256,128]{1,0:T(8,128)(2,1)}, u32[]{:S(2)}) copy-start(bf16[256,128]{1,0:T(8,128)(2,1)} %wv_ref.1) | copy-start | bytes 196612
  1.8 31.0 %copy-start.2 = (bf16[4096,32]{0,1:T(8,128)(2,1)S(1)}, bf16[4096,32]{0,1:T(8,128)(2,1)}, u32[]{:S(2)}) copy-start(bf16[4096,32]{0,1:T(8,128)(2,1)} %param.24) | copy-start | bytes 786436
  29.0 3.8 %copy-start.6 = (bf16[256,128]{1,0:T(8,128)(2,1)S(1)}, bf16[256,128]{1,0:T(8,128)(2,1)}, u32[]{:S(2)}) copy-start(bf16[256,128]{1,0:T(8,128)(2,1)} %wq_ref.1) | copy-start | bytes 196612
  33.7 16.4 %copy-start.1 = (f32[8,128,128]{2,1,0:T(8,128)S(1)}, f32[8,128,128]{2,1,0:T(8,128)}, u32[]{:S(2)}) copy-start(f32[8,128,128]{2,1,0:T(8,128)} %state_ref.1) | copy-start | bytes 1572868
  50.8 10.1 %copy-start.9 = (bf16[128,256]{1,0:T(8,128)(2,1)S(1)}, bf16[128,256]{1,0:T(8,128)(2,1)}, u32[]{:S(2)}) copy-start(bf16[128,256]{1,0:T(8,128)(2,1)} %w_ref.1) | copy-start | bytes 196612
  80.1 19.1 %copy-start.5 = (bf16[256,344]{0,1:T(8,128)(2,1)S(1)}, bf16[256,344]{0,1:T(8,128)(2,1)}, u32[]{:S(2)}) copy-start(bf16[256,344]{0,1:T(8,128)(2,1)} %param.32) | copy-start | bytes 528388
  80.1 19.1 %copy-start.4 = (bf16[256,344]{0,1:T(8,128)(2,1)S(1)}, bf16[256,344]{0,1:T(8,128)(2,1)}, u32[]{:S(2)}) copy-start(bf16[256,344]{0,1:T(8,128)(2,1)} %param.31) | copy-start | bytes 528388
